TPU v7x, 32 devices: a whole 2x2x4 slice. The times are simulated.
32 devices in a mesh: sp: 8 (over z, y), tp: 4 (over x, core).
Axes of the slice: x: 2, y: 2, z: 4, core: 2. Of those that a mesh axis runs over, the one named last changes fastest.
Arguments:
- mixer_input: bfloat16 [1024, 1024], P('sp', 'tp'), may hold values from -1800 to 1800
- time_step: float32 [2, 64], P(None, 'tp'), may hold values from 0 to 2, as said below
- damping: float32 [2, 1024, 64], P(None, 'sp', 'tp'), may hold values from 0 to 2
- input_map: bfloat16 [2, 2, 64, 64, 16], P(None, None, 'tp'), may hold values from -1 to 1
- readout: float32 [2, 2, 64, 16, 64], P(None, None, 'tp'), may hold values from -0.5 to 0.5
- skip_gain: float32 [1024], P('tp'), may hold values from -4 to 4
- out_gain: float32 [1024], P('tp'), may hold values from 0.1 to 1.9
- out_weight: bfloat16 [1024, 2048], replicated, may hold values from -0.1875 to 0.1875
- residual: bfloat16 [1024, 2048], P(('sp', 'tp')), may hold values from -6 to 6
- channel_gain: float32 [2048], replicated, may hold values from 0.1 to 1.9
- value_weight: bfloat16 [2048, 6144], P('sp', 'tp'), may hold values from -0.125 to 0.125
- gate_weight: bfloat16 [2048, 6144], P('sp', 'tp'), may hold values from -0.125 to 0.125
- value_taps: float32 [3, 6144], P(None, 'tp'), may hold values from -3 to 3
- gate_taps: float32 [3, 6144], P(None, 'tp'), may hold values from -3 to 3
- down_weight: bfloat16 [6144, 2048], P('tp', 'sp'), may hold values from -0.078125 to 0.078125
Outputs:
- output: bfloat16 [1024, 2048], P(('sp', 'tp'))
Inputs may be any that keep to these rules, and one draw needn't show every extreme that they name: `time_step`: positive.
All inputs are finite; a program needn't handle non-finite values.
Results may differ from a plain program's by a relative error of at most 0.017.
Values may be sent and summed in bfloat16 or wider, within the bound.
No kernel may reach another device: no remote copies, remote signals or barrier semaphores. Data moves between devices by JAX's collectives and lax.ppermute only.
A program may use at most 128 MiB of HBM per device.

v0:
```python
import math

import jax
import jax.numpy as jnp
from jax import lax
from jax.sharding import PartitionSpec as P

norm_eps = 1e-06
highest = lax.Precision.HIGHEST


def carried_in(value, axis, join, neutral, backward):
    count, mine = (lax.axis_size(axis), lax.axis_index(axis))
    pieces = jax.tree.map(lambda part: lax.all_gather(part, axis), value)
    if backward:
        pieces = jax.tree.map(lambda part: part[::-1], pieces)
        mine = count - 1 - mine
    total = jax.tree.map(
        lambda part, zero: jnp.full_like(part, 0) + jnp.asarray(zero, part.dtype), value, neutral
    )

    def step(position, total):
        longer = join(total, jax.tree.map(lambda part: part[position], pieces))
        return jax.tree.map(lambda new, old: jnp.where(position < mine, new, old), longer, total)

    return lax.fori_loop(0, count - 1, step, total)


def with_halo(cells, sides, width):
    for axis, dim in sides:
        count = lax.axis_size(axis)
        ends = count - 1
        head = lax.slice_in_dim(cells, 0, width, axis=dim)
        tail = lax.slice_in_dim(cells, cells.shape[dim] - width, cells.shape[dim], axis=dim)
        cells = jnp.concatenate(
            [
                lax.ppermute(tail, axis, [(i, (i + 1) % count) for i in range(ends)]),
                cells,
                lax.ppermute(head, axis, [((i + 1) % count, i) for i in range(ends)]),
            ],
            axis=dim,
        )
    return cells


def combine(earlier, latter):
    prod_real = latter[0] * earlier[0] - latter[1] * earlier[1]
    prod_imag = latter[0] * earlier[1] + latter[1] * earlier[0]
    sum_real = latter[0] * earlier[2] - latter[1] * earlier[3] + latter[2]
    sum_imag = latter[0] * earlier[3] + latter[1] * earlier[2] + latter[3]
    return (prod_real, prod_imag, sum_real, sum_imag)


def moved_rows(values, offset, filler_value, backward):
    filler = jnp.full((offset, values.shape[1]), filler_value, jnp.float32)
    if backward:
        return jnp.concatenate((values[offset:], filler), axis=0)
    return jnp.concatenate((filler, values[:-offset]), axis=0)


def prefix_rows(elements, backward):
    row_count = elements[0].shape[0]
    fills = (1.0, 0.0, 0.0, 0.0)
    offset = 1
    while offset < row_count:
        earlier = tuple(
            (moved_rows(elements[index], offset, fills[index], backward) for index in range(4))
        )
        elements = combine(earlier, elements)
        offset = offset * 2
    return elements


def mixer_branch(mixer_input, time_step, damping, input_map, readout):
    tok_rows = mixer_input.shape[0]
    group_count = time_step.shape[1]
    states = input_map.shape[3]
    channels = input_map.shape[4]
    flat_width = group_count * states
    frequency = math.pi * jnp.arange(states, dtype=jnp.float32)
    ones_narrow = jnp.eye(group_count, dtype=jnp.bfloat16)
    ones_wide = jnp.eye(group_count, dtype=jnp.float32)
    sign_pair = jnp.array([1.0, -1.0], jnp.float32)
    mixed_sum = jnp.zeros((tok_rows, group_count * channels), jnp.float32)
    for direction in range(2):
        step_size = time_step[direction]
        rotation = (step_size[:, None] * frequency[None, :]).reshape(flat_width)
        in_scale = jnp.repeat(jnp.sqrt(-jnp.expm1(-step_size)), states)
        magnitude = jnp.repeat(
            jnp.exp(-0.5 * step_size[None, :] - damping[direction]), states, axis=1
        )
        decay_real = magnitude * jnp.cos(rotation)[None, :]
        decay_imag = magnitude * jnp.sin(rotation)[None, :]
        in_block = jnp.einsum("pgnh,gk->ghpkn", input_map[direction], ones_narrow).reshape(
            group_count * channels, 2 * flat_width
        )
        projected = jnp.dot(mixer_input, in_block, preferred_element_type=jnp.float32)
        drive_real = projected[:, :flat_width] * in_scale[None, :]
        drive_imag = projected[:, flat_width:] * in_scale[None, :]
        backward = direction == 1
        scanned = prefix_rows((decay_real, decay_imag, drive_real, drive_imag), backward)
        last_row = 0 if backward else tok_rows - 1
        totals = (
            scanned[0][last_row],
            scanned[1][last_row],
            scanned[2][last_row],
            scanned[3][last_row],
        )
        zero_row = jnp.zeros((flat_width,), jnp.float32)
        identity = (jnp.ones((flat_width,), jnp.float32), zero_row, zero_row, zero_row)
        carried = carried_in(totals, "sp", combine, identity, backward)
        state_real = (
            scanned[2] + scanned[0] * carried[2][None, :] - scanned[1] * carried[3][None, :]
        )
        state_imag = (
            scanned[3] + scanned[0] * carried[3][None, :] + scanned[1] * carried[2][None, :]
        )
        signed = readout[direction] * sign_pair[:, None, None, None]
        out_block = jnp.einsum("pghn,gk->pgnkh", signed, ones_wide, precision=highest).reshape(
            2 * flat_width, group_count * channels
        )
        both_parts = jnp.concatenate((state_real, state_imag), axis=1)
        mixed_sum = mixed_sum + jnp.dot(both_parts, out_block, precision=highest)
    return mixed_sum


def body(
    mixer_input,
    time_step,
    damping,
    input_map,
    readout,
    skip_gain,
    out_gain,
    out_weight,
    residual,
    channel_gain,
    value_weight,
    gate_weight,
    value_taps,
    gate_taps,
    down_weight,
):
    tok_rows, local_width = mixer_input.shape
    tp_count = lax.axis_size("tp")
    mixed_y = mixer_branch(mixer_input, time_step, damping, input_map, readout)
    mixed_y = mixed_y + skip_gain[None, :] * mixer_input.astype(jnp.float32)
    square_sum = lax.psum(jnp.sum(mixed_y * mixed_y, axis=1), "tp")
    inverse = lax.rsqrt(square_sum / (local_width * tp_count) + norm_eps)
    normed_mix = (mixed_y * inverse[:, None] * out_gain[None, :]).astype(jnp.bfloat16)
    token_block = lax.all_to_all(normed_mix, "tp", split_axis=0, concat_axis=1, tiled=True)
    mixed_rows = jnp.dot(token_block, out_weight, preferred_element_type=jnp.float32)
    hidden_state = (residual.astype(jnp.float32) + mixed_rows).astype(jnp.bfloat16)
    state_wide = hidden_state.astype(jnp.float32)
    scale_rows = lax.rsqrt(jnp.mean(state_wide * state_wide, axis=1, keepdims=True) + norm_eps)
    normed = (state_wide * scale_rows * channel_gain[None, :]).astype(jnp.bfloat16)
    block_rows = lax.all_gather(normed, "tp", axis=0, tiled=True)
    hidden_width = value_weight.shape[1]
    value_up = jnp.dot(
        block_rows,
        lax.all_gather(value_weight, "sp", axis=0, tiled=True),
        preferred_element_type=jnp.float32,
    )
    gate_up = jnp.dot(
        block_rows,
        lax.all_gather(gate_weight, "sp", axis=0, tiled=True),
        preferred_element_type=jnp.float32,
    )
    both_up = jnp.concatenate((value_up.astype(jnp.bfloat16), gate_up.astype(jnp.bfloat16)), axis=1)
    padded = with_halo(both_up, (("sp", 0),), 1)
    tap_table = jnp.concatenate((value_taps, gate_taps), axis=1)
    convolved = (
        tap_table[0] * padded[:-2].astype(jnp.float32)
        + tap_table[1] * padded[1:-1].astype(jnp.float32)
        + tap_table[2] * padded[2:].astype(jnp.float32)
    )
    hidden = (convolved[:, :hidden_width] * jax.nn.silu(convolved[:, hidden_width:])).astype(
        jnp.bfloat16
    )
    down_full = lax.all_gather(down_weight, "sp", axis=1, tiled=True)
    summed = lax.psum_scatter(
        jnp.dot(hidden, down_full, preferred_element_type=jnp.float32).astype(jnp.bfloat16),
        "tp",
        scatter_dimension=0,
        tiled=True,
    ).astype(jnp.float32)
    return (state_wide + summed).astype(jnp.bfloat16)


def solution(mesh):
    in_specs = (
        P("sp", "tp"),
        P(None, "tp"),
        P(None, "sp", "tp"),
        P(None, None, "tp", None, None),
        P(None, None, "tp", None, None),
        P("tp"),
        P("tp"),
        P(),
        P(("sp", "tp"), None),
        P(),
        P("sp", "tp"),
        P("sp", "tp"),
        P(None, "tp"),
        P(None, "tp"),
        P("tp", "sp"),
    )
    out_specs = P(("sp", "tp"), None)
    return jax.shard_map(body, mesh=mesh, in_specs=in_specs, out_specs=out_specs, check_vma=False)
```

profile of v0, /device:TPU:0, one launch (start us, length us, event | category | flops | bytes accessed | tf_op | source)
XLA Modules:
  0.0 438.9 jit_solution(8273349476924241032)
XLA Ops:
  51.3 33.5 %all-gather.4 = f32[8,1,1024]{2,1,0:T(1,128)S(1)} all-gather(f32[1,1,1024]{2,1,0:T(1,128)S(1)} %slice_bitcast_fusion.5), channel_id=1, replica_groups=mesh['sp'=8,'tp'=4] {'sp'}, dimensions={0}, use_global_device_ids=true | all-gather | bytes 36864 | tf_op jit(solution)/shard_map/all_gather | solution.py:14
  85.4 3.9 rev.12
  89.3 31.1 %all-gather.5 = f32[8,1,1024]{2,1,0:T(1,128)S(1)} all-gather(f32[1,1,1024]{2,1,0:T(1,128)S(1)} %slice_bitcast_fusion.4), channel_id=1, replica_groups=mesh['sp'=8,'tp'=4] {'sp'}, dimensions={0}, use_global_device_ids=true | all-gather | bytes 36864 | tf_op jit(solution)/shard_map/all_gather | solution.py:14
  121.1 3.9 rev.13
  125.8 31.4 %all-gather.7 = f32[8,1,1024]{2,1,0:T(1,128)S(1)} all-gather(f32[1,1,1024]{2,1,0:T(1,128)S(1)} %slice_bitcast_fusion.2), channel_id=1, replica_groups=mesh['sp'=8,'tp'=4] {'sp'}, dimensions={0}, use_global_device_ids=true | all-gather | bytes 36864 | tf_op jit(solution)/shard_map/all_gather | solution.py:14
  157.8 3.9 rev.15
  162.5 32.2 %all-gather.6 = f32[8,1,1024]{2,1,0:T(1,128)S(1)} all-gather(f32[1,1,1024]{2,1,0:T(1,128)S(1)} %slice_bitcast_fusion.3), channel_id=1, replica_groups=mesh['sp'=8,'tp'=4] {'sp'}, dimensions={0}, use_global_device_ids=true | all-gather | bytes 36864 | tf_op jit(solution)/shard_map/all_gather | solution.py:14
  195.3 3.9 rev.14
  201.1 31.2 %all-gather.3 = f32[8,1,1024]{2,1,0:T(1,128)S(1)} all-gather(f32[1,1,1024]{2,1,0:T(1,128)S(1)} %slice_bitcast_fusion.6), channel_id=1, replica_groups=mesh['sp'=8,'tp'=4] {'sp'}, dimensions={0}, use_global_device_ids=true | all-gather | bytes 36864 | tf_op jit(solution)/shard_map/all_gather | solution.py:14
  232.3 31.5 %all-gather.1 = f32[8,1,1024]{2,1,0:T(1,128)S(1)} all-gather(f32[1,1,1024]{2,1,0:T(1,128)S(1)} %slice_bitcast_fusion.8), channel_id=1, replica_groups=mesh['sp'=8,'tp'=4] {'sp'}, dimensions={0}, use_global_device_ids=true | all-gather | bytes 36864 | tf_op jit(solution)/shard_map/all_gather | solution.py:14
  263.8 33.0 %all-gather = f32[8,1,1024]{2,1,0:T(1,128)S(1)} all-gather(f32[1,1,1024]{2,1,0:T(1,128)S(1)} %slice_bitcast_fusion.9), channel_id=1, replica_groups=mesh['sp'=8,'tp'=4] {'sp'}, dimensions={0}, use_global_device_ids=true | all-gather | bytes 36864 | tf_op jit(solution)/shard_map/all_gather | solution.py:14
  296.9 35.1 %all-gather.2 = f32[8,1,1024]{2,1,0:T(1,128)S(1)} all-gather(f32[1,1,1024]{2,1,0:T(1,128)S(1)} %slice_bitcast_fusion.7), channel_id=1, replica_groups=mesh['sp'=8,'tp'=4] {'sp'}, dimensions={0}, use_global_device_ids=true | all-gather | bytes 36864 | tf_op jit(solution)/shard_map/all_gather | solution.py:14
  332.4 4.5 %multiply_bitcast_fusion = (f32[2,16,64,16,16]{2,1,0,4,3:T(8,128)}, f32[2,16,64,16,16]{2,1,0,4,3:T(8,128)}) fusion(f32[16,2,16,64]{3,0,1,2:T(8,128)S(1)} %copy.41, f32[16,16]{0,1:T(8,128)S(1)} %copy-done.21, f32[16,2,16,64]{3,0,1,2:T(8,128)S(1)} %copy.37), kind=kLoop, calls=%fused_computation.12 | loop fusion | flops 1048576 | bytes 4457472 | tf_op jit(solution)/shard_map/pghn,gk->pgnkh/transpose | solution.py:119
  336.8 5.2 %reshape.94 = f32[2048,256]{0,1:T(8,128)} reshape(f32[2,16,64,16,16]{2,1,0,4,3:T(8,128)} %get-tuple-element.455) | data formatting | bytes 4194304 | tf_op jit(solution)/shard_map/reshape | solution.py:119
  342.1 3.7 reshape.97
  350.5 11.4 %while.33 = (s32[]{:T(128)}, f32[1024]{0:T(1024)S(1)}, f32[1024]{0:T(1024)S(1)}, s32[]{:T(128)}, f32[8,1024]{1,0:T(8,128)}, /*index=5*/f32[8,1024]{1,0:T(8,128)}...) while((s32[]{:T(128)}, f32[1024]{0:T(1024)S(1)}, f32[1024]{0:T(1024)S(1)}, ...), condition=%wide.region_3.4_spmd.clone, body=%wide.region_2.3_spmd.clone.sunk | while | flops 12292 | bytes 65665 | solution.py:26
  365.7 5.8 %psum.7 = f32[128]{0:T(128)S(1)} all-reduce(f32[128]{0:T(128)S(1)} %get-tuple-element.470), channel_id=1, replica_groups=mesh['sp'=8,'tp'=4] {'tp'}, use_global_device_ids=true, to_apply=%region_5.6 | all-reduce | flops 128 | bytes 1024 | tf_op jit(solution)/shard_map/psum | solution.py:148
  375.5 4.0 all-to-all-done
  382.8 6.6 %all_gather.44 = bf16[128,2048]{1,0:T(8,128)(2,1)S(1)} all-gather(bf16[32,2048]{1,0:T(8,128)(2,1)S(1)} %multiply_convert_fusion), channel_id=1, replica_groups=mesh['sp'=8,'tp'=4] {'tp'}, dimensions={0}, use_global_device_ids=true | all-gather | bytes 655360 | tf_op jit(solution)/shard_map/all_gather | solution.py:157
  389.4 3.8 convolution_convert_fusion.1
  393.2 3.8 convolution_convert_fusion.2
  399.7 4.2 collective-permute-done.1
  404.5 4.6 %convolution_convert_fusion = bf16[128,2048]{1,0:T(8,128)(2,1)} fusion(bf16[1536,2048]{1,0:T(8,128)(2,1)} %all-gather.16.cloned.1.call-done, f32[128,3072]{1,0:T(8,128)S(1)} %multiply_add_fusion), kind=kOutput, calls=%fused_computation.16 | convolution fusion | flops 806748160 | bytes 8388608 | tf_op jit(solution)/shard_map/dot_general | solution.py:182
  409.1 21.7 %reduce-scatter.2.cloned.1.call-done = bf16[32,2048]{1,0:T(8,128)(2,1)} async-done(((bf16[128,2048]{1,0:T(8,128)(2,1)}), bf16[32,2048]{1,0:T(8,128)(2,1)}) %reduce-scatter.2.cloned.1.call-update) | async-done | bytes 131088 | tf_op jit(solution)/shard_map/reduce_scatter | solution.py:181
  (261 shorter events, 82.1 us)
Async XLA Ops:
  6.5 382.8 %all-gather.14.cloned.1.call-start = ((), (), s32[]{:S(2)}) async-start(), calls=%async_computation.3 | async-start | bytes 7077888 | tf_op jit(solution)/shard_map/all_gather | solution.py:166
  7.3 385.9 %all-gather.12.cloned.1.call-start = ((), (), s32[]{:S(2)}) async-start(), calls=%async_computation.2 | async-start | bytes 7077888 | tf_op jit(solution)/shard_map/all_gather | solution.py:161
  8.0 396.5 %all-gather.16.cloned.1.call-start = ((), (), s32[]{:S(2)}) async-start(), calls=%async_computation.4 | async-start | bytes 7077888 | tf_op jit(solution)/shard_map/all_gather | solution.py:180
  50.2 149.1 %copy-start.6 = (f32[128,1024]{1,0:T(8,128)S(1)}, f32[128,1024]{1,0:T(8,128)}, u32[]{:S(2)}) copy-start(f32[128,1024]{1,0:T(8,128)} %fusion.28) | copy-start | bytes 1572868
  50.2 149.2 %copy-start.15 = (f32[96,1024]{1,0:T(8,128)S(1)}, f32[96,1024]{1,0:T(8,128)}, u32[]{:S(2)}) copy-start(f32[96,1024]{1,0:T(8,128)} %slice.352) | copy-start | bytes 1179652
  51.3 148.0 %copy-start.10 = (f32[128,1024]{1,0:T(8,128)}, f32[128,1024]{1,0:T(8,128)S(1)}, u32[]{:S(2)}) copy-start(f32[128,1024]{1,0:T(8,128)S(1)} %get-tuple-element.429) | copy-start | bytes 1572868
  51.3 148.0 %copy-start.12 = (f32[128,1024]{1,0:T(8,128)}, f32[128,1024]{1,0:T(8,128)S(1)}, u32[]{:S(2)}) copy-start(f32[128,1024]{1,0:T(8,128)S(1)} %get-tuple-element.430) | copy-start | bytes 1572868
  200.6 96.2 %copy-start.8 = (f32[128,1024]{1,0:T(8,128)}, f32[128,1024]{1,0:T(8,128)S(1)}, u32[]{:S(2)}) copy-start(f32[128,1024]{1,0:T(8,128)S(1)} %get-tuple-element.396) | copy-start | bytes 1572868
  200.7 131.3 %copy-start.18 = (f32[2,2,16,16,64]{4,3,2,1,0:T(8,128)S(1)}, f32[2,2,16,16,64]{4,3,2,1,0:T(8,128)}, u32[]{:S(2)}) copy-start(f32[2,2,16,16,64]{4,3,2,1,0:T(8,128)} %param.24) | copy-start | bytes 786436
  200.7 131.3 %copy-start.30 = (f32[2]{0:T(128)S(1)}, f32[2]{0:T(128)}, u32[]{:S(2)}) copy-start(f32[2]{0:T(128)} %constant.89.clone) | copy-start | bytes 28
  201.0 135.8 %copy-start.13 = (f32[128,1024]{1,0:T(8,128)}, f32[128,1024]{1,0:T(8,128)S(1)}, u32[]{:S(2)}) copy-start(f32[128,1024]{1,0:T(8,128)S(1)} %get-tuple-element.432) | copy-start | bytes 1572868
  201.0 135.8 %copy-start.14 = (f32[128,1024]{1,0:T(8,128)}, f32[128,1024]{1,0:T(8,128)S(1)}, u32[]{:S(2)}) copy-start(f32[128,1024]{1,0:T(8,128)S(1)} %get-tuple-element.442) | copy-start | bytes 1572868
  201.0 131.3 %copy-start.21 = (f32[16,16]{0,1:T(8,128)S(1)}, f32[16,16]{0,1:T(8,128)}, u32[]{:S(2)}) copy-start(f32[16,16]{0,1:T(8,128)} %fusion.55) | copy-start | bytes 3076
  347.9 14.0 %copy-start.7 = (f32[128,1024]{1,0:T(8,128)S(1)}, f32[128,1024]{1,0:T(8,128)}, u32[]{:S(2)}) copy-start(f32[128,1024]{1,0:T(8,128)} %get-tuple-element.375) | copy-start | bytes 1572868
  347.9 14.0 %copy-start.11 = (f32[128,1024]{1,0:T(8,128)S(1)}, f32[128,1024]{1,0:T(8,128)}, u32[]{:S(2)}) copy-start(f32[128,1024]{1,0:T(8,128)} %copy-done.10) | copy-start | bytes 1572868
  350.4 12.9 %copy-start.17 = (bf16[128,256]{1,0:T(8,128)(2,1)S(1)}, bf16[128,256]{1,0:T(8,128)(2,1)}, u32[]{:S(2)}) copy-start(bf16[128,256]{1,0:T(8,128)(2,1)} %param.20) | copy-start | bytes 196612
  350.4 12.9 %copy-start.28 = (f32[256]{0:T(256)S(1)}, f32[256]{0:T(256)}, u32[]{:S(2)}) copy-start(f32[256]{0:T(256)} %param.25) | copy-start | bytes 3076
  363.3 12.2 %copy-start.22 = (f32[3,1536]{1,0:T(4,128)S(1)}, f32[3,1536]{1,0:T(4,128)}, u32[]{:S(2)}) copy-start(f32[3,1536]{1,0:T(4,128)} %param.32) | copy-start | bytes 55300
  363.3 12.2 %copy-start.23 = (f32[3,1536]{1,0:T(4,128)S(1)}, f32[3,1536]{1,0:T(4,128)}, u32[]{:S(2)}) copy-start(f32[3,1536]{1,0:T(4,128)} %param.33) | copy-start | bytes 55300
  363.3 16.2 %copy-start.20 = (bf16[32,2048]{1,0:T(8,128)(2,1)S(1)}, bf16[32,2048]{1,0:T(8,128)(2,1)}, u32[]{:S(2)}) copy-start(bf16[32,2048]{1,0:T(8,128)(2,1)} %param.28) | copy-start | bytes 393220
  372.1 7.4 %all-to-all-start = ((bf16[4,32,256]{2,1,0:T(8,128)(2,1)}), bf16[4,32,256]{2,1,0:T(8,128)(2,1)S(1)}, u32[]{:S(2)}, u32[]{:S(2)}) async-start(bf16[4,32,256]{2,1,0:T(8,128)(2,1)} %bitcast.30), calls=%async_computation | async-start | bytes 131072 | tf_op jit(solution)/shard_map/all_to_all | solution.py:151
  375.4 55.4 %reduce-scatter.2.cloned.1.call-start = ((), (), s32[]{:S(2)}) async-start(), calls=%async_computation.5 | async-start | bytes 655360 | tf_op jit(solution)/shard_map/reduce_scatter | solution.py:181
  397.0 2.7 collective-permute-start
  398.3 5.6 %collective-permute-start.1 = (bf16[1,3072]{1,0:T(2,128)(2,1)S(1)}, bf16[1,3072]{1,0:T(2,128)(2,1)S(1)}, u32[]{:S(2)}, u32[]{:S(2)}) collective-permute-start(bf16[1,3072]{1,0:T(2,128)(2,1)S(1)} %get-tuple-element.444), channel_id=1, source_target_pairs={{4,0},{8,4},{12,8},{16,12},{20,16},{24,20},{28,24},{5,1},{9,5},{13... | collective-permute-start | bytes 18440 | tf_op jit(solution)/shard_map/ppermute | solution.py:39
  (14 other events, 40.3 us)
Sparse Core Ops, SparseCore 0:
  9.5 102.3 all-gather.13
  114.1 97.8 all-gather.11
  214.0 98.5 all-gather.15
  409.3 21.5 reduce-scatter.1
where the time goes:
time: 442 us; the launch traced here: 439 us
  blocking collectives  271 us (61%)
  local copies, waits for them, and re-layouts  60 us (14%)
  other arithmetic  33 us (7%)
  waiting for transfers between devices  32.1 us (7%)
  matrix products  21.7 us (5%)
  between operations  14.2 us (3%)
  starting transfers between devices  5.99 us (1%)
    all_gather x8, blocking collectives, carried_in(): pieces = jax.tree.map(lambda part: lax.all_gather(part, axis), value)  259 us
    reduce_scatter x1, waiting for transfers between devices, body(): lax.psum_scatter(jnp.dot(hidden, down_full, preferred_element_type=jnp.fl...  21.7 us
    rev x4, local copies, waits for them, and re-layouts, carried_in(): pieces = jax.tree.map(lambda part: part[::-1], pieces)  15.8 us
    add x14, other arithmetic, combine(): sum_real = latter[0] * earlier[2] - latter[1] * earlier[3] + latter[2]  11.8 us
    dynamic_slice x28, local copies, waits for them, and re-layouts, step(): longer = join(total, jax.tree.map(lambda part: part[position], pieces))  11.2 us
    reshape x2, local copies, waits for them, and re-layouts, mixer_branch(): jnp.einsum('pghn,gk->pgnkh', signed, ones_wide, precision=highest)  8.88 us
  transfers between devices with their start and end apart: 7, of which 4 were waited for; matrix products, arithmetic and copies ran while one was open for 24% of the time, Pallas kernels for 0%

commit v1 on v0

v1 whole, which is shorter than its diff:
```python
import math

import jax
import jax.numpy as jnp
from jax import lax
from jax.experimental import pallas as pl
from jax.experimental.pallas import tpu as pltpu
from jax.sharding import PartitionSpec as P

norm_eps = 1e-06
highest = lax.Precision.HIGHEST
f32 = jnp.float32
bf16 = jnp.bfloat16


def split2(a):
    top = a.astype(bf16)
    return top, (a - top.astype(f32)).astype(bf16)


def dot3(a, b):
    a0, a1 = split2(a)
    b0, b1 = split2(b)
    total = jnp.dot(a0, b0, preferred_element_type=f32)
    total += jnp.dot(a0, b1, preferred_element_type=f32)
    return total + jnp.dot(a1, b0, preferred_element_type=f32)


def cos_sin(coarse, fine, count):
    first = coarse * count
    first = first - jnp.floor(first + 0.5)
    turn = first + fine * count
    half = jnp.floor(2.0 * turn + 0.5)
    angle = (2.0 * math.pi) * (turn - 0.5 * half)
    odd = half - 2.0 * jnp.floor(0.5 * half)
    sign = 1.0 - 2.0 * odd
    z = angle * angle
    sine = jnp.full_like(z, -1.0 / 39916800.0)
    for c in (1.0 / 362880.0, -1.0 / 5040.0, 1.0 / 120.0, -1.0 / 6.0, 1.0):
        sine = sine * z + c
    cosine = jnp.full_like(z, 1.0 / 479001600.0)
    for c in (-1.0 / 3628800.0, 1.0 / 40320.0, -1.0 / 720.0, 1.0 / 24.0, -0.5, 1.0):
        cosine = cosine * z + c
    return cosine * sign, sine * (angle * sign)


def iota(shape, dim):
    return lax.broadcasted_iota(jnp.int32, shape, dim)


def turns_of(states, rows, backward):
    when = iota((states, rows), 1)
    when = rows - 1 - when if backward else when
    return (iota((states, rows), 0) * when).astype(f32)


def local_kernel(scal, xt, damp, in_map, readout, yt, ends, rows_a):
    groups, rows = damp.shape[1], damp.shape[2]
    states, chans = in_map.shape[3], in_map.shape[4]
    part, quarter = states // 2, 2 * groups
    lane = iota((part, ends.shape[1]), 1)
    row_id, col_id = iota((rows, rows), 0), iota((rows, rows), 1)
    kept = (row_id <= col_id, row_id >= col_id)
    for k in range(2):
        rows_a[k] = jnp.dot(damp[k], kept[k].astype(f32), precision=highest)
    counts = [turns_of(states, rows, k == 1) for k in range(2)]

    def group(g, held):
        at = pl.ds(pl.multiple_of(g * chans, chans), chans)
        x = xt[at, :]
        total = jnp.zeros((chans, rows), f32)
        for k in range(2):
            cosine, sine = cos_sin(scal[0, k, g], scal[1, k, g], counts[k])
            scale = scal[2, k, g]
            drive_r = jnp.dot(in_map[k, 0, g], x, preferred_element_type=f32) * scale
            drive_i = jnp.dot(in_map[k, 1, g], x, preferred_element_type=f32) * scale
            turned = jnp.concatenate(
                (cosine * drive_r + sine * drive_i, cosine * drive_i - sine * drive_r), axis=0
            )
            across = jnp.broadcast_to(rows_a[k, pl.ds(g, 1), :], (rows, rows))
            decay = jnp.exp(jnp.where(kept[k], across.T - across, -1e30))
            z = dot3(turned, decay)
            z_r, z_i = z[:states], z[states:]
            s_r = cosine * z_r - sine * z_i
            s_i = cosine * z_i + sine * z_r
            total += dot3(readout[k, 0, g], s_r) - dot3(readout[k, 1, g], s_i)
            last = 0 if k else rows - 1
            for p, s in enumerate((s_r, s_i)):
                col = s[:, last : last + 1]
                for half in range(2):
                    spot = (half * 2 + p) * quarter + k * groups + g
                    held = jnp.where(lane == spot, col[half * part : (half + 1) * part], held)
        yt[at, :] = total
        return held

    held = lax.fori_loop(0, groups, group, jnp.zeros((part, ends.shape[1]), f32))
    ends[...] = held


def carry_kernel(scal, place, xt, rows_a, lanes, every, readout, yt, skip, gain, out):
    groups, rows = rows_a.shape[1], rows_a.shape[2]
    chans, states = readout.shape[3], readout.shape[4]
    blocks = every.shape[0]
    part, quarter = states // 2, 2 * groups
    mine = place[0]
    number = iota((states, quarter), 0).astype(f32)
    backward = iota((states, quarter), 1) >= groups
    coarse, fine = lanes[0:1, :], lanes[1:2, :]
    far_r, far_i = cos_sin(coarse, fine, number * rows)
    near_r, near_i = cos_sin(coarse, fine, number)
    def piece(b, p):
        ref = every.at[b]
        return jnp.concatenate(
            [ref[:part, (h * 2 + p) * quarter : (h * 2 + p + 1) * quarter] for h in range(2)], axis=0
        )

    c_r = jnp.zeros((states, quarter), f32)
    c_i = jnp.zeros((states, quarter), f32)
    for b in range(blocks - 1):
        other = blocks - 1 - b
        e_r = jnp.where(backward, piece(other, 0), piece(b, 0))
        e_i = jnp.where(backward, piece(other, 1), piece(b, 1))
        span = jnp.where(
            backward[:1], every[other, part : part + 1, :quarter], every[b, part : part + 1, :quarter]
        )
        fade = jnp.exp(-span)
        n_r = fade * (far_r * c_r - far_i * c_i) + e_r
        n_i = fade * (far_r * c_i + far_i * c_r) + e_i
        place_in = jnp.where(backward, blocks - 1 - mine, mine)
        c_r = jnp.where(b < place_in, n_r, c_r)
        c_i = jnp.where(b < place_in, n_i, c_i)
    w_r = near_r * c_r - near_i * c_i
    w_i = near_r * c_i + near_i * c_r
    counts = [turns_of(states, rows, k == 1) for k in range(2)]
    squares = jnp.zeros((8, rows), f32)
    for g in range(groups):
        at = pl.ds(g * chans, chans)
        total = yt[at, :] + skip[at, :] * xt[at, :].astype(f32)
        for k in range(2):
            cosine, sine = cos_sin(scal[0, k, g], scal[1, k, g], counts[k])
            l = k * groups + g
            a, b = w_r[:, l : l + 1], w_i[:, l : l + 1]
            fade = jnp.exp(-rows_a[k, g : g + 1, :])
            s_r = (cosine * a - sine * b) * fade
            s_i = (cosine * b + sine * a) * fade
            total += dot3(readout[k, 0, g], s_r) - dot3(readout[k, 1, g], s_i)
        for r in range(0, chans, 8):
            squares += total[r : r + 8] * total[r : r + 8]
        out[at, :] = (total * gain[at, :]).astype(bf16)
    square = jnp.sum(squares, axis=0, keepdims=True)
    top = square.astype(bf16)
    rest = square - top.astype(f32)
    mid = rest.astype(bf16)
    low = (rest - mid.astype(f32)).astype(bf16)
    extra = out.shape[0] - groups * chans
    which = iota((extra, rows), 0)
    tail = jnp.where(which == 0, top.astype(f32), jnp.where(which == 1, mid.astype(f32), low.astype(f32)))
    tail = jnp.where(which < 3, tail, 0.0)
    out[pl.ds(groups * chans, extra), :] = tail.astype(bf16)


square_rows = 16


def vmem(count):
    return [pl.BlockSpec(memory_space=pltpu.VMEM)] * count


def mixer_local(mixer_input, time_step, damping, input_map, readout):
    rows, width = mixer_input.shape
    groups = time_step.shape[1]
    states = input_map.shape[3]
    half_step = 0.5 * time_step
    coarse = jnp.floor(half_step * 2048.0) / 2048.0
    scal = jnp.stack((coarse, half_step - coarse, jnp.sqrt(-jnp.expm1(-time_step))))
    damp = jnp.swapaxes(damping, 1, 2) + half_step[:, :, None]
    xt = mixer_input.T
    lanes = 8 * groups
    smem = pl.BlockSpec(memory_space=pltpu.SMEM)
    yt, ends, rows_a = pl.pallas_call(
        local_kernel,
        out_shape=(
            jax.ShapeDtypeStruct((width, rows), f32),
            jax.ShapeDtypeStruct((states // 2, lanes), f32),
            jax.ShapeDtypeStruct(damp.shape, f32),
        ),
        in_specs=[smem] + vmem(4),
        out_specs=tuple(vmem(3)),
        name="mixer_local",
    )(scal, xt, damp, input_map, readout)
    span = jnp.sum(damp, axis=2).reshape(1, -1)
    extra = jnp.zeros((8, lanes), f32).at[:1, : span.shape[1]].set(span)
    return scal, xt, yt, rows_a, jnp.concatenate((ends, extra), axis=0)


def mixer_carried(scal, xt, yt, rows_a, every, readout, skip_gain, out_gain):
    width, rows = xt.shape
    smem = pl.BlockSpec(memory_space=pltpu.SMEM)
    place = lax.axis_index("sp").reshape(1)
    lanes = scal[:2].reshape(2, -1)
    return pl.pallas_call(
        carry_kernel,
        out_shape=jax.ShapeDtypeStruct((width + square_rows, rows), bf16),
        in_specs=[smem, smem] + vmem(8),
        out_specs=pl.BlockSpec(memory_space=pltpu.VMEM),
        name="mixer_carried",
    )(scal, place, xt, rows_a, lanes, every, readout, yt, skip_gain[:, None], out_gain[:, None])


def with_halo(cells, axis):
    count = lax.axis_size(axis)
    return jnp.concatenate(
        [
            lax.ppermute(cells[-1:], axis, [(i, i + 1) for i in range(count - 1)]),
            cells,
            lax.ppermute(cells[:1], axis, [(i + 1, i) for i in range(count - 1)]),
        ],
        axis=0,
    )


def body(
    mixer_input,
    time_step,
    damping,
    input_map,
    readout,
    skip_gain,
    out_gain,
    out_weight,
    residual,
    channel_gain,
    value_weight,
    gate_weight,
    value_taps,
    gate_taps,
    down_weight,
):
    tp_count, sp_count = lax.axis_size("tp"), lax.axis_size("sp")
    tok_rows, local_width = mixer_input.shape
    residual_rows = lax.all_gather(residual, "tp", axis=0, tiled=True)
    scal, xt, yt, rows_a, ends = mixer_local(mixer_input, time_step, damping, input_map, readout)
    every = lax.all_to_all(
        jnp.broadcast_to(ends[None], (sp_count,) + ends.shape), "sp", 0, 0, tiled=True
    )
    mixed = mixer_carried(scal, xt, yt, rows_a, every, readout, skip_gain, out_gain)
    mixed = lax.all_gather(mixed, "tp", axis=0)
    squares = jnp.sum(mixed[:, local_width:].astype(f32), axis=(0, 1))
    inverse = lax.rsqrt(squares / (local_width * tp_count) + norm_eps)
    channels = mixed[:, :local_width].reshape(local_width * tp_count, tok_rows)
    mixed_rows = (
        lax.dot_general(channels, out_weight, (((0,), (0,)), ((), ())), preferred_element_type=f32)
        * inverse[:, None]
    )
    hidden_state = (residual_rows.astype(f32) + mixed_rows).astype(bf16)
    state_wide = hidden_state.astype(f32)
    scale_rows = lax.rsqrt(jnp.mean(state_wide * state_wide, axis=1, keepdims=True) + norm_eps)
    block_rows = (state_wide * scale_rows * channel_gain[None, :]).astype(bf16)
    hidden_width = value_weight.shape[1]
    value_up = jnp.dot(
        block_rows,
        lax.all_gather(value_weight, "sp", axis=0, tiled=True),
        preferred_element_type=f32,
    )
    gate_up = jnp.dot(
        block_rows,
        lax.all_gather(gate_weight, "sp", axis=0, tiled=True),
        preferred_element_type=f32,
    )
    both_up = jnp.concatenate((value_up.astype(bf16), gate_up.astype(bf16)), axis=1)
    padded = with_halo(both_up, "sp")
    taps = jnp.concatenate((value_taps, gate_taps), axis=1)
    convolved = (
        taps[0] * padded[:-2].astype(f32)
        + taps[1] * padded[1:-1].astype(f32)
        + taps[2] * padded[2:].astype(f32)
    )
    hidden = (convolved[:, :hidden_width] * jax.nn.silu(convolved[:, hidden_width:])).astype(bf16)
    down_full = lax.all_gather(down_weight, "sp", axis=1, tiled=True)
    partial = jnp.dot(hidden, down_full, preferred_element_type=f32).astype(bf16)
    pieces = lax.all_to_all(
        partial.reshape(tp_count, tok_rows // tp_count, -1), "tp", 0, 0, tiled=True
    )
    mine = lax.axis_index("tp") * (tok_rows // tp_count)
    own = lax.dynamic_slice_in_dim(state_wide, mine, tok_rows // tp_count, axis=0)
    return (own + jnp.sum(pieces.astype(f32), axis=0)).astype(bf16)


def solution(mesh):
    in_specs = (
        P("sp", "tp"),
        P(None, "tp"),
        P(None, "sp", "tp"),
        P(None, None, "tp", None, None),
        P(None, None, "tp", None, None),
        P("tp"),
        P("tp"),
        P(),
        P(("sp", "tp"), None),
        P(),
        P("sp", "tp"),
        P("sp", "tp"),
        P(None, "tp"),
        P(None, "tp"),
        P("tp", "sp"),
    )
    out_specs = P(("sp", "tp"), None)
    return jax.shard_map(body, mesh=mesh, in_specs=in_specs, out_specs=out_specs, check_vma=False)
```

time: 442 us -> 339 us (0.77)
  blocking collectives: 271 us -> 13.2 us
  waiting for transfers between devices: 32.1 us -> 252 us
  local copies, waits for them, and re-layouts: 60 us -> 5.39 us
  other arithmetic: 33 us -> 3.99 us
  Pallas kernels: 0 us -> 20.2 us
  starting transfers between devices: 5.99 us -> 14.6 us
  matrix products: 21.7 us -> 15.3 us
    all_gather x9 -> x2, blocking collectives: 266 us -> 13.2 us  [the longest x1 7.15 us: body(): residual_rows = lax.all_gather(residual, 'tp', axis=0, tiled=True)]
    all_gather x1, waiting for transfers between devices: 0.01 us -> 95.3 us  [body(): lax.all_gather(gate_weight, 'sp', axis=0, tiled=True)]
    all_gather x1, waiting for transfers between devices: 0.02 us -> 87.6 us  [body(): down_full = lax.all_gather(down_weight, 'sp', axis=1, tiled=True)]
    all_gather x1, waiting for transfers between devices: 0.02 us -> 51.4 us  [body(): lax.all_gather(value_weight, 'sp', axis=0, tiled=True)]
    reduce_scatter x1 -> x0, waiting for transfers between devices: 21.7 us -> none  [body(): lax.psum_scatter(jnp.dot(hidden, down_full, preferred_element_type=jnp.fl...]
    pallas_call x0 -> x2, Pallas kernels: none -> 20.2 us  [the longest x1 15.6 us: mixer_local(): pl.pallas_call(local_kernel, out_shape=(jax.ShapeDtypeStruct((width, rows...]
    reshape x6 -> x0, local copies, waits for them, and re-layouts: 17 us -> none  [the longest x2 8.88 us: mixer_branch(): jnp.einsum('pghn,gk->pgnkh', signed, ones_wide, precision=highest)]
    add x27 -> x1, other arithmetic: 16.7 us -> 0.54 us  [body(): taps[0] * padded[:-2].astype(f32) + taps[1] * padded[1:-1].astype(f32)]
  transfers between devices with their start and end apart: 7 -> 7, of which waited for: 4 -> 7; matrix products, arithmetic and copies ran while one was open for 24% -> 5% of each run, Pallas kernels for 0% -> 6%
where the time goes in v1:
time: 339 us; the launch traced here: 338 us
  waiting for transfers between devices  252 us (74%)
  Pallas kernels  20.2 us (6%)
  matrix products  15.3 us (5%)
  starting transfers between devices  14.6 us (4%)
  blocking collectives  13.2 us (4%)
  between operations  13.2 us (4%)
  local copies, waits for them, and re-layouts  5.39 us (2%)
  other arithmetic  3.99 us (1%)
    all_gather x1, waiting for transfers between devices, body(): lax.all_gather(gate_weight, 'sp', axis=0, tiled=True)  95.3 us
    all_gather x1, waiting for transfers between devices, body(): down_full = lax.all_gather(down_weight, 'sp', axis=1, tiled=True)  87.6 us
    all_gather x1, waiting for transfers between devices, body(): lax.all_gather(value_weight, 'sp', axis=0, tiled=True)  51.4 us
    pallas_call x1, Pallas kernels, mixer_local(): pl.pallas_call(local_kernel, out_shape=(jax.ShapeDtypeStruct((width, rows...  15.6 us
    all_to_all x1, waiting for transfers between devices, body(): lax.all_to_all(partial.reshape(tp_count, tok_rows // tp_count, -1), 'tp',...  8.78 us
    all_to_all x1, starting transfers between devices, body(): lax.all_to_all(jnp.broadcast_to(ends[None], (sp_count,) + ends.shape), 's...  7.31 us
    all_gather x1, blocking collectives, body(): residual_rows = lax.all_gather(residual, 'tp', axis=0, tiled=True)  7.15 us
  transfers between devices with their start and end apart: 7, of which 7 were waited for; matrix products, arithmetic and copies ran while one was open for 5% of the time, Pallas kernels for 6%

profile of v1, /device:TPU:0, one launch (start us, length us, event | category | flops | bytes accessed | tf_op | source)
XLA Modules:
  0.0 338.0 jit_solution(16176832802932094641)
XLA Ops:
  6.5 0.7 all-gather.5.cloned.1.call-update
  8.8 0.7 copy.18
  9.5 1.3 copy.19.in_map
  12.3 15.6 %mixer_local.1 = (f32[256,128]{1,0:T(8,128)}, f32[32,128]{1,0:T(8,128)}, f32[2,16,128]{2,1,0:T(8,128)}) custom-call(f32[3,2,16]{2,1,0:T(2,128)} %pad_maximum_fusion.5.scal, bf16[256,128]{1,0:T(8,128)(2,1)} %bitcast.27, f32[2,16,128]{2,1,0:T(8,128)} %get-tuple-element.24.damp, bf16[2,2,16,64,16]{4,3,2,1,0:T(8,128)(2,1)} %copy.19.in_map, ...), custom_call_target="tpu_custom_call" | custom-call | tf_op jit(solution)/shard_map/mixer_local/pallas_call | solution.py:180
  27.8 0.7 select_maximum_fusion
  29.2 7.3 %all-to-all-start = ((f32[8,40,128]{2,1,0:T(8,128)}), f32[8,40,128]{2,1,0:T(8,128)S(1)}, u32[]{:S(2)}, u32[]{:S(2)}) async-start(f32[8,40,128]{2,1,0:T(8,128)} %broadcast_in_dim.6), calls=%async_computation | async-start | bytes 327680 | tf_op jit(solution)/shard_map/all_to_all | solution.py:243
  36.7 0.8 copy.20.skip
  37.5 0.8 copy.21.gain
  38.3 7.2 %all_gather.18 = bf16[128,2048]{1,0:T(8,128)(2,1)S(1)} all-gather(bf16[32,2048]{1,0:T(8,128)(2,1)S(1)} %copy-done.2), channel_id=1, replica_groups=mesh['sp'=8,'tp'=4] {'tp'}, dimensions={0}, use_global_device_ids=true | all-gather | bytes 655360 | tf_op jit(solution)/shard_map/all_gather | solution.py:241
  46.1 2.6 all-to-all-done.every
  49.4 4.6 %mixer_carried.1 = bf16[272,128]{1,0:T(8,128)(2,1)} custom-call(f32[3,2,16]{2,1,0:T(2,128)} %pad_maximum_fusion.5.scal, s32[1]{0:T(128)} %bitcast.3.place, bf16[256,128]{1,0:T(8,128)(2,1)} %bitcast.28, f32[2,16,128]{2,1,0:T(8,128)} %get-tuple-element.20.rows_a, f32[2,32]{1,0:T(2,128)} %pad_maximum_fusion.6.lanes, f32[8,40,128]{2,1,0:T(8,128)} %copy-done, ...), custom_call_target="tpu_custom_call" | custom-call | tf_op jit(solution)/shard_map/mixer_carried/pallas_call | solution.py:201
  54.0 6.0 %all-gather = bf16[1088,128]{1,0:T(8,128)(2,1)S(1)} all-gather(bf16[272,128]{1,0:T(8,128)(2,1)} %mixer_carried.1), channel_id=2, replica_groups=mesh['sp'=8,'tp'=4] {'tp'}, dimensions={0}, use_global_device_ids=true | all-gather | bytes 348160 | tf_op jit(solution)/shard_map/all_gather | solution.py:247
  60.1 3.0 multiply_reduce_fusion
  63.2 51.4 %all-gather.5.cloned.1.call-done = bf16[2048,1536]{1,0:T(8,128)(2,1)} async-done(((bf16[256,1536]{1,0:T(8,128)(2,1)}), bf16[2048,1536]{1,0:T(8,128)(2,1)}) %all-gather.5.cloned.1.call-update) | async-done | bytes 6291472 | tf_op jit(solution)/shard_map/all_gather | solution.py:262
  114.6 3.8 %convolution_convert_fusion.2 = bf16[128,1536]{1,0:T(8,128)(2,1)S(1)} fusion(bf16[2048,1536]{1,0:T(8,128)(2,1)} %all-gather.5.cloned.1.call-done, f32[128,2048]{1,0:T(8,128)S(1)} %get-tuple-element.37, f32[2048]{0:T(1024)S(1)} %copy-done.4, f32[128]{0:T(128)S(1)} %add_rsqrt_fusion), kind=kOutput, calls=%fused_computation.6 | convolution fusion | flops 806289408 | bytes 7741952 | tf_op jit(solution)/shard_map/dot_general | solution.py:260
  118.4 95.3 %all-gather.7.cloned.1.call-done = bf16[2048,1536]{1,0:T(8,128)(2,1)} async-done(((bf16[256,1536]{1,0:T(8,128)(2,1)}), bf16[2048,1536]{1,0:T(8,128)(2,1)}) %all-gather.7.cloned.1.call-update) | async-done | bytes 6291472 | tf_op jit(solution)/shard_map/all_gather | solution.py:267
  213.6 3.8 %convolution_convert_fusion.1 = bf16[128,1536]{1,0:T(8,128)(2,1)S(1)} fusion(bf16[2048,1536]{1,0:T(8,128)(2,1)} %all-gather.7.cloned.1.call-done, f32[128,2048]{1,0:T(8,128)S(1)} %get-tuple-element.37, f32[2048]{0:T(1024)S(1)} %copy-done.4, f32[128]{0:T(128)S(1)} %add_rsqrt_fusion), kind=kOutput, calls=%fused_computation.5 | convolution fusion | flops 806289408 | bytes 7741952 | tf_op jit(solution)/shard_map/dot_general | solution.py:265
  217.5 2.5 collective-permute-start
  220.0 1.3 collective-permute-start.1
  221.4 4.2 %collective-permute-done.1 = bf16[1,3072]{1,0:T(2,128)(2,1)S(1)} collective-permute-done((bf16[1,3072]{1,0:T(2,128)(2,1)S(1)}, bf16[1,3072]{1,0:T(2,128)(2,1)S(1)}, u32[]{:S(2)}, u32[]{:S(2)}) %collective-permute-start.1) | collective-permute-done | bytes 6176 | tf_op jit(solution)/shard_map/ppermute | solution.py:216
  226.1 87.6 %all-gather.9.cloned.1.call-done = bf16[1536,2048]{1,0:T(8,128)(2,1)} async-done(((bf16[1536,256]{1,0:T(8,128)(2,1)}), bf16[1536,2048]{1,0:T(8,128)(2,1)}) %all-gather.9.cloned.1.call-update) | async-done | bytes 6291472 | tf_op jit(solution)/shard_map/all_gather | solution.py:279
  313.8 4.6 %convolution_convert_fusion = bf16[128,2048]{1,0:T(8,128)(2,1)} fusion(bf16[1536,2048]{1,0:T(8,128)(2,1)} %all-gather.9.cloned.1.call-done, f32[128,3072]{1,0:T(8,128)S(1)} %multiply_add_fusion), kind=kOutput, calls=%fused_computation.3 | convolution fusion | flops 806748160 | bytes 8388608 | tf_op jit(solution)/shard_map/dot_general | solution.py:280
  318.4 3.5 %all-to-all-start.1 = ((bf16[4,32,2048]{2,1,0:T(8,128)(2,1)}), bf16[4,32,2048]{2,1,0:T(8,128)(2,1)S(1)}, u32[]{:S(2)}, u32[]{:S(2)}) async-start(bf16[4,32,2048]{2,1,0:T(8,128)(2,1)} %bitcast.13), calls=%async_computation.1 | async-start | bytes 1048576 | tf_op jit(solution)/shard_map/all_to_all | solution.py:281
  321.9 8.8 %all-to-all-done.1 = bf16[4,32,2048]{2,1,0:T(8,128)(2,1)S(1)} async-done(((bf16[4,32,2048]{2,1,0:T(8,128)(2,1)}), bf16[4,32,2048]{2,1,0:T(8,128)(2,1)S(1)}, u32[]{:S(2)}, u32[]{:S(2)}) %all-to-all-start.1) | async-done | bytes 524320 | tf_op jit(solution)/shard_map/all_to_all | solution.py:281
  (47 shorter events, 6.5 us)
Async XLA Ops:
  6.5 2.2 copy-start.3
  6.5 3.0 copy-start.1
  6.5 108.0 %all-gather.5.cloned.1.call-start = ((), (), s32[]{:S(2)}) async-start(), calls=%async_computation.2 | async-start | bytes 7077888 | tf_op jit(solution)/shard_map/all_gather | solution.py:262
  7.3 3.6 %copy-start.10 = (f32[2,16]{1,0:T(2,128)S(1)}, f32[2,16]{1,0:T(2,128)}, u32[]{:S(2)}) copy-start(f32[2,16]{1,0:T(2,128)} %param.18) | copy-start | bytes 388
  7.3 3.6 %copy-start.7 = (f32[2,128,16]{1,2,0:T(8,128)S(1)}, f32[2,128,16]{1,2,0:T(8,128)}, u32[]{:S(2)}) copy-start(f32[2,128,16]{1,2,0:T(8,128)} %param.19) | copy-start | bytes 49156
  7.3 206.4 %all-gather.7.cloned.1.call-start = ((), (), s32[]{:S(2)}) async-start(), calls=%async_computation.3 | async-start | bytes 7077888 | tf_op jit(solution)/shard_map/all_gather | solution.py:267
  8.0 305.7 %all-gather.9.cloned.1.call-start = ((), (), s32[]{:S(2)}) async-start(), calls=%async_computation.4 | async-start | bytes 7077888 | tf_op jit(solution)/shard_map/all_gather | solution.py:279
  9.5 27.2 %copy-start.8 = (f32[256]{0:T(256)S(1)}, f32[256]{0:T(256)}, u32[]{:S(2)}) copy-start(f32[256]{0:T(256)} %param.22) | copy-start | bytes 3076
  9.5 28.0 %copy-start.9 = (f32[256]{0:T(256)S(1)}, f32[256]{0:T(256)}, u32[]{:S(2)}) copy-start(f32[256]{0:T(256)} %param.23) | copy-start | bytes 3076
  10.9 27.4 %copy-start.2 = (bf16[32,2048]{1,0:T(8,128)(2,1)S(1)}, bf16[32,2048]{1,0:T(8,128)(2,1)}, u32[]{:S(2)}) copy-start(bf16[32,2048]{1,0:T(8,128)(2,1)} %param.25) | copy-start | bytes 393220
  12.3 33.2 %copy-start.5 = (f32[3,1536]{1,0:T(4,128)S(1)}, f32[3,1536]{1,0:T(4,128)}, u32[]{:S(2)}) copy-start(f32[3,1536]{1,0:T(4,128)} %param.29) | copy-start | bytes 55300
  12.3 33.8 %copy-start.6 = (f32[3,1536]{1,0:T(4,128)S(1)}, f32[3,1536]{1,0:T(4,128)}, u32[]{:S(2)}) copy-start(f32[3,1536]{1,0:T(4,128)} %param.30) | copy-start | bytes 55300
  29.2 19.5 %all-to-all-start = ((f32[8,40,128]{2,1,0:T(8,128)}), f32[8,40,128]{2,1,0:T(8,128)S(1)}, u32[]{:S(2)}, u32[]{:S(2)}) async-start(f32[8,40,128]{2,1,0:T(8,128)} %broadcast_in_dim.6), calls=%async_computation | async-start | bytes 327680 | tf_op jit(solution)/shard_map/all_to_all | solution.py:243
  48.7 0.7 copy-start
  60.1 54.5 %copy-start.4 = (f32[2048]{0:T(1024)S(1)}, f32[2048]{0:T(1024)}, u32[]{:S(2)}) copy-start(f32[2048]{0:T(1024)} %param.26) | copy-start | bytes 24580
  217.5 3.9 %collective-permute-start = (bf16[1,3072]{1,0:T(2,128)(2,1)S(1)}, bf16[1,3072]{1,0:T(2,128)(2,1)S(1)}, u32[]{:S(2)}, u32[]{:S(2)}) collective-permute-start(bf16[1,3072]{1,0:T(2,128)(2,1)S(1)} %get-tuple-element.25), channel_id=1, source_target_pairs={{0,4},{4,8},{8,12},{12,16},{16,20},{20,24},{24,28},{1,5},{5,9},{9,... | collective-permute-start | bytes 18440 | tf_op jit(solution)/shard_map/ppermute | solution.py:214
  220.0 5.6 %collective-permute-start.1 = (bf16[1,3072]{1,0:T(2,128)(2,1)S(1)}, bf16[1,3072]{1,0:T(2,128)(2,1)S(1)}, u32[]{:S(2)}, u32[]{:S(2)}) collective-permute-start(bf16[1,3072]{1,0:T(2,128)(2,1)S(1)} %get-tuple-element.26), channel_id=1, source_target_pairs={{4,0},{8,4},{12,8},{16,12},{20,16},{24,20},{28,24},{5,1},{9,5},{13... | collective-permute-start | bytes 18440 | tf_op jit(solution)/shard_map/ppermute | solution.py:216
  318.4 12.3 %all-to-all-start.1 = ((bf16[4,32,2048]{2,1,0:T(8,128)(2,1)}), bf16[4,32,2048]{2,1,0:T(8,128)(2,1)S(1)}, u32[]{:S(2)}, u32[]{:S(2)}) async-start(bf16[4,32,2048]{2,1,0:T(8,128)(2,1)} %bitcast.13), calls=%async_computation.1 | async-start | bytes 1048576 | tf_op jit(solution)/shard_map/all_to_all | solution.py:281
Sparse Core Ops, SparseCore 0:
  9.5 104.9 all-gather.4
  116.7 96.8 all-gather.6
  215.7 98.0 all-gather.8

commit v2 on v1

--- a/solution.py
+++ b/solution.py
@@ -219,7 +219,7 @@
     )
 
 
-def body(
+def gathered_body(
     mixer_input,
     time_step,
     damping,
@@ -286,6 +286,248 @@
     return (own + jnp.sum(pieces.astype(f32), axis=0)).astype(bf16)
 
 
+def ring(axis, inner, step, low=0):
+    size = lax.axis_size(axis)
+    outer = size // inner
+    return [
+        (i, ((i // inner + step) % outer) * inner + (i + low) % inner) for i in range(size)
+    ]
+
+
+def outer_send(pick, axis, inner):
+    outer = lax.axis_size(axis) // inner
+    return [lax.ppermute(pick(s), axis, ring(axis, inner, s)) for s in range(1, outer)]
+
+
+def spread(slices):
+    outer = slices.shape[0]
+    mine = lax.axis_index("sp") // pair
+
+    def pick(step):
+        return lax.dynamic_index_in_dim(slices, lax.rem(mine + step, outer), 0, False)
+
+    own = jnp.stack([pick(0)] + outer_send(pick, "sp", pair))
+    beside = lax.ppermute(own, "sp", ring("sp", pair, 0, 1))
+    over = ring("tp", pair, 0, 1)
+    return own, beside, lax.ppermute(own, "tp", over), lax.ppermute(beside, "tp", over)
+
+
+pair = 2
+
+
+def row_block(outer, which, step):
+    sp = lax.axis_index("sp")
+    far = lax.rem(sp // pair + outer - step, outer)
+    return far * pair + lax.rem(sp + which, pair)
+
+
+def up_kernel(x, *refs):
+    stacks, (out, full, sems) = refs[:8], refs[8:]
+    outer, rows, cols = stacks[0].shape
+    groups = []
+    for kind in range(2):
+        for core in range(2):
+            copies = []
+            for which in range(2):
+                ref = stacks[kind * 4 + core * 2 + which]
+                for s in range(outer):
+                    first = pl.multiple_of(row_block(outer, which, s) * rows, rows)
+                    slot = kind * 2 + core
+                    copy = pltpu.make_async_copy(
+                        ref.at[s],
+                        full.at[slot, pl.ds(first, rows), :],
+                        sems.at[slot, which * outer + s],
+                    )
+                    copy.start()
+                    copies.append(copy)
+            groups.append(copies)
+    for slot, copies in enumerate(groups):
+        for copy in copies:
+            copy.wait()
+        out[:, slot * cols : (slot + 1) * cols] = jnp.dot(
+            x[...], full[slot], preferred_element_type=f32
+        ).astype(bf16)
+
+
+def down_kernel(up, before, after, taps, *refs):
+    stacks, (out, full, sems) = refs[:4], refs[4:]
+    outer, rows, cols = stacks[0].shape
+    copies = []
+    for core in range(2):
+        for which in range(2):
+            ref = stacks[core * 2 + which]
+            for s in range(outer):
+                first = pl.multiple_of(row_block(outer, which, s) * cols, cols)
+                copy = pltpu.make_async_copy(
+                    ref.at[s],
+                    full.at[pl.ds(core * rows, rows), pl.ds(first, cols)],
+                    sems.at[core * 2 + which, s],
+                )
+                copy.start()
+                copies.append(copy)
+    width = 2 * rows
+    count, pieces = up.shape[0], before.shape[0]
+    length = count // pieces
+
+    def convolved(start):
+        at = slice(start, start + width)
+        rows_id = iota((length, width), 0)
+        done = []
+        for p in range(pieces):
+            cells = up[p * length : (p + 1) * length, at].astype(f32)
+            left = pltpu.roll(cells, 1, 0)
+            left = jnp.where(rows_id == 0, before[p : p + 1, at].astype(f32), left)
+            right = pltpu.roll(cells, length - 1, 0)
+            right = jnp.where(rows_id == length - 1, after[p : p + 1, at].astype(f32), right)
+            done.append(taps[0:1, at] * left + taps[1:2, at] * cells + taps[2:3, at] * right)
+        return jnp.concatenate(done, axis=0)
+
+    gate = convolved(width)
+    hidden = (convolved(0) * (gate / (1.0 + jnp.exp(-gate)))).astype(bf16)
+    for copy in copies:
+        copy.wait()
+    out[...] = jnp.dot(hidden, full[...], preferred_element_type=f32).astype(bf16)
+
+
+def up_projection(x, stacks):
+    outer, rows, cols = stacks[0].shape
+    return pl.pallas_call(
+        up_kernel,
+        out_shape=jax.ShapeDtypeStruct((x.shape[0], 4 * cols), bf16),
+        in_specs=vmem(1) + [pl.BlockSpec(memory_space=pltpu.HBM)] * 8,
+        out_specs=pl.BlockSpec(memory_space=pltpu.VMEM),
+        scratch_shapes=[
+            pltpu.VMEM((4, 2 * outer * rows, cols), bf16),
+            pltpu.SemaphoreType.DMA((4, 2 * outer)),
+        ],
+        name="up_projection",
+    )(x, *stacks)
+
+
+def down_projection(up, before, after, taps, stacks):
+    outer, rows, cols = stacks[0].shape
+    return pl.pallas_call(
+        down_kernel,
+        out_shape=jax.ShapeDtypeStruct((up.shape[0], 2 * outer * cols), bf16),
+        in_specs=vmem(4) + [pl.BlockSpec(memory_space=pltpu.HBM)] * 4,
+        out_specs=pl.BlockSpec(memory_space=pltpu.VMEM),
+        scratch_shapes=[
+            pltpu.VMEM((2 * rows, 2 * outer * cols), bf16),
+            pltpu.SemaphoreType.DMA((4, outer)),
+        ],
+        name="down_projection",
+    )(up, before, after, taps, *stacks)
+
+
+def edges_of(up, outer, inner):
+    sp, tp = lax.axis_index("sp"), lax.axis_index("tp")
+    z, y, x, c = sp // pair, lax.rem(sp, pair), tp // pair, lax.rem(tp, pair)
+    cells = up.reshape(outer, inner, -1, 2, 2, up.shape[1] // 4)[:, :, :, :, ::-1]
+    cells = cells.reshape(outer, inner, -1, up.shape[1])
+    ends = jnp.stack((cells[:, :, 0], cells[:, :, -1]))
+    across = lax.ppermute(ends, "tp", ring("tp", pair, 0, 1))
+    rim = jnp.where(c == 0, lax.rem(inner - x, inner), inner - 1 - x)
+    out_edge = lax.dynamic_index_in_dim(
+        lax.dynamic_index_in_dim(ends, c, 0, False), rim, 1, False
+    )
+    sizes = (lax.axis_size("sp"), lax.axis_size("tp"))
+    hops = [
+        (i * sizes[1] + j, (i ^ 1) * sizes[1] + (j ^ 1))
+        for i in range(sizes[0])
+        for j in range(sizes[1])
+    ]
+    rim_rows = lax.ppermute(out_edge, ("sp", "tp"), hops)
+    block = lax.rem(z + outer - jnp.arange(outer), outer)
+    before_rim = jnp.where(y == 0, jnp.roll(rim_rows, -1, axis=0), rim_rows)
+    before_rim = jnp.where(((block == 0) & (y == 0))[:, None], 0, before_rim)
+    after_rim = jnp.where(y == pair - 1, jnp.roll(rim_rows, 1, axis=0), rim_rows)
+    after_rim = jnp.where(((block == outer - 1) & (y == pair - 1))[:, None], 0, after_rim)
+    sub = lax.rem(x + jnp.arange(inner), inner)[None, :, None]
+    before_low = jnp.where(sub == 0, before_rim[:, None], jnp.roll(across[1], 1, axis=1))
+    after_high = jnp.where(sub == inner - 1, after_rim[:, None], jnp.roll(across[0], -1, axis=1))
+    before = jnp.where(c == 0, before_low, across[1])
+    after = jnp.where(c == 0, across[0], after_high)
+    return before.reshape(outer * inner, -1), after.reshape(outer * inner, -1)
+
+
+def spread_body(
+    mixer_input,
+    time_step,
+    damping,
+    input_map,
+    readout,
+    skip_gain,
+    out_gain,
+    out_weight,
+    residual,
+    channel_gain,
+    value_weight,
+    gate_weight,
+    value_taps,
+    gate_taps,
+    down_weight,
+):
+    tp_count, sp_count = lax.axis_size("tp"), lax.axis_size("sp")
+    outer, inner = sp_count // pair, tp_count // pair
+    tok_rows, local_width = mixer_input.shape
+    own_rows = tok_rows // tp_count
+    model = residual.shape[1]
+    z, tp = lax.axis_index("sp") // pair, lax.axis_index("tp")
+
+    def columns(weight):
+        return jnp.swapaxes(weight.reshape(weight.shape[0], outer, -1), 0, 1)
+
+    value_stacks = spread(columns(value_weight))
+    scal, xt, yt, rows_a, ends = mixer_local(mixer_input, time_step, damping, input_map, readout)
+    every = lax.all_to_all(
+        jnp.broadcast_to(ends[None], (sp_count,) + ends.shape), "sp", 0, 0, tiled=True
+    )
+    gate_stacks = spread(columns(gate_weight))
+    others = outer_send(lambda s: residual, "tp", pair)
+    taps = jnp.stack((value_taps, gate_taps), axis=1).reshape(-1, value_taps.shape[1])
+    taps = lax.dynamic_index_in_dim(taps.reshape(taps.shape[0], outer, -1), z, 1, False)
+    taps_over = lax.ppermute(taps, "tp", ring("tp", pair, 0, 1))
+    taps = jnp.stack((taps, taps_over), axis=1).reshape(value_taps.shape[0], -1)
+
+    mixed = mixer_carried(scal, xt, yt, rows_a, every, readout, skip_gain, out_gain)
+    mixed = lax.all_gather(mixed, "tp", axis=0)
+    squares = jnp.sum(mixed[:, local_width:].astype(f32), axis=(0, 1))
+    inverse = lax.rsqrt(squares / (local_width * tp_count) + norm_eps)
+    channels = mixed[:, :local_width].reshape(local_width * tp_count, tok_rows)
+    mixed_rows = (
+        lax.dot_general(channels, out_weight, (((0,), (0,)), ((), ())), preferred_element_type=f32)
+        * inverse[:, None]
+    )
+    picked = [
+        lax.dynamic_slice_in_dim(
+            mixed_rows, lax.rem(tp + tp_count - pair * r, tp_count) * own_rows, own_rows, axis=0
+        )
+        for r in range(inner)
+    ]
+    order = [0] + list(range(inner - 1, 0, -1))
+    picked = jnp.concatenate([picked[r] for r in order], axis=0)
+    mine = [residual] + others
+    rows = jnp.concatenate([mine[r] for r in order], axis=0)
+    hidden_state = (rows.astype(f32) + picked).astype(bf16)
+    state_wide = hidden_state.astype(f32)
+    scale_rows = lax.rsqrt(jnp.mean(state_wide * state_wide, axis=1, keepdims=True) + norm_eps)
+    normed = (state_wide * scale_rows * channel_gain[None, :]).astype(bf16)
+    x_rows = jnp.concatenate([normed] + outer_send(lambda s: normed, "sp", pair), axis=0)
+    up = up_projection(x_rows, value_stacks + gate_stacks)
+    down_stacks = spread(down_weight.reshape(outer, -1, down_weight.shape[1]))
+    before, after = edges_of(up, outer, inner)
+    partial = down_projection(up, before, after, taps, down_stacks)
+    parts = partial.reshape(outer, inner, own_rows, model)
+    total = parts[:, 0].astype(f32)
+    for got in outer_send(lambda s: parts[:, s], "tp", pair):
+        total = total + got.astype(f32)
+    total = total.astype(bf16)
+    summed = total[0].astype(f32)
+    for got in outer_send(lambda s: total[outer - s], "sp", pair):
+        summed = summed + got.astype(f32)
+    return (state_wide[:own_rows] + summed).astype(bf16)
+
+
 def solution(mesh):
     in_specs = (
         P("sp", "tp"),
@@ -305,4 +547,12 @@
         P("tp", "sp"),
     )
     out_specs = P(("sp", "tp"), None)
+
+    def body(*args):
+        value_weight = args[10]
+        sp, tp = mesh.shape["sp"], mesh.shape["tp"]
+        even = sp % pair == 0 and tp % pair == 0
+        whole_lanes = even and (value_weight.shape[1] // (sp // pair)) % 128 == 0
+        return (spread_body if whole_lanes else gathered_body)(*args)
+
     return jax.shard_map(body, mesh=mesh, in_specs=in_specs, out_specs=out_specs, check_vma=False)

time: 339 us -> 206 us (0.61)
  waiting for transfers between devices: 252 us -> 62.5 us
  starting transfers between devices: 14.6 us -> 61.8 us
  local copies, waits for them, and re-layouts: 5.39 us -> 24.6 us
  between operations: 13.2 us -> 0.67 us
  matrix products: 15.3 us -> 2.96 us
  Pallas kernels: 20.2 us -> 32.2 us
  other arithmetic: 3.99 us -> 14.5 us
  blocking collectives: 13.2 us -> 6.03 us
    all_gather x3 -> x0, waiting for transfers between devices: 234 us -> none  [the longest x1 95.3 us: body(): lax.all_gather(gate_weight, 'sp', axis=0, tiled=True)]
    ppermute x2 -> x29, waiting for transfers between devices: 4.29 us -> 62.5 us  [the longest x17 45.7 us: outer_send(): lax.ppermute(pick(s), axis, ring(axis, inner, s))]
    ppermute x2 -> x29, starting transfers between devices: 3.75 us -> 54.5 us  [the longest x17 49 us: outer_send(): lax.ppermute(pick(s), axis, ring(axis, inner, s))]
    dot_general x4 -> x1, matrix products: 15.3 us -> 2.96 us  [spread_body(): lax.dot_general(channels, out_weight, (((0,), (0,)), ((), ())), preferred...]
    pallas_call x0 -> x2, Pallas kernels: none -> 12.1 us  [the longest x1 6.81 us: up_projection(): pl.pallas_call(up_kernel, out_shape=jax.ShapeDtypeStruct((x.shape[0], 4 *...]
    all_to_all x2 -> x1, waiting for transfers between devices: 11.4 us -> 0.01 us  [spread_body(): lax.all_to_all(jnp.broadcast_to(ends[None], (sp_count,) + ends.shape), 's...]
    all_gather x2 -> x1, blocking collectives: 13.2 us -> 6.03 us  [spread_body(): mixed = lax.all_gather(mixed, 'tp', axis=0)]
    unnamed x25 -> x45, local copies, waits for them, and re-layouts: 2.8 us -> 8.29 us
  transfers between devices with their start and end apart: 7 -> 30, of which waited for: 7 -> 9; matrix products, arithmetic and copies ran while one was open for 5% -> 15% of each run, Pallas kernels for 6% -> 6%
where the time goes in v2:
time: 206 us; the launch traced here: 205 us
  waiting for transfers between devices  62.5 us (30%)
  starting transfers between devices  61.8 us (30%)
  Pallas kernels  32.2 us (16%)
  local copies, waits for them, and re-layouts  24.6 us (12%)
  other arithmetic  14.5 us (7%)
  blocking collectives  6.03 us (3%)
  matrix products  2.96 us (1%)
    ppermute x17, starting transfers between devices, outer_send(): lax.ppermute(pick(s), axis, ring(axis, inner, s))  49 us
    ppermute x17, waiting for transfers between devices, outer_send(): lax.ppermute(pick(s), axis, ring(axis, inner, s))  45.7 us
    pallas_call x1, Pallas kernels, mixer_local(): pl.pallas_call(local_kernel, out_shape=(jax.ShapeDtypeStruct((width, rows...  15.5 us
    ppermute x3, waiting for transfers between devices, spread(): beside = lax.ppermute(own, 'sp', ring('sp', pair, 0, 1))  15 us
    unnamed x45, local copies, waits for them, and re-layouts  8.29 us
    all_to_all x1, starting transfers between devices, spread_body(): lax.all_to_all(jnp.broadcast_to(ends[None], (sp_count,) + ends.shape), 's...  7.31 us
    pallas_call x1, Pallas kernels, up_projection(): pl.pallas_call(up_kernel, out_shape=jax.ShapeDtypeStruct((x.shape[0], 4 *...  6.81 us
    all_gather x1, blocking collectives, spread_body(): mixed = lax.all_gather(mixed, 'tp', axis=0)  6.03 us
  transfers between devices with their start and end apart: 30, of which 9 were waited for; matrix products, arithmetic and copies ran while one was open for 15% of the time, Pallas kernels for 6%

profile of v2, /device:TPU:0, one launch (start us, length us, event | category | flops | bytes accessed | tf_op | source)
XLA Modules:
  0.0 205.4 jit_solution(10985965344452210933)
XLA Ops:
  2.4 2.3 %copy.30.in_map = bf16[2,2,16,64,16]{4,3,2,1,0:T(8,128)(2,1)} copy(bf16[2,2,16,64,16]{3,4,2,1,0:T(8,128)(2,1)} %param.20) | data formatting | bytes 262144 | tf_op args[3]
  6.8 15.5 %mixer_local.1 = (f32[256,128]{1,0:T(8,128)}, f32[32,128]{1,0:T(8,128)}, f32[2,16,128]{2,1,0:T(8,128)}) custom-call(f32[3,2,16]{2,1,0:T(2,128)} %pad_maximum_fusion.9.scal, bf16[256,128]{1,0:T(8,128)(2,1)} %bitcast.105, f32[2,16,128]{2,1,0:T(8,128)} %get-tuple-element.26.damp, bf16[2,2,16,64,16]{4,3,2,1,0:T(8,128)(2,1)} %copy.30.in_map, ...), custom_call_target="tpu_custom_call" | custom-call | tf_op jit(solution)/shard_map/mixer_local/pallas_call | solution.py:180
  23.7 7.3 %all-to-all-start = ((f32[8,40,128]{2,1,0:T(8,128)}), f32[8,40,128]{2,1,0:T(8,128)S(1)}, u32[]{:S(2)}, u32[]{:S(2)}) async-start(f32[8,40,128]{2,1,0:T(8,128)} %broadcast_in_dim.78), calls=%async_computation | async-start | bytes 327680 | tf_op jit(solution)/shard_map/all_to_all | solution.py:482
  31.4 3.3 %constant_dynamic-slice_fusion.5 = (bf16[256,1,384]{2,1,0:T(2,128)(2,1)S(1)}, bf16[256,1,384]{2,1,0:T(2,128)(2,1)S(1)}, bf16[256,1,384]{2,1,0:T(2,128)(2,1)S(1)}...) fusion(bf16[256,4,384]{2,1,0:T(4,128)(2,1)S(1)} %reshape.153, ...), kind=kLoop, calls=%fused_computation.61 | loop fusion | bytes 3145744 | tf_op jit(solution)/shard_map/dynamic-slice.10
  34.8 3.9 %collective-permute-start.6 = (bf16[256,384]{1,0:T(8,128)(2,1)S(1)}, bf16[256,384]{1,0:T(8,128)(2,1)S(1)}, u32[]{:S(2)}, u32[]{:S(2)}) collective-permute-start(bf16[256,384]{1,0:T(8,128)(2,1)S(1)} %bitcast.115), channel_id=1, source_target_pairs={{0,24},{4,28},{8,0},{12,4},{16,8},{20,12},{24,16},{28,20},{1,25},{... | collective-permute-start | bytes 589832 | tf_op jit(solution)/shard_map/ppermute | solution.py:299
  41.9 2.7 %collective-permute-start.12 = (bf16[256,384]{1,0:T(8,128)(2,1)}, bf16[256,384]{1,0:T(8,128)(2,1)S(1)}, u32[]{:S(2)}, u32[]{:S(2)}) collective-permute-start(bf16[256,384]{1,0:T(8,128)(2,1)} %bitcast.86), channel_id=1, source_target_pairs={{0,24},{4,28},{8,0},{12,4},{16,8},{20,12},{24,16},{28,20},{1,25},{... | collective-permute-start | bytes 589832 | tf_op jit(solution)/shard_map/ppermute | solution.py:299
  50.6 6.5 %collective-permute-done.5 = bf16[256,384]{1,0:T(8,128)(2,1)} collective-permute-done((bf16[256,384]{1,0:T(8,128)(2,1)}, bf16[256,384]{1,0:T(8,128)(2,1)}, u32[]{:S(2)}, u32[]{:S(2)}) %collective-permute-start.5) | collective-permute-done | bytes 196640 | tf_op jit(solution)/shard_map/ppermute | solution.py:299
  59.9 5.0 %collective-permute-start.21 = (bf16[384,256]{1,0:T(8,128)(2,1)}, bf16[384,256]{1,0:T(8,128)(2,1)}, u32[]{:S(2)}, u32[]{:S(2)}) collective-permute-start(bf16[384,256]{1,0:T(8,128)(2,1)} %get-tuple-element.30), channel_id=1, source_target_pairs={{0,24},{4,28},{8,0},{12,4},{16,8},{20,12},{24,16},{28,20},{1,25},{... | collective-permute-start | bytes 589832 | tf_op jit(solution)/shard_map/ppermute | solution.py:299
  64.9 7.8 %collective-permute-done.11 = bf16[256,384]{1,0:T(8,128)(2,1)} collective-permute-done((bf16[256,384]{1,0:T(8,128)(2,1)}, bf16[256,384]{1,0:T(8,128)(2,1)}, u32[]{:S(2)}, u32[]{:S(2)}) %collective-permute-start.11) | collective-permute-done | bytes 196640 | tf_op jit(solution)/shard_map/ppermute | solution.py:299
  75.9 4.6 %mixer_carried.1 = bf16[272,128]{1,0:T(8,128)(2,1)} custom-call(f32[3,2,16]{2,1,0:T(2,128)} %pad_maximum_fusion.9.scal, s32[1]{0:T(128)} %bitcast.3.place, bf16[256,128]{1,0:T(8,128)(2,1)} %bitcast.106, f32[2,16,128]{2,1,0:T(8,128)} %get-tuple-element.20.rows_a, f32[2,32]{1,0:T(2,128)} %pad_maximum_fusion.10.lanes, f32[8,40,128]{2,1,0:T(8,128)} %copy-done.6, ...), custom_call_target="tpu_custom_call" | custom-call | tf_op jit(solution)/shard_map/mixer_carried/pallas_call | solution.py:201
  80.5 6.0 %all-gather = bf16[1088,128]{1,0:T(8,128)(2,1)S(1)} all-gather(bf16[272,128]{1,0:T(8,128)(2,1)} %mixer_carried.1), channel_id=2, replica_groups=mesh['sp'=8,'tp'=4] {'tp'}, dimensions={0}, use_global_device_ids=true | all-gather | bytes 348160 | tf_op jit(solution)/shard_map/all_gather | solution.py:493
  86.6 3.0 %convolution_multiply_fusion = f32[128,2048]{1,0:T(8,128)S(1)} fusion(bf16[1024,128]{1,0:T(8,128)(2,1)S(1)} %bitcast.101, bf16[1024,2048]{1,0:T(8,128)(2,1)} %param.24, f32[128]{0:T(128)S(1)} %add_rsqrt_fusion.1), kind=kOutput, calls=%fused_computation | convolution fusion | flops 537133056 | bytes 5505536 | tf_op jit(solution)/shard_map/dot_general | solution.py:498
  91.4 9.3 %collective-permute-start.19 = (bf16[384,256]{1,0:T(8,128)(2,1)S(1)}, bf16[384,256]{1,0:T(8,128)(2,1)S(1)}, u32[]{:S(2)}, u32[]{:S(2)}) collective-permute-start(bf16[384,256]{1,0:T(8,128)(2,1)S(1)} %get-tuple-element.32), channel_id=1, source_target_pairs={{0,8},{4,12},{8,16},{12,20},{16,24},{20,28},{24,0},{28,4},{1,9},{5... | collective-permute-start | bytes 589832 | tf_op jit(solution)/shard_map/ppermute | solution.py:299
  101.0 3.8 %collective-permute-start.2 = (bf16[64,2048]{1,0:T(8,128)(2,1)S(1)}, bf16[64,2048]{1,0:T(8,128)(2,1)}, u32[]{:S(2)}, u32[]{:S(2)}) collective-permute-start(bf16[64,2048]{1,0:T(8,128)(2,1)S(1)} %multiply_convert_fusion), channel_id=1, source_target_pairs={{0,16},{4,20},{8,24},{12,28},{16,0},{20,4},{24,8},{28,12},{1,17},{... | collective-permute-start | bytes 786440 | tf_op jit(solution)/shard_map/ppermute | solution.py:299
  106.0 13.6 %collective-permute-start.1 = (bf16[64,2048]{1,0:T(8,128)(2,1)S(1)}, bf16[64,2048]{1,0:T(8,128)(2,1)S(1)}, u32[]{:S(2)}, u32[]{:S(2)}) collective-permute-start(bf16[64,2048]{1,0:T(8,128)(2,1)S(1)} %multiply_convert_fusion), channel_id=1, source_target_pairs={{0,8},{4,12},{8,16},{12,20},{16,24},{20,28},{24,0},{28,4},{1,9},{5... | collective-permute-start | bytes 786440 | tf_op jit(solution)/shard_map/ppermute | solution.py:299
  120.9 7.1 %collective-permute-done.2 = bf16[64,2048]{1,0:T(8,128)(2,1)} collective-permute-done((bf16[64,2048]{1,0:T(8,128)(2,1)S(1)}, bf16[64,2048]{1,0:T(8,128)(2,1)}, u32[]{:S(2)}, u32[]{:S(2)}) %collective-permute-start.2) | collective-permute-done | bytes 262176 | tf_op jit(solution)/shard_map/ppermute | solution.py:299
  133.0 15.0 %collective-permute-done.22.refs_1_ = bf16[4,384,256]{2,1,0:T(8,128)(2,1)} collective-permute-done((bf16[4,384,256]{2,1,0:T(8,128)(2,1)S(1)}, bf16[4,384,256]{2,1,0:T(8,128)(2,1)}, u32[]{:S(2)}, u32[]{:S(2)}) %collective-permute-start.22) | collective-permute-done | bytes 786464 | tf_op jit(solution)/shard_map/ppermute | solution.py:310
  148.1 6.8 %up_projection.1.up = bf16[256,1536]{1,0:T(8,128)(2,1)} custom-call(bf16[256,2048]{1,0:T(8,128)(2,1)} %pad_maximum_fusion.x, bf16[4,256,384]{2,1,0:T(8,128)(2,1)} %copy-done.1, bf16[4,256,384]{2,1,0:T(8,128)(2,1)} %collective-permute-done.7.refs_1_, bf16[4,256,384]{2,1,0:T(8,128)(2,1)} %collective-permute-done.8.refs_2_, ...), custom_call_target="tpu_custom_call" | custom-call | tf_op jit(solution)/shard_map/up_projection/pallas_call | solution.py:394
  157.1 4.2 %rev.3 = bf16[4,2,32,2,2,384]{5,4,3,2,1,0:T(2,128)(2,1)S(1)} reverse(bf16[4,2,32,2,2,384]{5,4,3,2,1,0:T(2,128)(2,1)S(1)} %reshape.154), dimensions={4} | reverse | bytes 1572864 | tf_op jit(solution)/shard_map/rev | solution.py:425
  167.1 5.2 %down_projection.1 = bf16[256,2048]{1,0:T(8,128)(2,1)} custom-call(bf16[256,1536]{1,0:T(8,128)(2,1)} %up_projection.1.up, bf16[8,1536]{1,0:T(8,128)(2,1)} %select_select_fusion.1.before, bf16[8,1536]{1,0:T(8,128)(2,1)} %select_select_fusion.after, f32[3,1536]{1,0:T(4,128)} %reshape.156.taps, bf16[4,384,256]{2,1,0:T(8,128)(2,1)} %copy-done, ...), custom_call_target="tpu_custom_call" | custom-call | tf_op jit(solution)/shard_map/down_projection/pallas_call | solution.py:409
  175.0 12.8 %collective-permute-done.25 = bf16[4,32,2048]{2,1,0:T(8,128)(2,1)S(1)} collective-permute-done((bf16[4,32,2048]{2,1,0:T(8,128)(2,1)S(1)}, bf16[4,32,2048]{2,1,0:T(8,128)(2,1)S(1)}, u32[]{:S(2)}, u32[]{:S(2)}) %collective-permute-start.25) | collective-permute-done | bytes 524320 | tf_op jit(solution)/shard_map/ppermute | solution.py:299
  189.1 4.6 %collective-permute-start.28 = (bf16[32,2048]{1,0:T(8,128)(2,1)S(1)}, bf16[32,2048]{1,0:T(8,128)(2,1)S(1)}, u32[]{:S(2)}, u32[]{:S(2)}) collective-permute-start(bf16[32,2048]{1,0:T(8,128)(2,1)S(1)} %get-tuple-element.44), channel_id=1, source_target_pairs={{0,24},{4,28},{8,0},{12,4},{16,8},{20,12},{24,16},{28,20},{1,25},{... | collective-permute-start | bytes 393224 | tf_op jit(solution)/shard_map/ppermute | solution.py:299
  194.3 3.2 %collective-permute-done.28 = bf16[32,2048]{1,0:T(8,128)(2,1)S(1)} collective-permute-done((bf16[32,2048]{1,0:T(8,128)(2,1)S(1)}, bf16[32,2048]{1,0:T(8,128)(2,1)S(1)}, u32[]{:S(2)}, u32[]{:S(2)}) %collective-permute-start.28) | collective-permute-done | bytes 131104 | tf_op jit(solution)/shard_map/ppermute | solution.py:299
  197.6 7.0 %collective-permute-done.27 = bf16[32,2048]{1,0:T(8,128)(2,1)S(1)} collective-permute-done((bf16[32,2048]{1,0:T(8,128)(2,1)S(1)}, bf16[32,2048]{1,0:T(8,128)(2,1)S(1)}, u32[]{:S(2)}, u32[]{:S(2)}) %collective-permute-start.27) | collective-permute-done | bytes 131104 | tf_op jit(solution)/shard_map/ppermute | solution.py:299
  (158 shorter events, 43.9 us)
Async XLA Ops:
  23.7 51.5 %all-to-all-start = ((f32[8,40,128]{2,1,0:T(8,128)}), f32[8,40,128]{2,1,0:T(8,128)S(1)}, u32[]{:S(2)}, u32[]{:S(2)}) async-start(f32[8,40,128]{2,1,0:T(8,128)} %broadcast_in_dim.78), calls=%async_computation | async-start | bytes 327680 | tf_op jit(solution)/shard_map/all_to_all | solution.py:482
  34.8 13.4 %collective-permute-start.6 = (bf16[256,384]{1,0:T(8,128)(2,1)S(1)}, bf16[256,384]{1,0:T(8,128)(2,1)S(1)}, u32[]{:S(2)}, u32[]{:S(2)}) collective-permute-start(bf16[256,384]{1,0:T(8,128)(2,1)S(1)} %bitcast.115), channel_id=1, source_target_pairs={{0,24},{4,28},{8,0},{12,4},{16,8},{20,12},{24,16},{28,20},{1,25},{... | collective-permute-start | bytes 589832 | tf_op jit(solution)/shard_map/ppermute | solution.py:299
  39.4 17.7 %collective-permute-start.5 = (bf16[256,384]{1,0:T(8,128)(2,1)}, bf16[256,384]{1,0:T(8,128)(2,1)}, u32[]{:S(2)}, u32[]{:S(2)}) collective-permute-start(bf16[256,384]{1,0:T(8,128)(2,1)} %bitcast.91), channel_id=1, source_target_pairs={{0,16},{4,20},{8,24},{12,28},{16,0},{20,4},{24,8},{28,12},{1,17},{... | collective-permute-start | bytes 589832 | tf_op jit(solution)/shard_map/ppermute | solution.py:299
  40.1 18.5 %collective-permute-start.4 = (bf16[256,384]{1,0:T(8,128)(2,1)}, bf16[256,384]{1,0:T(8,128)(2,1)}, u32[]{:S(2)}, u32[]{:S(2)}) collective-permute-start(bf16[256,384]{1,0:T(8,128)(2,1)} %bitcast.92), channel_id=1, source_target_pairs={{0,8},{4,12},{8,16},{12,20},{16,24},{20,28},{24,0},{28,4},{1,9},{5... | collective-permute-start | bytes 589832 | tf_op jit(solution)/shard_map/ppermute | solution.py:299
  41.9 17.9 %collective-permute-start.12 = (bf16[256,384]{1,0:T(8,128)(2,1)}, bf16[256,384]{1,0:T(8,128)(2,1)S(1)}, u32[]{:S(2)}, u32[]{:S(2)}) collective-permute-start(bf16[256,384]{1,0:T(8,128)(2,1)} %bitcast.86), channel_id=1, source_target_pairs={{0,24},{4,28},{8,0},{12,4},{16,8},{20,12},{24,16},{28,20},{1,25},{... | collective-permute-start | bytes 589832 | tf_op jit(solution)/shard_map/ppermute | solution.py:299
  45.3 27.3 %collective-permute-start.11 = (bf16[256,384]{1,0:T(8,128)(2,1)}, bf16[256,384]{1,0:T(8,128)(2,1)}, u32[]{:S(2)}, u32[]{:S(2)}) collective-permute-start(bf16[256,384]{1,0:T(8,128)(2,1)} %bitcast.87), channel_id=1, source_target_pairs={{0,16},{4,20},{8,24},{12,28},{16,0},{20,4},{24,8},{28,12},{1,17},{... | collective-permute-start | bytes 589832 | tf_op jit(solution)/shard_map/ppermute | solution.py:299
  48.3 24.4 %collective-permute-start.10 = (bf16[256,384]{1,0:T(8,128)(2,1)}, bf16[256,384]{1,0:T(8,128)(2,1)S(1)}, u32[]{:S(2)}, u32[]{:S(2)}) collective-permute-start(bf16[256,384]{1,0:T(8,128)(2,1)} %bitcast.88), channel_id=1, source_target_pairs={{0,8},{4,12},{8,16},{12,20},{16,24},{20,28},{24,0},{28,4},{1,9},{5... | collective-permute-start | bytes 589832 | tf_op jit(solution)/shard_map/ppermute | solution.py:299
  57.1 32.6 %collective-permute-start = (bf16[32,2048]{1,0:T(8,128)(2,1)}, bf16[32,2048]{1,0:T(8,128)(2,1)S(1)}, u32[]{:S(2)}, u32[]{:S(2)}) collective-permute-start(bf16[32,2048]{1,0:T(8,128)(2,1)} %param.25), channel_id=1, source_target_pairs={{0,2},{1,3},{2,0},{3,1},{4,6},{5,7},{6,4},{7,5},{8,10},{9,11},{10,... | collective-permute-start | bytes 393224 | tf_op jit(solution)/shard_map/ppermute | solution.py:299
  58.6 32.8 %collective-permute-start.18 = (f32[6,384]{1,0:T(8,128)S(1)}, f32[6,384]{1,0:T(8,128)S(1)}, u32[]{:S(2)}, u32[]{:S(2)}) collective-permute-start(f32[6,384]{1,0:T(8,128)S(1)} %bitcast.118), channel_id=1, source_target_pairs={{0,1},{1,0},{2,3},{3,2},{4,5},{5,4},{6,7},{7,6},{8,9},{9,8},{10,11... | collective-permute-start | bytes 27656 | tf_op jit(solution)/shard_map/ppermute | solution.py:489
  59.9 41.0 %collective-permute-start.21 = (bf16[384,256]{1,0:T(8,128)(2,1)}, bf16[384,256]{1,0:T(8,128)(2,1)}, u32[]{:S(2)}, u32[]{:S(2)}) collective-permute-start(bf16[384,256]{1,0:T(8,128)(2,1)} %get-tuple-element.30), channel_id=1, source_target_pairs={{0,24},{4,28},{8,0},{12,4},{16,8},{20,12},{24,16},{28,20},{1,25},{... | collective-permute-start | bytes 589832 | tf_op jit(solution)/shard_map/ppermute | solution.py:299
  72.7 28.3 %collective-permute-start.20 = (bf16[384,256]{1,0:T(8,128)(2,1)}, bf16[384,256]{1,0:T(8,128)(2,1)}, u32[]{:S(2)}, u32[]{:S(2)}) collective-permute-start(bf16[384,256]{1,0:T(8,128)(2,1)} %get-tuple-element.31), channel_id=1, source_target_pairs={{0,16},{4,20},{8,24},{12,28},{16,0},{20,4},{24,8},{28,12},{1,17},{... | collective-permute-start | bytes 589832 | tf_op jit(solution)/shard_map/ppermute | solution.py:299
  72.7 56.6 %collective-permute-start.7 = (bf16[4,256,384]{2,1,0:T(8,128)(2,1)S(1)}, bf16[4,256,384]{2,1,0:T(8,128)(2,1)}, u32[]{:S(2)}, u32[]{:S(2)}) collective-permute-start(bf16[4,256,384]{2,1,0:T(8,128)(2,1)S(1)} %pad_maximum_fusion.1.refs_0_), channel_id=1, source_target_pairs={{0,4},{4,0},{8,12},{12,8},{16,20},{20,16},{24,28},{28,24},{1,5},{5... | collective-permute-start | bytes 2359304 | tf_op jit(solution)/shard_map/ppermute | solution.py:310
  89.7 39.7 %collective-permute-start.13 = (bf16[4,256,384]{2,1,0:T(8,128)(2,1)S(1)}, bf16[4,256,384]{2,1,0:T(8,128)(2,1)}, u32[]{:S(2)}, u32[]{:S(2)}) collective-permute-start(bf16[4,256,384]{2,1,0:T(8,128)(2,1)S(1)} %pad_maximum_fusion.2.refs_4_), channel_id=1, source_target_pairs={{0,4},{4,0},{8,12},{12,8},{16,20},{20,16},{24,28},{28,24},{1,5},{5... | collective-permute-start | bytes 2359304 | tf_op jit(solution)/shard_map/ppermute | solution.py:310
  91.4 14.6 %collective-permute-start.19 = (bf16[384,256]{1,0:T(8,128)(2,1)S(1)}, bf16[384,256]{1,0:T(8,128)(2,1)S(1)}, u32[]{:S(2)}, u32[]{:S(2)}) collective-permute-start(bf16[384,256]{1,0:T(8,128)(2,1)S(1)} %get-tuple-element.32), channel_id=1, source_target_pairs={{0,8},{4,12},{8,16},{12,20},{16,24},{20,28},{24,0},{28,4},{1,9},{5... | collective-permute-start | bytes 589832 | tf_op jit(solution)/shard_map/ppermute | solution.py:299
  100.9 19.9 %collective-permute-start.3 = (bf16[64,2048]{1,0:T(8,128)(2,1)S(1)}, bf16[64,2048]{1,0:T(8,128)(2,1)}, u32[]{:S(2)}, u32[]{:S(2)}) collective-permute-start(bf16[64,2048]{1,0:T(8,128)(2,1)S(1)} %multiply_convert_fusion), channel_id=1, source_target_pairs={{0,24},{4,28},{8,0},{12,4},{16,8},{20,12},{24,16},{28,20},{1,25},{... | collective-permute-start | bytes 786440 | tf_op jit(solution)/shard_map/ppermute | solution.py:299
  101.0 27.0 %collective-permute-start.2 = (bf16[64,2048]{1,0:T(8,128)(2,1)S(1)}, bf16[64,2048]{1,0:T(8,128)(2,1)}, u32[]{:S(2)}, u32[]{:S(2)}) collective-permute-start(bf16[64,2048]{1,0:T(8,128)(2,1)S(1)} %multiply_convert_fusion), channel_id=1, source_target_pairs={{0,16},{4,20},{8,24},{12,28},{16,0},{20,4},{24,8},{28,12},{1,17},{... | collective-permute-start | bytes 786440 | tf_op jit(solution)/shard_map/ppermute | solution.py:299
  106.0 21.9 %collective-permute-start.1 = (bf16[64,2048]{1,0:T(8,128)(2,1)S(1)}, bf16[64,2048]{1,0:T(8,128)(2,1)S(1)}, u32[]{:S(2)}, u32[]{:S(2)}) collective-permute-start(bf16[64,2048]{1,0:T(8,128)(2,1)S(1)} %multiply_convert_fusion), channel_id=1, source_target_pairs={{0,8},{4,12},{8,16},{12,20},{16,24},{20,28},{24,0},{28,4},{1,9},{5... | collective-permute-start | bytes 786440 | tf_op jit(solution)/shard_map/ppermute | solution.py:299
  128.0 20.1 %collective-permute-start.14 = (bf16[4,256,384]{2,1,0:T(8,128)(2,1)S(1)}, bf16[4,256,384]{2,1,0:T(8,128)(2,1)}, u32[]{:S(2)}, u32[]{:S(2)}) collective-permute-start(bf16[4,256,384]{2,1,0:T(8,128)(2,1)S(1)} %pad_maximum_fusion.2.refs_4_), channel_id=1, source_target_pairs={{0,1},{1,0},{2,3},{3,2},{4,5},{5,4},{6,7},{7,6},{8,9},{9,8},{10,11... | collective-permute-start | bytes 2359304 | tf_op jit(solution)/shard_map/ppermute | solution.py:312
  128.0 20.0 %collective-permute-start.22 = (bf16[4,384,256]{2,1,0:T(8,128)(2,1)S(1)}, bf16[4,384,256]{2,1,0:T(8,128)(2,1)}, u32[]{:S(2)}, u32[]{:S(2)}) collective-permute-start(bf16[4,384,256]{2,1,0:T(8,128)(2,1)S(1)} %pad_maximum_fusion.3.refs_0_), channel_id=1, source_target_pairs={{0,4},{4,0},{8,12},{12,8},{16,20},{20,16},{24,28},{28,24},{1,5},{5... | collective-permute-start | bytes 2359304 | tf_op jit(solution)/shard_map/ppermute | solution.py:310
  129.2 18.8 %collective-permute-start.9 = (bf16[4,256,384]{2,1,0:T(8,128)(2,1)}, bf16[4,256,384]{2,1,0:T(8,128)(2,1)}, u32[]{:S(2)}, u32[]{:S(2)}) collective-permute-start(bf16[4,256,384]{2,1,0:T(8,128)(2,1)} %collective-permute-done.7.refs_1_), channel_id=1, source_target_pairs={{0,1},{1,0},{2,3},{3,2},{4,5},{5,4},{6,7},{7,6},{8,9},{9,8},{10,11... | collective-permute-start | bytes 2359304 | tf_op jit(solution)/shard_map/ppermute | solution.py:312
  129.4 18.7 %collective-permute-start.15 = (bf16[4,256,384]{2,1,0:T(8,128)(2,1)}, bf16[4,256,384]{2,1,0:T(8,128)(2,1)}, u32[]{:S(2)}, u32[]{:S(2)}) collective-permute-start(bf16[4,256,384]{2,1,0:T(8,128)(2,1)} %collective-permute-done.13.refs_5_), channel_id=1, source_target_pairs={{0,1},{1,0},{2,3},{3,2},{4,5},{5,4},{6,7},{7,6},{8,9},{9,8},{10,11... | collective-permute-start | bytes 2359304 | tf_op jit(solution)/shard_map/ppermute | solution.py:312
  132.9 34.2 %collective-permute-start.23 = (bf16[4,384,256]{2,1,0:T(8,128)(2,1)S(1)}, bf16[4,384,256]{2,1,0:T(8,128)(2,1)}, u32[]{:S(2)}, u32[]{:S(2)}) collective-permute-start(bf16[4,384,256]{2,1,0:T(8,128)(2,1)S(1)} %pad_maximum_fusion.3.refs_0_), channel_id=1, source_target_pairs={{0,1},{1,0},{2,3},{3,2},{4,5},{5,4},{6,7},{7,6},{8,9},{9,8},{10,11... | collective-permute-start | bytes 2359304 | tf_op jit(solution)/shard_map/ppermute | solution.py:312
  148.1 19.1 %collective-permute-start.24 = (bf16[4,384,256]{2,1,0:T(8,128)(2,1)}, bf16[4,384,256]{2,1,0:T(8,128)(2,1)}, u32[]{:S(2)}, u32[]{:S(2)}) collective-permute-start(bf16[4,384,256]{2,1,0:T(8,128)(2,1)} %collective-permute-done.22.refs_1_), channel_id=1, source_target_pairs={{0,1},{1,0},{2,3},{3,2},{4,5},{5,4},{6,7},{7,6},{8,9},{9,8},{10,11... | collective-permute-start | bytes 2359304 | tf_op jit(solution)/shard_map/ppermute | solution.py:312
  173.4 14.4 %collective-permute-start.25 = (bf16[4,32,2048]{2,1,0:T(8,128)(2,1)S(1)}, bf16[4,32,2048]{2,1,0:T(8,128)(2,1)S(1)}, u32[]{:S(2)}, u32[]{:S(2)}) collective-permute-start(bf16[4,32,2048]{2,1,0:T(8,128)(2,1)S(1)} %slice_bitcast_fusion), channel_id=1, source_target_pairs={{0,2},{1,3},{2,0},{3,1},{4,6},{5,7},{6,4},{7,5},{8,10},{9,11},{10,... | collective-permute-start | bytes 1572872 | tf_op jit(solution)/shard_map/ppermute | solution.py:299
  (22 other events, 338.7 us)

commit v3 on v2

--- a/solution.py
+++ b/solution.py
@@ -7,6 +7,7 @@
 from jax.experimental.pallas import tpu as pltpu
 from jax.sharding import PartitionSpec as P
 
+
 norm_eps = 1e-06
 highest = lax.Precision.HIGHEST
 f32 = jnp.float32
@@ -24,6 +25,10 @@
     total = jnp.dot(a0, b0, preferred_element_type=f32)
     total += jnp.dot(a0, b1, preferred_element_type=f32)
     return total + jnp.dot(a1, b0, preferred_element_type=f32)
+
+
+def over_rows(a, b):
+    return lax.dot_general(a, b, (((0,), (0,)), ((), ())), preferred_element_type=f32)
 
 
 def cos_sin(coarse, fine, count):
@@ -54,26 +59,29 @@
     return (iota((states, rows), 0) * when).astype(f32)
 
 
-def local_kernel(scal, xt, damp, in_map, readout, yt, ends, rows_a):
+def local_kernel(scal, half_step, xt, damp, in_map, readout, yt, ends, rows_a):
     groups, rows = damp.shape[1], damp.shape[2]
-    states, chans = in_map.shape[3], in_map.shape[4]
+    chans, states = in_map.shape[3], in_map.shape[4]
     part, quarter = states // 2, 2 * groups
-    lane = iota((part, ends.shape[1]), 1)
+    lane = iota((part, ends.shape[2]), 1)
+    slim = iota((8, ends.shape[2]), 1)
     row_id, col_id = iota((rows, rows), 0), iota((rows, rows), 1)
     kept = (row_id <= col_id, row_id >= col_id)
     for k in range(2):
-        rows_a[k] = jnp.dot(damp[k], kept[k].astype(f32), precision=highest)
+        steps = damp[k] + half_step[k]
+        rows_a[k] = jnp.dot(steps, kept[k].astype(f32), precision=highest)
     counts = [turns_of(states, rows, k == 1) for k in range(2)]
 
-    def group(g, held):
+    def group(g, carry):
+        held, spans = carry
         at = pl.ds(pl.multiple_of(g * chans, chans), chans)
         x = xt[at, :]
         total = jnp.zeros((chans, rows), f32)
         for k in range(2):
             cosine, sine = cos_sin(scal[0, k, g], scal[1, k, g], counts[k])
             scale = scal[2, k, g]
-            drive_r = jnp.dot(in_map[k, 0, g], x, preferred_element_type=f32) * scale
-            drive_i = jnp.dot(in_map[k, 1, g], x, preferred_element_type=f32) * scale
+            drive_r = over_rows(in_map[k, 0, g], x) * scale
+            drive_i = over_rows(in_map[k, 1, g], x) * scale
             turned = jnp.concatenate(
                 (cosine * drive_r + sine * drive_i, cosine * drive_i - sine * drive_r), axis=0
             )
@@ -85,16 +93,20 @@
             s_i = cosine * z_i + sine * z_r
             total += dot3(readout[k, 0, g], s_r) - dot3(readout[k, 1, g], s_i)
             last = 0 if k else rows - 1
+            spans = jnp.where(slim == k * groups + g, across[:8, last : last + 1], spans)
             for p, s in enumerate((s_r, s_i)):
                 col = s[:, last : last + 1]
                 for half in range(2):
                     spot = (half * 2 + p) * quarter + k * groups + g
                     held = jnp.where(lane == spot, col[half * part : (half + 1) * part], held)
         yt[at, :] = total
-        return held
-
-    held = lax.fori_loop(0, groups, group, jnp.zeros((part, ends.shape[1]), f32))
-    ends[...] = held
+        return held, spans
+
+    start = (jnp.zeros(lane.shape, f32), jnp.zeros(slim.shape, f32))
+    held, spans = lax.fori_loop(0, groups, group, start, unroll=4)
+    for peer in range(ends.shape[0]):
+        ends[peer, :part] = held
+        ends[peer, part:] = spans
 
 
 def carry_kernel(scal, place, xt, rows_a, lanes, every, readout, yt, skip, gain, out):
@@ -108,6 +120,7 @@
     coarse, fine = lanes[0:1, :], lanes[1:2, :]
     far_r, far_i = cos_sin(coarse, fine, number * rows)
     near_r, near_i = cos_sin(coarse, fine, number)
+
     def piece(b, p):
         ref = every.at[b]
         return jnp.concatenate(
@@ -173,7 +186,7 @@
     half_step = 0.5 * time_step
     coarse = jnp.floor(half_step * 2048.0) / 2048.0
     scal = jnp.stack((coarse, half_step - coarse, jnp.sqrt(-jnp.expm1(-time_step))))
-    damp = jnp.swapaxes(damping, 1, 2) + half_step[:, :, None]
+    damp = jnp.swapaxes(damping, 1, 2)
     xt = mixer_input.T
     lanes = 8 * groups
     smem = pl.BlockSpec(memory_space=pltpu.SMEM)
@@ -181,16 +194,14 @@
         local_kernel,
         out_shape=(
             jax.ShapeDtypeStruct((width, rows), f32),
-            jax.ShapeDtypeStruct((states // 2, lanes), f32),
+            jax.ShapeDtypeStruct((lax.axis_size("sp"), states // 2 + 8, lanes), f32),
             jax.ShapeDtypeStruct(damp.shape, f32),
         ),
-        in_specs=[smem] + vmem(4),
+        in_specs=[smem] + vmem(5),
         out_specs=tuple(vmem(3)),
         name="mixer_local",
-    )(scal, xt, damp, input_map, readout)
-    span = jnp.sum(damp, axis=2).reshape(1, -1)
-    extra = jnp.zeros((8, lanes), f32).at[:1, : span.shape[1]].set(span)
-    return scal, xt, yt, rows_a, jnp.concatenate((ends, extra), axis=0)
+    )(scal, half_step[:, :, None], xt, damp, jnp.swapaxes(input_map, 3, 4), readout)
+    return scal, xt, yt, rows_a, ends
 
 
 def mixer_carried(scal, xt, yt, rows_a, every, readout, skip_gain, out_gain):
@@ -236,13 +247,11 @@
     gate_taps,
     down_weight,
 ):
-    tp_count, sp_count = lax.axis_size("tp"), lax.axis_size("sp")
+    tp_count = lax.axis_size("tp")
     tok_rows, local_width = mixer_input.shape
     residual_rows = lax.all_gather(residual, "tp", axis=0, tiled=True)
     scal, xt, yt, rows_a, ends = mixer_local(mixer_input, time_step, damping, input_map, readout)
-    every = lax.all_to_all(
-        jnp.broadcast_to(ends[None], (sp_count,) + ends.shape), "sp", 0, 0, tiled=True
-    )
+    every = lax.all_to_all(ends, "sp", 0, 0, tiled=True)
     mixed = mixer_carried(scal, xt, yt, rows_a, every, readout, skip_gain, out_gain)
     mixed = lax.all_gather(mixed, "tp", axis=0)
     squares = jnp.sum(mixed[:, local_width:].astype(f32), axis=(0, 1))
@@ -299,17 +308,56 @@
     return [lax.ppermute(pick(s), axis, ring(axis, inner, s)) for s in range(1, outer)]
 
 
-def spread(slices):
-    outer = slices.shape[0]
-    mine = lax.axis_index("sp") // pair
-
-    def pick(step):
-        return lax.dynamic_index_in_dim(slices, lax.rem(mine + step, outer), 0, False)
-
-    own = jnp.stack([pick(0)] + outer_send(pick, "sp", pair))
+def cut_of(shapes, outer):
+    def call(*weights):
+        outs = tuple(
+            jax.ShapeDtypeStruct(shape, bf16) for shape in shapes for _ in range(outer)
+        )
+        hbm = pl.BlockSpec(memory_space=pltpu.HBM)
+        pieces = pl.pallas_call(
+            cut_all(len(weights)),
+            out_shape=outs,
+            in_specs=[hbm] * len(weights),
+            out_specs=tuple(vmem(len(outs))),
+            scratch_shapes=[pltpu.SemaphoreType.DMA((len(outs),))],
+            name="cut_weights",
+        )(*weights)
+        return [pieces[k * outer : (k + 1) * outer] for k in range(len(weights))]
+
+    return call
+
+
+def cut_all(count):
+    def kernel(*refs):
+        ins, outs, sems = refs[:count], refs[count:-1], refs[-1]
+        outer = len(outs) // count
+        mine = lax.axis_index("sp") // pair
+        copies = []
+        for w in range(count):
+            for s in range(outer):
+                out = outs[w * outer + s]
+                rows, cols = out.shape
+                there = lax.rem(mine + s, outer)
+                if rows == ins[w].shape[0]:
+                    part = ins[w].at[:, pl.ds(pl.multiple_of(there * cols, cols), cols)]
+                else:
+                    part = ins[w].at[pl.ds(pl.multiple_of(there * rows, rows), rows), :]
+                copy = pltpu.make_async_copy(part, out, sems.at[w * outer + s])
+                copy.start()
+                copies.append(copy)
+        for copy in copies:
+            copy.wait()
+
+    return kernel
+
+
+def spread(pieces):
+    moved = outer_send(lambda s: pieces[s], "sp", pair)
+    own = jnp.stack([pieces[0]] + moved)
     beside = lax.ppermute(own, "sp", ring("sp", pair, 0, 1))
     over = ring("tp", pair, 0, 1)
-    return own, beside, lax.ppermute(own, "tp", over), lax.ppermute(beside, "tp", over)
+    across = lax.ppermute(own, "tp", over)
+    return own, beside, across, lax.ppermute(beside, "tp", over)
 
 
 pair = 2
@@ -321,36 +369,47 @@
     return far * pair + lax.rem(sp + which, pair)
 
 
-def up_kernel(x, *refs):
-    stacks, (out, full, sems) = refs[:8], refs[8:]
+def up_kernel(*refs):
+    stacks, (out, edges, x, last, full, sems) = refs[:8], refs[-6:]
+    rows_in = refs[8:-6]
     outer, rows, cols = stacks[0].shape
     groups = []
     for kind in range(2):
+        copies = []
         for core in range(2):
-            copies = []
             for which in range(2):
                 ref = stacks[kind * 4 + core * 2 + which]
                 for s in range(outer):
                     first = pl.multiple_of(row_block(outer, which, s) * rows, rows)
-                    slot = kind * 2 + core
                     copy = pltpu.make_async_copy(
                         ref.at[s],
-                        full.at[slot, pl.ds(first, rows), :],
-                        sems.at[slot, which * outer + s],
+                        full.at[kind, pl.ds(first, rows), pl.ds(core * cols, cols)],
+                        sems.at[kind * 2 + core, which * outer + s],
                     )
                     copy.start()
                     copies.append(copy)
-            groups.append(copies)
-    for slot, copies in enumerate(groups):
+        groups.append(copies)
+    each = rows_in[0].shape[0]
+    for s, ref in enumerate(rows_in):
+        x[s * each : (s + 1) * each, :] = ref[...]
+    pieces = edges.shape[1]
+    for kind, copies in enumerate(groups):
         for copy in copies:
             copy.wait()
-        out[:, slot * cols : (slot + 1) * cols] = jnp.dot(
-            x[...], full[slot], preferred_element_type=f32
-        ).astype(bf16)
+        part = jnp.dot(x[...], full[kind], preferred_element_type=f32)
+        first = 2 * kind * cols
+        out[:, first : first + 2 * cols] = part.astype(bf16)
+        length = part.shape[0] // pieces
+        for p in range(pieces):
+            for end, at in ((0, p * length), (1, (p + 1) * length - 1)):
+                row = part[at : at + 1]
+                last[end, p : p + 1, first : first + cols] = row[:, cols:]
+                last[end, p : p + 1, first + cols : first + 2 * cols] = row[:, :cols]
+    edges[...] = last[...].astype(bf16)
 
 
 def down_kernel(up, before, after, taps, *refs):
-    stacks, (out, full, sems) = refs[:4], refs[4:]
+    stacks, outs, (full, sems) = refs[:4], refs[4:-2], refs[-2:]
     outer, rows, cols = stacks[0].shape
     copies = []
     for core in range(2):
@@ -386,31 +445,44 @@
     hidden = (convolved(0) * (gate / (1.0 + jnp.exp(-gate)))).astype(bf16)
     for copy in copies:
         copy.wait()
-    out[...] = jnp.dot(hidden, full[...], preferred_element_type=f32).astype(bf16)
-
-
-def up_projection(x, stacks):
+    partial = jnp.dot(hidden, full[...], preferred_element_type=f32).astype(bf16)
+    for p in range(pieces):
+        outs[p % len(outs)][p // len(outs)] = partial[p * length : (p + 1) * length]
+
+
+def up_projection(rows_in, stacks, pieces):
     outer, rows, cols = stacks[0].shape
+    count = sum(r.shape[0] for r in rows_in)
     return pl.pallas_call(
         up_kernel,
-        out_shape=jax.ShapeDtypeStruct((x.shape[0], 4 * cols), bf16),
-        in_specs=vmem(1) + [pl.BlockSpec(memory_space=pltpu.HBM)] * 8,
-        out_specs=pl.BlockSpec(memory_space=pltpu.VMEM),
+        out_shape=(
+            jax.ShapeDtypeStruct((count, 4 * cols), bf16),
+            jax.ShapeDtypeStruct((2, pieces, 4 * cols), bf16),
+        ),
+        in_specs=[pl.BlockSpec(memory_space=pltpu.HBM)] * 8 + vmem(len(rows_in)),
+        out_specs=tuple(vmem(2)),
         scratch_shapes=[
-            pltpu.VMEM((4, 2 * outer * rows, cols), bf16),
+            pltpu.VMEM((count, rows_in[0].shape[1]), bf16),
+            pltpu.VMEM((2, pieces, 4 * cols), f32),
+            pltpu.VMEM((2, 2 * outer * rows, 2 * cols), bf16),
             pltpu.SemaphoreType.DMA((4, 2 * outer)),
         ],
         name="up_projection",
-    )(x, *stacks)
-
-
-def down_projection(up, before, after, taps, stacks):
+    )(*stacks, *rows_in)
+
+
+def down_projection(up, before, after, taps, stacks, inner):
     outer, rows, cols = stacks[0].shape
     return pl.pallas_call(
         down_kernel,
-        out_shape=jax.ShapeDtypeStruct((up.shape[0], 2 * outer * cols), bf16),
+        out_shape=(
+            jax.ShapeDtypeStruct(
+                (outer, up.shape[0] // (outer * inner), 2 * outer * cols), bf16
+            ),
+        )
+        * inner,
         in_specs=vmem(4) + [pl.BlockSpec(memory_space=pltpu.HBM)] * 4,
-        out_specs=pl.BlockSpec(memory_space=pltpu.VMEM),
+        out_specs=tuple(vmem(inner)),
         scratch_shapes=[
             pltpu.VMEM((2 * rows, 2 * outer * cols), bf16),
             pltpu.SemaphoreType.DMA((4, outer)),
@@ -419,12 +491,10 @@
     )(up, before, after, taps, *stacks)
 
 
-def edges_of(up, outer, inner):
+def edges_of(ends, outer, inner):
     sp, tp = lax.axis_index("sp"), lax.axis_index("tp")
     z, y, x, c = sp // pair, lax.rem(sp, pair), tp // pair, lax.rem(tp, pair)
-    cells = up.reshape(outer, inner, -1, 2, 2, up.shape[1] // 4)[:, :, :, :, ::-1]
-    cells = cells.reshape(outer, inner, -1, up.shape[1])
-    ends = jnp.stack((cells[:, :, 0], cells[:, :, -1]))
+    ends = ends.reshape(2, outer, inner, -1)
     across = lax.ppermute(ends, "tp", ring("tp", pair, 0, 1))
     rim = jnp.where(c == 0, lax.rem(inner - x, inner), inner - 1 - x)
     out_edge = lax.dynamic_index_in_dim(
@@ -471,18 +541,16 @@
     outer, inner = sp_count // pair, tp_count // pair
     tok_rows, local_width = mixer_input.shape
     own_rows = tok_rows // tp_count
-    model = residual.shape[1]
     z, tp = lax.axis_index("sp") // pair, lax.axis_index("tp")
 
-    def columns(weight):
-        return jnp.swapaxes(weight.reshape(weight.shape[0], outer, -1), 0, 1)
-
-    value_stacks = spread(columns(value_weight))
+    wide = (value_weight.shape[0], value_weight.shape[1] // outer)
+    deep = (down_weight.shape[0] // outer, down_weight.shape[1])
+    (value_pieces,) = cut_of((wide,), outer)(value_weight)
+    gate_pieces, down_pieces = cut_of((wide, deep), outer)(gate_weight, down_weight)
+    value_stacks = spread(value_pieces)
     scal, xt, yt, rows_a, ends = mixer_local(mixer_input, time_step, damping, input_map, readout)
-    every = lax.all_to_all(
-        jnp.broadcast_to(ends[None], (sp_count,) + ends.shape), "sp", 0, 0, tiled=True
-    )
-    gate_stacks = spread(columns(gate_weight))
+    every = lax.all_to_all(ends, "sp", 0, 0, tiled=True)
+    gate_stacks = spread(gate_pieces)
     others = outer_send(lambda s: residual, "tp", pair)
     taps = jnp.stack((value_taps, gate_taps), axis=1).reshape(-1, value_taps.shape[1])
     taps = lax.dynamic_index_in_dim(taps.reshape(taps.shape[0], outer, -1), z, 1, False)
@@ -512,14 +580,13 @@
     state_wide = hidden_state.astype(f32)
     scale_rows = lax.rsqrt(jnp.mean(state_wide * state_wide, axis=1, keepdims=True) + norm_eps)
     normed = (state_wide * scale_rows * channel_gain[None, :]).astype(bf16)
-    x_rows = jnp.concatenate([normed] + outer_send(lambda s: normed, "sp", pair), axis=0)
-    up = up_projection(x_rows, value_stacks + gate_stacks)
-    down_stacks = spread(down_weight.reshape(outer, -1, down_weight.shape[1]))
-    before, after = edges_of(up, outer, inner)
-    partial = down_projection(up, before, after, taps, down_stacks)
-    parts = partial.reshape(outer, inner, own_rows, model)
-    total = parts[:, 0].astype(f32)
-    for got in outer_send(lambda s: parts[:, s], "tp", pair):
+    moved = outer_send(lambda s: normed, "sp", pair)
+    up, ends = up_projection([normed] + moved, value_stacks + gate_stacks, outer * inner)
+    down_stacks = spread(down_pieces)
+    before, after = edges_of(ends, outer, inner)
+    parts = down_projection(up, before, after, taps, down_stacks, inner)
+    total = parts[0].astype(f32)
+    for got in outer_send(lambda s: parts[s], "tp", pair):
         total = total + got.astype(f32)
     total = total.astype(bf16)
     summed = total[0].astype(f32)
@@ -553,6 +620,8 @@
         sp, tp = mesh.shape["sp"], mesh.shape["tp"]
         even = sp % pair == 0 and tp % pair == 0
         whole_lanes = even and (value_weight.shape[1] // (sp // pair)) % 128 == 0
-        return (spread_body if whole_lanes else gathered_body)(*args)
+        if not whole_lanes:
+            return gathered_body(*args)
+        return spread_body(*args)
 
     return jax.shard_map(body, mesh=mesh, in_specs=in_specs, out_specs=out_specs, check_vma=False)

time: 206 us -> 183 us (0.89)
  local copies, waits for them, and re-layouts: 24.6 us -> 9.43 us
  other arithmetic: 14.5 us -> 9.74 us
  waiting for transfers between devices: 62.5 us -> 58.8 us
  Pallas kernels: 32.2 us -> 35.7 us
  starting transfers between devices: 61.8 us -> 58.3 us
    ppermute x3, waiting for transfers between devices: 15 us -> 7.39 us  [spread(): beside = lax.ppermute(own, 'sp', ring('sp', pair, 0, 1))]
    pallas_call x2 -> x4, Pallas kernels: 12.1 us -> 17 us  [the longest x1 6.88 us: up_projection(): pl.pallas_call(up_kernel, out_shape=(jax.ShapeDtypeStruct((count, 4 * col...]
    rev x1 -> x0, local copies, waits for them, and re-layouts: 4.17 us -> none  [edges_of(): up.reshape(outer, inner, -1, 2, 2, up.shape[1] // 4)[:, :, :, :, ::-1]]
    unnamed x45 -> x35, local copies, waits for them, and re-layouts: 8.29 us -> 4.18 us
    ppermute x17, starting transfers between devices: 49 us -> 45.1 us  [outer_send(): lax.ppermute(pick(s), axis, ring(axis, inner, s))]
    ppermute x17, waiting for transfers between devices: 45.7 us -> 49.5 us  [outer_send(): lax.ppermute(pick(s), axis, ring(axis, inner, s))]
    another operation x2 -> x0, local copies, waits for them, and re-layouts: 3.39 us -> none
    concatenate x2 -> x0, other arithmetic: 2.95 us -> none  [the longest x1 2.22 us: spread_body(): jnp.concatenate([normed] + outer_send(lambda s: normed, 'sp', pair), axis=0)]
  transfers between devices with their start and end apart: 30 -> 30, of which waited for: 9 -> 9; matrix products, arithmetic and copies ran while one was open for 15% -> 8% of each run, Pallas kernels for 6% -> 9%
where the time goes in v3:
time: 183 us; the launch traced here: 181 us
  waiting for transfers between devices  58.8 us (32%)
  starting transfers between devices  58.3 us (32%)
  Pallas kernels  35.7 us (20%)
  other arithmetic  9.74 us (5%)
  local copies, waits for them, and re-layouts  9.43 us (5%)
  blocking collectives  6.04 us (3%)
  matrix products  2.98 us (2%)
    ppermute x17, waiting for transfers between devices, outer_send(): lax.ppermute(pick(s), axis, ring(axis, inner, s))  49.5 us
    ppermute x17, starting transfers between devices, outer_send(): lax.ppermute(pick(s), axis, ring(axis, inner, s))  45.1 us
    pallas_call x1, Pallas kernels, mixer_local(): pl.pallas_call(local_kernel, out_shape=(jax.ShapeDtypeStruct((width, rows...  14.1 us
    ppermute x3, waiting for transfers between devices, spread(): beside = lax.ppermute(own, 'sp', ring('sp', pair, 0, 1))  7.39 us
    all_to_all x1, starting transfers between devices, spread_body(): every = lax.all_to_all(ends, 'sp', 0, 0, tiled=True)  7.31 us
    pallas_call x1, Pallas kernels, up_projection(): pl.pallas_call(up_kernel, out_shape=(jax.ShapeDtypeStruct((count, 4 * col...  6.88 us
    all_gather x1, blocking collectives, spread_body(): mixed = lax.all_gather(mixed, 'tp', axis=0)  6.04 us
    pallas_call x1, Pallas kernels, down_projection(): pl.pallas_call(down_kernel, out_shape=(jax.ShapeDtypeStruct((outer, up.sh...  5.22 us
  transfers between devices with their start and end apart: 30, of which 9 were waited for; matrix products, arithmetic and copies ran while one was open for 8% of the time, Pallas kernels for 9%

profile of v3, /device:TPU:0, one launch (start us, length us, event | category | flops | bytes accessed | tf_op | source)
XLA Modules:
  0.0 181.5 jit_solution(1681721056720371588)
XLA Ops:
  3.6 14.1 %mixer_local.1 = (f32[256,128]{1,0:T(8,128)}, f32[8,40,128]{2,1,0:T(8,128)}, f32[2,16,128]{2,1,0:T(8,128)}) custom-call(f32[3,2,16]{2,1,0:T(2,128)} %pad_maximum_fusion.7.scal, f32[2,16,1]{2,1,0:T(8,128)} %copy.19.half_step, bf16[256,128]{1,0:T(8,128)(2,1)} %bitcast.56, f32[2,16,128]{2,1,0:T(8,128)} %bitcast.72, bf16[2,2,16,16,64]{4,3,2,1,0:T(8,128)(2,1)} %bitcast.58, ...), custom_call_target="tpu_custom_call" | custom-call | tf_op jit(solution)/shard_map/mixer_local/pallas_call | solution.py:193
  17.7 7.3 %all-to-all-start = ((f32[8,40,128]{2,1,0:T(8,128)}), f32[8,40,128]{2,1,0:T(8,128)S(1)}, u32[]{:S(2)}, u32[]{:S(2)}) async-start(f32[8,40,128]{2,1,0:T(8,128)} %get-tuple-element.25), calls=%async_computation | async-start | bytes 327680 | tf_op jit(solution)/shard_map/all_to_all | solution.py:552
  25.0 2.8 %cut_weights.3 = (bf16[256,384]{1,0:T(8,128)(2,1)}, bf16[256,384]{1,0:T(8,128)(2,1)}, bf16[256,384]{1,0:T(8,128)(2,1)}, bf16[256,384]{1,0:T(8,128)(2,1)}, bf16[3...) custom-call(bf16[256,1536]{1,0:T(8,128)(2,1)} %refs_0_.3, ...), custom_call_target="tpu_custom_call" | custom-call | tf_op jit(solution)/shard_map/cut_weights/pallas_call | solution.py:317
  27.7 2.1 %collective-permute-start.7 = (bf16[256,384]{1,0:T(8,128)(2,1)}, bf16[256,384]{1,0:T(8,128)(2,1)S(1)}, u32[]{:S(2)}, u32[]{:S(2)}) collective-permute-start(bf16[256,384]{1,0:T(8,128)(2,1)} %get-tuple-element.32), channel_id=1, source_target_pairs={{0,8},{4,12},{8,16},{12,20},{16,24},{20,28},{24,0},{28,4},{1,9},{5... | collective-permute-start | bytes 589832 | tf_op jit(solution)/shard_map/ppermute | solution.py:308
  29.8 2.4 %collective-permute-start.8 = (bf16[256,384]{1,0:T(8,128)(2,1)}, bf16[256,384]{1,0:T(8,128)(2,1)S(1)}, u32[]{:S(2)}, u32[]{:S(2)}) collective-permute-start(bf16[256,384]{1,0:T(8,128)(2,1)} %get-tuple-element.33), channel_id=1, source_target_pairs={{0,16},{4,20},{8,24},{12,28},{16,0},{20,4},{24,8},{28,12},{1,17},{... | collective-permute-start | bytes 589832 | tf_op jit(solution)/shard_map/ppermute | solution.py:308
  33.6 2.1 %cut_weights.2 = (bf16[256,384]{1,0:T(8,128)(2,1)}, bf16[256,384]{1,0:T(8,128)(2,1)}, bf16[256,384]{1,0:T(8,128)(2,1)}, bf16[256,384]{1,0:T(8,128)(2,1)}) custom-call(bf16[256,1536]{1,0:T(8,128)(2,1)} %refs_0_.2), custom_call_target="tpu_custom_call" | custom-call | tf_op jit(solution)/shard_map/cut_weights/pallas_call | solution.py:317
  38.0 2.8 %collective-permute-start.3 = (bf16[256,384]{1,0:T(8,128)(2,1)}, bf16[256,384]{1,0:T(8,128)(2,1)S(1)}, u32[]{:S(2)}, u32[]{:S(2)}) collective-permute-start(bf16[256,384]{1,0:T(8,128)(2,1)} %get-tuple-element.30), channel_id=1, source_target_pairs={{0,24},{4,28},{8,0},{12,4},{16,8},{20,12},{24,16},{28,20},{1,25},{... | collective-permute-start | bytes 589832 | tf_op jit(solution)/shard_map/ppermute | solution.py:308
  43.6 8.4 %collective-permute-done.8 = bf16[256,384]{1,0:T(8,128)(2,1)S(1)} collective-permute-done((bf16[256,384]{1,0:T(8,128)(2,1)}, bf16[256,384]{1,0:T(8,128)(2,1)S(1)}, u32[]{:S(2)}, u32[]{:S(2)}) %collective-permute-start.8) | collective-permute-done | bytes 196640 | tf_op jit(solution)/shard_map/ppermute | solution.py:308
  54.6 7.6 %collective-permute-start.19 = (bf16[384,256]{1,0:T(8,128)(2,1)}, bf16[384,256]{1,0:T(8,128)(2,1)S(1)}, u32[]{:S(2)}, u32[]{:S(2)}) collective-permute-start(bf16[384,256]{1,0:T(8,128)(2,1)} %get-tuple-element.38), channel_id=1, source_target_pairs={{0,8},{4,12},{8,16},{12,20},{16,24},{20,28},{24,0},{28,4},{1,9},{5... | collective-permute-start | bytes 589832 | tf_op jit(solution)/shard_map/ppermute | solution.py:308
  67.2 4.6 %mixer_carried.1 = bf16[272,128]{1,0:T(8,128)(2,1)} custom-call(f32[3,2,16]{2,1,0:T(2,128)} %pad_maximum_fusion.7.scal, s32[1]{0:T(128)} %bitcast.3.place, bf16[256,128]{1,0:T(8,128)(2,1)} %bitcast.57, f32[2,16,128]{2,1,0:T(8,128)} %get-tuple-element.24.rows_a, f32[2,32]{1,0:T(2,128)} %pad_maximum_fusion.8.lanes, f32[8,40,128]{2,1,0:T(8,128)} %copy-done.6, ...), custom_call_target="tpu_custom_call" | custom-call | tf_op jit(solution)/shard_map/mixer_carried/pallas_call | solution.py:212
  71.9 6.0 %all-gather = bf16[1088,128]{1,0:T(8,128)(2,1)S(1)} all-gather(bf16[272,128]{1,0:T(8,128)(2,1)} %mixer_carried.1), channel_id=2, replica_groups=mesh['sp'=8,'tp'=4] {'tp'}, dimensions={0}, use_global_device_ids=true | all-gather | bytes 348160 | tf_op jit(solution)/shard_map/all_gather | solution.py:561
  78.0 3.0 %convolution_multiply_fusion = f32[128,2048]{1,0:T(8,128)S(1)} fusion(bf16[1024,128]{1,0:T(8,128)(2,1)S(1)} %bitcast.55, bf16[1024,2048]{1,0:T(8,128)(2,1)} %param.22, f32[128]{0:T(128)S(1)} %add_rsqrt_fusion.1), kind=kOutput, calls=%fused_computation | convolution fusion | flops 537133056 | bytes 5505536 | tf_op jit(solution)/shard_map/dot_general | solution.py:566
  82.0 10.9 %collective-permute-start.13 = (bf16[64,2048]{1,0:T(8,128)(2,1)S(1)}, bf16[64,2048]{1,0:T(8,128)(2,1)S(1)}, u32[]{:S(2)}, u32[]{:S(2)}) collective-permute-start(bf16[64,2048]{1,0:T(8,128)(2,1)S(1)} %multiply_convert_fusion.refs_8_), channel_id=1, source_target_pairs={{0,8},{4,12},{8,16},{12,20},{16,24},{20,28},{24,0},{28,4},{1,9},{5... | collective-permute-start | bytes 786440 | tf_op jit(solution)/shard_map/ppermute | solution.py:308
  94.5 9.4 %collective-permute-done.21 = bf16[384,256]{1,0:T(8,128)(2,1)S(1)} collective-permute-done((bf16[384,256]{1,0:T(8,128)(2,1)S(1)}, bf16[384,256]{1,0:T(8,128)(2,1)S(1)}, u32[]{:S(2)}, u32[]{:S(2)}) %collective-permute-start.21) | collective-permute-done | bytes 196640 | tf_op jit(solution)/shard_map/ppermute | solution.py:308
  105.0 5.9 %collective-permute-done.14.refs_10_ = bf16[64,2048]{1,0:T(8,128)(2,1)S(1)} collective-permute-done((bf16[64,2048]{1,0:T(8,128)(2,1)S(1)}, bf16[64,2048]{1,0:T(8,128)(2,1)S(1)}, u32[]{:S(2)}, u32[]{:S(2)}) %collective-permute-start.14) | collective-permute-done | bytes 262176 | tf_op jit(solution)/shard_map/ppermute | solution.py:308
  110.8 6.4 %collective-permute-start.15 = (bf16[64,2048]{1,0:T(8,128)(2,1)S(1)}, bf16[64,2048]{1,0:T(8,128)(2,1)S(1)}, u32[]{:S(2)}, u32[]{:S(2)}) collective-permute-start(bf16[64,2048]{1,0:T(8,128)(2,1)S(1)} %multiply_convert_fusion.refs_8_), channel_id=1, source_target_pairs={{0,24},{4,28},{8,0},{12,4},{16,8},{20,12},{24,16},{28,20},{1,25},{... | collective-permute-start | bytes 786440 | tf_op jit(solution)/shard_map/ppermute | solution.py:308
  118.4 4.1 %collective-permute-done.15.refs_11_ = bf16[64,2048]{1,0:T(8,128)(2,1)S(1)} collective-permute-done((bf16[64,2048]{1,0:T(8,128)(2,1)S(1)}, bf16[64,2048]{1,0:T(8,128)(2,1)S(1)}, u32[]{:S(2)}, u32[]{:S(2)}) %collective-permute-start.15) | collective-permute-done | bytes 262176 | tf_op jit(solution)/shard_map/ppermute | solution.py:308
  125.0 6.9 %up_projection.1 = (bf16[256,1536]{1,0:T(8,128)(2,1)}, bf16[2,8,1536]{2,1,0:T(8,128)(2,1)}) custom-call(bf16[4,256,384]{2,1,0:T(8,128)(2,1)} %copy-done.1, bf16[4,256,384]{2,1,0:T(8,128)(2,1)} %collective-permute-done.4.refs_1_, bf16[4,256,384]{2,1,0:T(8,128)(2,1)} %collective-permute-done.5.refs_2_, bf16[4,256,384]{2,1,0:T(8,128)(2,1)} %collective-permute-done.6.refs_3_, ...), custom_call_target="tpu_custom_call" | custom-call | tf_op jit(solution)/shard_map/up_projection/pallas_call | solution.py:456
  134.1 7.4 %collective-permute-done.22.refs_1_ = bf16[4,384,256]{2,1,0:T(8,128)(2,1)} collective-permute-done((bf16[4,384,256]{2,1,0:T(8,128)(2,1)S(1)}, bf16[4,384,256]{2,1,0:T(8,128)(2,1)}, u32[]{:S(2)}, u32[]{:S(2)}) %collective-permute-start.22) | collective-permute-done | bytes 786464 | tf_op jit(solution)/shard_map/ppermute | solution.py:357
  147.0 5.2 %down_projection.1 = (bf16[4,32,2048]{2,1,0:T(8,128)(2,1)}, bf16[4,32,2048]{2,1,0:T(8,128)(2,1)}) custom-call(bf16[256,1536]{1,0:T(8,128)(2,1)} %get-tuple-element.35.up, bf16[8,1536]{1,0:T(8,128)(2,1)} %select_select_fusion.1.before, bf16[8,1536]{1,0:T(8,128)(2,1)} %select_select_fusion.after, f32[3,1536]{1,0:T(4,128)} %reshape.82.taps, ...), custom_call_target="tpu_custom_call" | custom-call | tf_op jit(solution)/shard_map/down_projection/pallas_call | solution.py:476
  152.8 13.6 %collective-permute-done.25 = bf16[4,32,2048]{2,1,0:T(8,128)(2,1)S(1)} collective-permute-done((bf16[4,32,2048]{2,1,0:T(8,128)(2,1)}, bf16[4,32,2048]{2,1,0:T(8,128)(2,1)S(1)}, u32[]{:S(2)}, u32[]{:S(2)}) %collective-permute-start.25) | collective-permute-done | bytes 524320 | tf_op jit(solution)/shard_map/ppermute | solution.py:308
  167.7 4.8 %collective-permute-start.27 = (bf16[32,2048]{1,0:T(8,128)(2,1)S(1)}, bf16[32,2048]{1,0:T(8,128)(2,1)S(1)}, u32[]{:S(2)}, u32[]{:S(2)}) collective-permute-start(bf16[32,2048]{1,0:T(8,128)(2,1)S(1)} %get-tuple-element.49), channel_id=1, source_target_pairs={{0,16},{4,20},{8,24},{12,28},{16,0},{20,4},{24,8},{28,12},{1,17},{... | collective-permute-start | bytes 393224 | tf_op jit(solution)/shard_map/ppermute | solution.py:308
  172.6 3.9 %collective-permute-done.26 = bf16[32,2048]{1,0:T(8,128)(2,1)S(1)} collective-permute-done((bf16[32,2048]{1,0:T(8,128)(2,1)S(1)}, bf16[32,2048]{1,0:T(8,128)(2,1)S(1)}, u32[]{:S(2)}, u32[]{:S(2)}) %collective-permute-start.26) | collective-permute-done | bytes 131104 | tf_op jit(solution)/shard_map/ppermute | solution.py:308
  176.5 4.2 %collective-permute-done.27 = bf16[32,2048]{1,0:T(8,128)(2,1)S(1)} collective-permute-done((bf16[32,2048]{1,0:T(8,128)(2,1)S(1)}, bf16[32,2048]{1,0:T(8,128)(2,1)S(1)}, u32[]{:S(2)}, u32[]{:S(2)}) %collective-permute-start.27) | collective-permute-done | bytes 131104 | tf_op jit(solution)/shard_map/ppermute | solution.py:308
  (132 shorter events, 35.1 us)
Async XLA Ops:
  17.7 48.9 %all-to-all-start = ((f32[8,40,128]{2,1,0:T(8,128)}), f32[8,40,128]{2,1,0:T(8,128)S(1)}, u32[]{:S(2)}, u32[]{:S(2)}) async-start(f32[8,40,128]{2,1,0:T(8,128)} %get-tuple-element.25), calls=%async_computation | async-start | bytes 327680 | tf_op jit(solution)/shard_map/all_to_all | solution.py:552
  29.8 22.2 %collective-permute-start.8 = (bf16[256,384]{1,0:T(8,128)(2,1)}, bf16[256,384]{1,0:T(8,128)(2,1)S(1)}, u32[]{:S(2)}, u32[]{:S(2)}) collective-permute-start(bf16[256,384]{1,0:T(8,128)(2,1)} %get-tuple-element.33), channel_id=1, source_target_pairs={{0,16},{4,20},{8,24},{12,28},{16,0},{20,4},{24,8},{28,12},{1,17},{... | collective-permute-start | bytes 589832 | tf_op jit(solution)/shard_map/ppermute | solution.py:308
  32.2 21.4 %collective-permute-start.9 = (bf16[256,384]{1,0:T(8,128)(2,1)}, bf16[256,384]{1,0:T(8,128)(2,1)S(1)}, u32[]{:S(2)}, u32[]{:S(2)}) collective-permute-start(bf16[256,384]{1,0:T(8,128)(2,1)} %get-tuple-element.34), channel_id=1, source_target_pairs={{0,24},{4,28},{8,0},{12,4},{16,8},{20,12},{24,16},{28,20},{1,25},{... | collective-permute-start | bytes 589832 | tf_op jit(solution)/shard_map/ppermute | solution.py:308
  35.8 18.8 %collective-permute-start.1 = (bf16[256,384]{1,0:T(8,128)(2,1)}, bf16[256,384]{1,0:T(8,128)(2,1)S(1)}, u32[]{:S(2)}, u32[]{:S(2)}) collective-permute-start(bf16[256,384]{1,0:T(8,128)(2,1)} %get-tuple-element.28), channel_id=1, source_target_pairs={{0,8},{4,12},{8,16},{12,20},{16,24},{20,28},{24,0},{28,4},{1,9},{5... | collective-permute-start | bytes 589832 | tf_op jit(solution)/shard_map/ppermute | solution.py:308
  36.4 25.8 %collective-permute-start.2 = (bf16[256,384]{1,0:T(8,128)(2,1)}, bf16[256,384]{1,0:T(8,128)(2,1)S(1)}, u32[]{:S(2)}, u32[]{:S(2)}) collective-permute-start(bf16[256,384]{1,0:T(8,128)(2,1)} %get-tuple-element.29), channel_id=1, source_target_pairs={{0,16},{4,20},{8,24},{12,28},{16,0},{20,4},{24,8},{28,12},{1,17},{... | collective-permute-start | bytes 589832 | tf_op jit(solution)/shard_map/ppermute | solution.py:308
  38.0 26.0 %collective-permute-start.3 = (bf16[256,384]{1,0:T(8,128)(2,1)}, bf16[256,384]{1,0:T(8,128)(2,1)S(1)}, u32[]{:S(2)}, u32[]{:S(2)}) collective-permute-start(bf16[256,384]{1,0:T(8,128)(2,1)} %get-tuple-element.30), channel_id=1, source_target_pairs={{0,24},{4,28},{8,0},{12,4},{16,8},{20,12},{24,16},{28,20},{1,25},{... | collective-permute-start | bytes 589832 | tf_op jit(solution)/shard_map/ppermute | solution.py:308
  52.0 29.0 %collective-permute-start = (bf16[32,2048]{1,0:T(8,128)(2,1)S(1)}, bf16[32,2048]{1,0:T(8,128)(2,1)S(1)}, u32[]{:S(2)}, u32[]{:S(2)}) collective-permute-start(bf16[32,2048]{1,0:T(8,128)(2,1)S(1)} %copy-done.12), channel_id=1, source_target_pairs={{0,2},{1,3},{2,0},{3,1},{4,6},{5,7},{6,4},{7,5},{8,10},{9,11},{10,... | collective-permute-start | bytes 393224 | tf_op jit(solution)/shard_map/ppermute | solution.py:308
  53.5 28.5 %collective-permute-start.18 = (f32[6,384]{1,0:T(8,128)S(1)}, f32[6,384]{1,0:T(8,128)S(1)}, u32[]{:S(2)}, u32[]{:S(2)}) collective-permute-start(f32[6,384]{1,0:T(8,128)S(1)} %bitcast.73), channel_id=1, source_target_pairs={{0,1},{1,0},{2,3},{3,2},{4,5},{5,4},{6,7},{7,6},{8,9},{9,8},{10,11... | collective-permute-start | bytes 27656 | tf_op jit(solution)/shard_map/ppermute | solution.py:557
  54.6 38.3 %collective-permute-start.19 = (bf16[384,256]{1,0:T(8,128)(2,1)}, bf16[384,256]{1,0:T(8,128)(2,1)S(1)}, u32[]{:S(2)}, u32[]{:S(2)}) collective-permute-start(bf16[384,256]{1,0:T(8,128)(2,1)} %get-tuple-element.38), channel_id=1, source_target_pairs={{0,8},{4,12},{8,16},{12,20},{16,24},{20,28},{24,0},{28,4},{1,9},{5... | collective-permute-start | bytes 589832 | tf_op jit(solution)/shard_map/ppermute | solution.py:308
  62.2 30.8 %collective-permute-start.20 = (bf16[384,256]{1,0:T(8,128)(2,1)}, bf16[384,256]{1,0:T(8,128)(2,1)}, u32[]{:S(2)}, u32[]{:S(2)}) collective-permute-start(bf16[384,256]{1,0:T(8,128)(2,1)} %get-tuple-element.39), channel_id=1, source_target_pairs={{0,16},{4,20},{8,24},{12,28},{16,0},{20,4},{24,8},{28,12},{1,17},{... | collective-permute-start | bytes 589832 | tf_op jit(solution)/shard_map/ppermute | solution.py:308
  64.0 40.5 %collective-permute-start.10 = (bf16[4,256,384]{2,1,0:T(8,128)(2,1)S(1)}, bf16[4,256,384]{2,1,0:T(8,128)(2,1)}, u32[]{:S(2)}, u32[]{:S(2)}) collective-permute-start(bf16[4,256,384]{2,1,0:T(8,128)(2,1)S(1)} %pad_maximum_fusion.1.refs_4_), channel_id=1, source_target_pairs={{0,4},{4,0},{8,12},{12,8},{16,20},{20,16},{24,28},{28,24},{1,5},{5... | collective-permute-start | bytes 2359304 | tf_op jit(solution)/shard_map/ppermute | solution.py:357
  81.0 23.5 %collective-permute-start.4 = (bf16[4,256,384]{2,1,0:T(8,128)(2,1)S(1)}, bf16[4,256,384]{2,1,0:T(8,128)(2,1)}, u32[]{:S(2)}, u32[]{:S(2)}) collective-permute-start(bf16[4,256,384]{2,1,0:T(8,128)(2,1)S(1)} %pad_maximum_fusion.refs_0_), channel_id=1, source_target_pairs={{0,4},{4,0},{8,12},{12,8},{16,20},{20,16},{24,28},{28,24},{1,5},{5... | collective-permute-start | bytes 2359304 | tf_op jit(solution)/shard_map/ppermute | solution.py:357
  82.0 21.9 %collective-permute-start.13 = (bf16[64,2048]{1,0:T(8,128)(2,1)S(1)}, bf16[64,2048]{1,0:T(8,128)(2,1)S(1)}, u32[]{:S(2)}, u32[]{:S(2)}) collective-permute-start(bf16[64,2048]{1,0:T(8,128)(2,1)S(1)} %multiply_convert_fusion.refs_8_), channel_id=1, source_target_pairs={{0,8},{4,12},{8,16},{12,20},{16,24},{20,28},{24,0},{28,4},{1,9},{5... | collective-permute-start | bytes 786440 | tf_op jit(solution)/shard_map/ppermute | solution.py:308
  92.9 10.9 %collective-permute-start.21 = (bf16[384,256]{1,0:T(8,128)(2,1)S(1)}, bf16[384,256]{1,0:T(8,128)(2,1)S(1)}, u32[]{:S(2)}, u32[]{:S(2)}) collective-permute-start(bf16[384,256]{1,0:T(8,128)(2,1)S(1)} %copy-done.15), channel_id=1, source_target_pairs={{0,24},{4,28},{8,0},{12,4},{16,8},{20,12},{24,16},{28,20},{1,25},{... | collective-permute-start | bytes 589832 | tf_op jit(solution)/shard_map/ppermute | solution.py:308
  93.0 17.8 %collective-permute-start.14 = (bf16[64,2048]{1,0:T(8,128)(2,1)S(1)}, bf16[64,2048]{1,0:T(8,128)(2,1)S(1)}, u32[]{:S(2)}, u32[]{:S(2)}) collective-permute-start(bf16[64,2048]{1,0:T(8,128)(2,1)S(1)} %multiply_convert_fusion.refs_8_), channel_id=1, source_target_pairs={{0,16},{4,20},{8,24},{12,28},{16,0},{20,4},{24,8},{28,12},{1,17},{... | collective-permute-start | bytes 786440 | tf_op jit(solution)/shard_map/ppermute | solution.py:308
  103.9 21.1 %collective-permute-start.11 = (bf16[4,256,384]{2,1,0:T(8,128)(2,1)S(1)}, bf16[4,256,384]{2,1,0:T(8,128)(2,1)}, u32[]{:S(2)}, u32[]{:S(2)}) collective-permute-start(bf16[4,256,384]{2,1,0:T(8,128)(2,1)S(1)} %pad_maximum_fusion.1.refs_4_), channel_id=1, source_target_pairs={{0,1},{1,0},{2,3},{3,2},{4,5},{5,4},{6,7},{7,6},{8,9},{9,8},{10,11... | collective-permute-start | bytes 2359304 | tf_op jit(solution)/shard_map/ppermute | solution.py:359
  103.9 21.1 %collective-permute-start.5 = (bf16[4,256,384]{2,1,0:T(8,128)(2,1)S(1)}, bf16[4,256,384]{2,1,0:T(8,128)(2,1)}, u32[]{:S(2)}, u32[]{:S(2)}) collective-permute-start(bf16[4,256,384]{2,1,0:T(8,128)(2,1)S(1)} %pad_maximum_fusion.refs_0_), channel_id=1, source_target_pairs={{0,1},{1,0},{2,3},{3,2},{4,5},{5,4},{6,7},{7,6},{8,9},{9,8},{10,11... | collective-permute-start | bytes 2359304 | tf_op jit(solution)/shard_map/ppermute | solution.py:359
  104.5 20.5 %collective-permute-start.12 = (bf16[4,256,384]{2,1,0:T(8,128)(2,1)}, bf16[4,256,384]{2,1,0:T(8,128)(2,1)}, u32[]{:S(2)}, u32[]{:S(2)}) collective-permute-start(bf16[4,256,384]{2,1,0:T(8,128)(2,1)} %collective-permute-done.10.refs_5_), channel_id=1, source_target_pairs={{0,1},{1,0},{2,3},{3,2},{4,5},{5,4},{6,7},{7,6},{8,9},{9,8},{10,11... | collective-permute-start | bytes 2359304 | tf_op jit(solution)/shard_map/ppermute | solution.py:360
  104.6 20.4 %collective-permute-start.6 = (bf16[4,256,384]{2,1,0:T(8,128)(2,1)}, bf16[4,256,384]{2,1,0:T(8,128)(2,1)}, u32[]{:S(2)}, u32[]{:S(2)}) collective-permute-start(bf16[4,256,384]{2,1,0:T(8,128)(2,1)} %collective-permute-done.4.refs_1_), channel_id=1, source_target_pairs={{0,1},{1,0},{2,3},{3,2},{4,5},{5,4},{6,7},{7,6},{8,9},{9,8},{10,11... | collective-permute-start | bytes 2359304 | tf_op jit(solution)/shard_map/ppermute | solution.py:360
  110.8 11.7 %collective-permute-start.15 = (bf16[64,2048]{1,0:T(8,128)(2,1)S(1)}, bf16[64,2048]{1,0:T(8,128)(2,1)S(1)}, u32[]{:S(2)}, u32[]{:S(2)}) collective-permute-start(bf16[64,2048]{1,0:T(8,128)(2,1)S(1)} %multiply_convert_fusion.refs_8_), channel_id=1, source_target_pairs={{0,24},{4,28},{8,0},{12,4},{16,8},{20,12},{24,16},{28,20},{1,25},{... | collective-permute-start | bytes 786440 | tf_op jit(solution)/shard_map/ppermute | solution.py:308
  123.2 18.3 %collective-permute-start.22 = (bf16[4,384,256]{2,1,0:T(8,128)(2,1)S(1)}, bf16[4,384,256]{2,1,0:T(8,128)(2,1)}, u32[]{:S(2)}, u32[]{:S(2)}) collective-permute-start(bf16[4,384,256]{2,1,0:T(8,128)(2,1)S(1)} %pad_maximum_fusion.2.refs_0_), channel_id=1, source_target_pairs={{0,4},{4,0},{8,12},{12,8},{16,20},{20,16},{24,28},{28,24},{1,5},{5... | collective-permute-start | bytes 2359304 | tf_op jit(solution)/shard_map/ppermute | solution.py:357
  133.5 12.3 %collective-permute-start.23 = (bf16[4,384,256]{2,1,0:T(8,128)(2,1)S(1)}, bf16[4,384,256]{2,1,0:T(8,128)(2,1)S(1)}, u32[]{:S(2)}, u32[]{:S(2)}) collective-permute-start(bf16[4,384,256]{2,1,0:T(8,128)(2,1)S(1)} %pad_maximum_fusion.2.refs_0_), channel_id=1, source_target_pairs={{0,1},{1,0},{2,3},{3,2},{4,5},{5,4},{6,7},{7,6},{8,9},{9,8},{10,11... | collective-permute-start | bytes 2359304 | tf_op jit(solution)/shard_map/ppermute | solution.py:359
  152.2 14.2 %collective-permute-start.25 = (bf16[4,32,2048]{2,1,0:T(8,128)(2,1)}, bf16[4,32,2048]{2,1,0:T(8,128)(2,1)S(1)}, u32[]{:S(2)}, u32[]{:S(2)}) collective-permute-start(bf16[4,32,2048]{2,1,0:T(8,128)(2,1)} %get-tuple-element.42), channel_id=1, source_target_pairs={{0,2},{1,3},{2,0},{3,1},{4,6},{5,7},{6,4},{7,5},{8,10},{9,11},{10,... | collective-permute-start | bytes 1572872 | tf_op jit(solution)/shard_map/ppermute | solution.py:308
  167.7 13.0 %collective-permute-start.27 = (bf16[32,2048]{1,0:T(8,128)(2,1)S(1)}, bf16[32,2048]{1,0:T(8,128)(2,1)S(1)}, u32[]{:S(2)}, u32[]{:S(2)}) collective-permute-start(bf16[32,2048]{1,0:T(8,128)(2,1)S(1)} %get-tuple-element.49), channel_id=1, source_target_pairs={{0,16},{4,20},{8,24},{12,28},{16,0},{20,4},{24,8},{28,12},{1,17},{... | collective-permute-start | bytes 393224 | tf_op jit(solution)/shard_map/ppermute | solution.py:308
  (22 other events, 407.3 us)

commit v4 on v3

--- a/solution.py
+++ b/solution.py
@@ -1,3 +1,4 @@
+import functools
 import math
 
 import jax
@@ -9,7 +10,6 @@
 
 
 norm_eps = 1e-06
-highest = lax.Precision.HIGHEST
 f32 = jnp.float32
 bf16 = jnp.bfloat16
 
@@ -20,11 +20,20 @@
 
 
 def dot3(a, b):
+    rows = a.shape[0]
     a0, a1 = split2(a)
     b0, b1 = split2(b)
-    total = jnp.dot(a0, b0, preferred_element_type=f32)
-    total += jnp.dot(a0, b1, preferred_element_type=f32)
-    return total + jnp.dot(a1, b0, preferred_element_type=f32)
+    both = jnp.dot(jnp.concatenate((a0, a1), axis=0), b0, preferred_element_type=f32)
+    return both[:rows] + both[rows:] + jnp.dot(a0, b1, preferred_element_type=f32)
+
+
+def four_wide(ref, g):
+    return jnp.concatenate([ref[k, p, g] for k in range(2) for p in range(2)], axis=1)
+
+
+def signed_wide(readout, g):
+    parts = [readout[k, p, g] for k in range(2) for p in range(2)]
+    return jnp.concatenate((parts[0], -parts[1], parts[2], -parts[3]), axis=1)
 
 
 def over_rows(a, b):
@@ -59,7 +68,7 @@
     return (iota((states, rows), 0) * when).astype(f32)
 
 
-def local_kernel(scal, half_step, xt, damp, in_map, readout, yt, ends, rows_a):
+def local_kernel(scal, x_in, damp, in_map, readout, yt, xt, ends, rows_a):
     groups, rows = damp.shape[1], damp.shape[2]
     chans, states = in_map.shape[3], in_map.shape[4]
     part, quarter = states // 2, 2 * groups
@@ -68,30 +77,42 @@
     row_id, col_id = iota((rows, rows), 0), iota((rows, rows), 1)
     kept = (row_id <= col_id, row_id >= col_id)
     for k in range(2):
-        steps = damp[k] + half_step[k]
-        rows_a[k] = jnp.dot(steps, kept[k].astype(f32), precision=highest)
+        ones = kept[k].astype(f32).astype(bf16)
+        left = damp[k]
+        sums = jnp.zeros(left.shape, f32)
+        for _ in range(3):
+            part_of = left.astype(bf16)
+            sums += jnp.dot(part_of, ones, preferred_element_type=f32)
+            left = left - part_of.astype(f32)
+        rows_a[k] = sums
+    xt[...] = x_in[...].astype(f32).T.astype(bf16)
+    since = iota((1, rows), 1).astype(f32) + 1.0
+    elapsed = (since, rows + 1.0 - since)
     counts = [turns_of(states, rows, k == 1) for k in range(2)]
 
     def group(g, carry):
         held, spans = carry
         at = pl.ds(pl.multiple_of(g * chans, chans), chans)
         x = xt[at, :]
-        total = jnp.zeros((chans, rows), f32)
+        drives = over_rows(four_wide(in_map, g), x)
+        joined = []
         for k in range(2):
             cosine, sine = cos_sin(scal[0, k, g], scal[1, k, g], counts[k])
             scale = scal[2, k, g]
-            drive_r = over_rows(in_map[k, 0, g], x) * scale
-            drive_i = over_rows(in_map[k, 1, g], x) * scale
+            drive_r = drives[2 * k * states : (2 * k + 1) * states] * scale
+            drive_i = drives[(2 * k + 1) * states : (2 * k + 2) * states] * scale
             turned = jnp.concatenate(
                 (cosine * drive_r + sine * drive_i, cosine * drive_i - sine * drive_r), axis=0
             )
-            across = jnp.broadcast_to(rows_a[k, pl.ds(g, 1), :], (rows, rows))
+            summed = rows_a[k, pl.ds(g, 1), :] + (scal[0, k, g] + scal[1, k, g]) * elapsed[k]
+            rows_a[k, pl.ds(g, 1), :] = summed
+            across = jnp.broadcast_to(summed, (rows, rows))
             decay = jnp.exp(jnp.where(kept[k], across.T - across, -1e30))
             z = dot3(turned, decay)
             z_r, z_i = z[:states], z[states:]
             s_r = cosine * z_r - sine * z_i
             s_i = cosine * z_i + sine * z_r
-            total += dot3(readout[k, 0, g], s_r) - dot3(readout[k, 1, g], s_i)
+            joined += [s_r, s_i]
             last = 0 if k else rows - 1
             spans = jnp.where(slim == k * groups + g, across[:8, last : last + 1], spans)
             for p, s in enumerate((s_r, s_i)):
@@ -99,7 +120,7 @@
                 for half in range(2):
                     spot = (half * 2 + p) * quarter + k * groups + g
                     held = jnp.where(lane == spot, col[half * part : (half + 1) * part], held)
-        yt[at, :] = total
+        yt[at, :] = dot3(signed_wide(readout, g), jnp.concatenate(joined, axis=0))
         return held, spans
 
     start = (jnp.zeros(lane.shape, f32), jnp.zeros(slim.shape, f32))
@@ -109,15 +130,24 @@
         ends[peer, part:] = spans
 
 
-def carry_kernel(scal, place, xt, rows_a, lanes, every, readout, yt, skip, gain, out):
+def carry_kernel(scal, xt, rows_a, every, readout, yt, skip, gain, out, wide):
     groups, rows = rows_a.shape[1], rows_a.shape[2]
     chans, states = readout.shape[3], readout.shape[4]
     blocks = every.shape[0]
     part, quarter = states // 2, 2 * groups
-    mine = place[0]
+    mine = lax.axis_index("sp")
     number = iota((states, quarter), 0).astype(f32)
     backward = iota((states, quarter), 1) >= groups
-    coarse, fine = lanes[0:1, :], lanes[1:2, :]
+    spot = iota((1, quarter), 1)
+    coarse = jnp.zeros((1, quarter), f32)
+    fine = jnp.zeros((1, quarter), f32)
+    for k in range(2):
+        for g in range(groups):
+            coarse = jnp.where(spot == k * groups + g, scal[0, k, g], coarse)
+            fine = jnp.where(spot == k * groups + g, scal[1, k, g], fine)
+    width = skip.shape[1]
+    wide[0] = jnp.broadcast_to(skip[...], (rows, width)).T
+    wide[1] = jnp.broadcast_to(gain[...], (rows, width)).T
     far_r, far_i = cos_sin(coarse, fine, number * rows)
     near_r, near_i = cos_sin(coarse, fine, number)
 
@@ -148,18 +178,18 @@
     squares = jnp.zeros((8, rows), f32)
     for g in range(groups):
         at = pl.ds(g * chans, chans)
-        total = yt[at, :] + skip[at, :] * xt[at, :].astype(f32)
+        total = yt[at, :] + wide[0, at, :] * xt[at, :].astype(f32)
+        joined = []
         for k in range(2):
             cosine, sine = cos_sin(scal[0, k, g], scal[1, k, g], counts[k])
             l = k * groups + g
             a, b = w_r[:, l : l + 1], w_i[:, l : l + 1]
             fade = jnp.exp(-rows_a[k, g : g + 1, :])
-            s_r = (cosine * a - sine * b) * fade
-            s_i = (cosine * b + sine * a) * fade
-            total += dot3(readout[k, 0, g], s_r) - dot3(readout[k, 1, g], s_i)
+            joined += [(cosine * a - sine * b) * fade, (cosine * b + sine * a) * fade]
+        total += dot3(signed_wide(readout, g), jnp.concatenate(joined, axis=0))
         for r in range(0, chans, 8):
             squares += total[r : r + 8] * total[r : r + 8]
-        out[at, :] = (total * gain[at, :]).astype(bf16)
+        out[at, :] = (total * wide[1, at, :]).astype(bf16)
     square = jnp.sum(squares, axis=0, keepdims=True)
     top = square.astype(bf16)
     rest = square - top.astype(f32)
@@ -187,35 +217,34 @@
     coarse = jnp.floor(half_step * 2048.0) / 2048.0
     scal = jnp.stack((coarse, half_step - coarse, jnp.sqrt(-jnp.expm1(-time_step))))
     damp = jnp.swapaxes(damping, 1, 2)
-    xt = mixer_input.T
     lanes = 8 * groups
     smem = pl.BlockSpec(memory_space=pltpu.SMEM)
-    yt, ends, rows_a = pl.pallas_call(
+    yt, xt, ends, rows_a = pl.pallas_call(
         local_kernel,
         out_shape=(
             jax.ShapeDtypeStruct((width, rows), f32),
+            jax.ShapeDtypeStruct((width, rows), bf16),
             jax.ShapeDtypeStruct((lax.axis_size("sp"), states // 2 + 8, lanes), f32),
             jax.ShapeDtypeStruct(damp.shape, f32),
         ),
-        in_specs=[smem] + vmem(5),
-        out_specs=tuple(vmem(3)),
-        name="mixer_local",
-    )(scal, half_step[:, :, None], xt, damp, jnp.swapaxes(input_map, 3, 4), readout)
+        in_specs=[smem] + vmem(4),
+        out_specs=tuple(vmem(4)),
+        name="mixl",
+    )(scal, mixer_input, damp, jnp.swapaxes(input_map, 3, 4), readout)
     return scal, xt, yt, rows_a, ends
 
 
 def mixer_carried(scal, xt, yt, rows_a, every, readout, skip_gain, out_gain):
     width, rows = xt.shape
     smem = pl.BlockSpec(memory_space=pltpu.SMEM)
-    place = lax.axis_index("sp").reshape(1)
-    lanes = scal[:2].reshape(2, -1)
     return pl.pallas_call(
         carry_kernel,
         out_shape=jax.ShapeDtypeStruct((width + square_rows, rows), bf16),
-        in_specs=[smem, smem] + vmem(8),
+        in_specs=[smem] + vmem(7),
         out_specs=pl.BlockSpec(memory_space=pltpu.VMEM),
-        name="mixer_carried",
-    )(scal, place, xt, rows_a, lanes, every, readout, yt, skip_gain[:, None], out_gain[:, None])
+        scratch_shapes=[pltpu.VMEM((2, width, rows), f32)],
+        name="mixc",
+    )(scal, xt, rows_a, every, readout, yt, skip_gain[None, :], out_gain[None, :])
 
 
 def with_halo(cells, axis):
@@ -308,47 +337,57 @@
     return [lax.ppermute(pick(s), axis, ring(axis, inner, s)) for s in range(1, outer)]
 
 
-def cut_of(shapes, outer):
-    def call(*weights):
-        outs = tuple(
-            jax.ShapeDtypeStruct(shape, bf16) for shape in shapes for _ in range(outer)
-        )
-        hbm = pl.BlockSpec(memory_space=pltpu.HBM)
-        pieces = pl.pallas_call(
-            cut_all(len(weights)),
-            out_shape=outs,
-            in_specs=[hbm] * len(weights),
-            out_specs=tuple(vmem(len(outs))),
-            scratch_shapes=[pltpu.SemaphoreType.DMA((len(outs),))],
-            name="cut_weights",
-        )(*weights)
-        return [pieces[k * outer : (k + 1) * outer] for k in range(len(weights))]
-
-    return call
-
-
-def cut_all(count):
+def cut_weights(weights, outer):
+    def shape_of(weight):
+        rows, cols = weight.shape
+        return (rows // outer, cols) if rows > cols else (rows, cols // outer)
+
     def kernel(*refs):
-        ins, outs, sems = refs[:count], refs[count:-1], refs[-1]
-        outer = len(outs) // count
+        ins, outs, sems = refs[: len(weights)], refs[len(weights) : -1], refs[-1]
         mine = lax.axis_index("sp") // pair
         copies = []
-        for w in range(count):
+        for w, ref in enumerate(ins):
             for s in range(outer):
+                there = lax.rem(mine + s, outer)
                 out = outs[w * outer + s]
                 rows, cols = out.shape
-                there = lax.rem(mine + s, outer)
-                if rows == ins[w].shape[0]:
-                    part = ins[w].at[:, pl.ds(pl.multiple_of(there * cols, cols), cols)]
+                if rows == ref.shape[0]:
+                    part = ref.at[:, pl.ds(pl.multiple_of(there * cols, cols), cols)]
                 else:
-                    part = ins[w].at[pl.ds(pl.multiple_of(there * rows, rows), rows), :]
-                copy = pltpu.make_async_copy(part, out, sems.at[w * outer + s])
+                    part = ref.at[pl.ds(pl.multiple_of(there * rows, rows), rows), :]
+                copy = pltpu.make_async_copy(part, out, sems.at[w, s])
                 copy.start()
                 copies.append(copy)
         for copy in copies:
             copy.wait()
 
-    return kernel
+    outs = tuple(
+        jax.ShapeDtypeStruct(shape_of(weight), bf16) for weight in weights for _ in range(outer)
+    )
+    pieces = pl.pallas_call(
+        kernel,
+        out_shape=outs,
+        in_specs=[pl.BlockSpec(memory_space=pltpu.HBM)] * len(weights),
+        out_specs=tuple(vmem(len(outs))),
+        scratch_shapes=[pltpu.SemaphoreType.DMA((len(weights), outer))],
+        name="cutk",
+    )(*weights)
+    return [pieces[w * outer : (w + 1) * outer] for w in range(len(weights))]
+
+
+def spread_pieces(pieces):
+    outer = len(pieces)
+    own = [pieces[0]]
+    for s in range(1, outer):
+        own.append(lax.ppermute(pieces[s], "sp", ring("sp", pair, s)))
+    beside = []
+    for s in range(outer):
+        beside.append(lax.ppermute(own[s], "sp", ring("sp", pair, 0, 1)))
+    over = ring("tp", pair, 0, 1)
+    across = []
+    for piece in own + beside:
+        across.append(lax.ppermute(piece, "tp", over))
+    return own + beside + across
 
 
 def spread(pieces):
@@ -370,9 +409,16 @@
 
 
 def up_kernel(*refs):
-    stacks, (out, edges, x, last, full, sems) = refs[:8], refs[-6:]
-    rows_in = refs[8:-6]
+    stacks, (out, edges, rim, x, last, full, sems, row_sems) = refs[:8], refs[-8:]
+    rows_in = refs[8:-8]
     outer, rows, cols = stacks[0].shape
+    at, row_copies = 0, []
+    for n, ref in enumerate(rows_in):
+        size = ref.shape[0]
+        copy = pltpu.make_async_copy(ref, x.at[at : at + size, :], row_sems.at[n])
+        copy.start()
+        row_copies.append(copy)
+        at += size
     groups = []
     for kind in range(2):
         copies = []
@@ -389,9 +435,8 @@
                     copy.start()
                     copies.append(copy)
         groups.append(copies)
-    each = rows_in[0].shape[0]
-    for s, ref in enumerate(rows_in):
-        x[s * each : (s + 1) * each, :] = ref[...]
+    for copy in row_copies:
+        copy.wait()
     pieces = edges.shape[1]
     for kind, copies in enumerate(groups):
         for copy in copies:
@@ -406,48 +451,90 @@
                 last[end, p : p + 1, first : first + cols] = row[:, cols:]
                 last[end, p : p + 1, first + cols : first + 2 * cols] = row[:, :cols]
     edges[...] = last[...].astype(bf16)
-
-
-def down_kernel(up, before, after, taps, *refs):
-    stacks, outs, (full, sems) = refs[:4], refs[4:-2], refs[-2:]
-    outer, rows, cols = stacks[0].shape
+    tp = lax.axis_index("tp")
+    x_at, c_at = tp // pair, lax.rem(tp, pair)
+    inner = pieces // outer
+    for s in range(outer):
+        row = jnp.zeros((1, last.shape[2]), f32)
+        for r in range(inner):
+            sub = lax.rem(x_at + r, inner)
+            low = last[0, s * inner + r : s * inner + r + 1, :]
+            high = last[1, s * inner + r : s * inner + r + 1, :]
+            row = jnp.where((c_at == 0) & (sub == 0), low, row)
+            row = jnp.where((c_at == 1) & (sub == inner - 1), high, row)
+        last[0, s : s + 1, :] = row
+    rim[...] = last[0, :outer, :].astype(bf16)
+
+
+def load_down(held, outer, full, sems):
+    rows, cols = held[0].shape
+    y = lax.rem(lax.axis_index("sp"), pair)
     copies = []
     for core in range(2):
-        for which in range(2):
-            ref = stacks[core * 2 + which]
-            for s in range(outer):
-                first = pl.multiple_of(row_block(outer, which, s) * cols, cols)
+        for s in range(outer):
+            far = lax.rem(lax.axis_index("sp") // pair + outer - s, outer)
+            first = pl.multiple_of(far * cols, cols)
+            for which in range(2):
+                n = (core * 2 + which) * outer + s
+                into = lax.rem(y + which, pair)
                 copy = pltpu.make_async_copy(
-                    ref.at[s],
-                    full.at[pl.ds(core * rows, rows), pl.ds(first, cols)],
-                    sems.at[core * 2 + which, s],
+                    held[n],
+                    full.at[into, pl.ds(core * rows, rows), pl.ds(first, cols)],
+                    sems.at[n],
                 )
                 copy.start()
                 copies.append(copy)
+    return copies
+
+
+def down_kernel(outer, up, across, beyond, taps, taps_over, *refs):
+    held, outs, (full, sems) = refs[: 4 * outer], refs[4 * outer : -2], refs[-2:]
+    copies = load_down(held, outer, full, sems)
+    rows = held[0].shape[0]
     width = 2 * rows
-    count, pieces = up.shape[0], before.shape[0]
-    length = count // pieces
+    count, pieces = up.shape[0], across.shape[1]
+    length, inner = count // pieces, pieces // outer
+    sp, tp = lax.axis_index("sp"), lax.axis_index("tp")
+    z, y, x, c = sp // pair, lax.rem(sp, pair), tp // pair, lax.rem(tp, pair)
 
     def convolved(start):
         at = slice(start, start + width)
+        low, high = across[0, :, at].astype(f32), across[1, :, at].astype(f32)
+        rims = beyond[:, at].astype(f32)
         rows_id = iota((length, width), 0)
+        first = 3 if start else 0
+        tap = [
+            jnp.concatenate((taps[t : t + 1, :], taps_over[t : t + 1, :]), axis=1)
+            for t in range(first, first + 3)
+        ]
         done = []
         for p in range(pieces):
+            s, r = p // inner, p % inner
+            sub, block = lax.rem(x + r, inner), lax.rem(z + outer - s, outer)
+            down, over = (s + 1) % outer, (s + outer - 1) % outer
+            back, on = s * inner + (r - 1) % inner, s * inner + (r + 1) % inner
+            rim_before = jnp.where(y == 0, rims[down : down + 1], rims[s : s + 1])
+            rim_before = jnp.where((block == 0) & (y == 0), 0.0, rim_before)
+            rim_after = jnp.where(y == pair - 1, rims[over : over + 1], rims[s : s + 1])
+            rim_after = jnp.where((block == outer - 1) & (y == pair - 1), 0.0, rim_after)
+            before = jnp.where(sub == 0, rim_before, high[back : back + 1])
+            before = jnp.where(c == 0, before, high[p : p + 1])
+            after = jnp.where(sub == inner - 1, rim_after, low[on : on + 1])
+            after = jnp.where(c == 0, low[p : p + 1], after)
             cells = up[p * length : (p + 1) * length, at].astype(f32)
-            left = pltpu.roll(cells, 1, 0)
-            left = jnp.where(rows_id == 0, before[p : p + 1, at].astype(f32), left)
-            right = pltpu.roll(cells, length - 1, 0)
-            right = jnp.where(rows_id == length - 1, after[p : p + 1, at].astype(f32), right)
-            done.append(taps[0:1, at] * left + taps[1:2, at] * cells + taps[2:3, at] * right)
+            left = jnp.where(rows_id == 0, before, pltpu.roll(cells, 1, 0))
+            right = jnp.where(rows_id == length - 1, after, pltpu.roll(cells, length - 1, 0))
+            done.append(tap[0] * left + tap[1] * cells + tap[2] * right)
         return jnp.concatenate(done, axis=0)
 
     gate = convolved(width)
     hidden = (convolved(0) * (gate / (1.0 + jnp.exp(-gate)))).astype(bf16)
     for copy in copies:
         copy.wait()
-    partial = jnp.dot(hidden, full[...], preferred_element_type=f32).astype(bf16)
-    for p in range(pieces):
-        outs[p % len(outs)][p // len(outs)] = partial[p * length : (p + 1) * length]
+    for half in range(2):
+        partial = jnp.dot(hidden, full[half], preferred_element_type=f32).astype(bf16)
+        for p in range(pieces):
+            outs[half * inner + p % inner][p // inner] = partial[p * length : (p + 1) * length]
 
 
 def up_projection(rows_in, stacks, pieces):
@@ -458,66 +545,48 @@
         out_shape=(
             jax.ShapeDtypeStruct((count, 4 * cols), bf16),
             jax.ShapeDtypeStruct((2, pieces, 4 * cols), bf16),
+            jax.ShapeDtypeStruct((outer, 4 * cols), bf16),
         ),
-        in_specs=[pl.BlockSpec(memory_space=pltpu.HBM)] * 8 + vmem(len(rows_in)),
-        out_specs=tuple(vmem(2)),
+        in_specs=[pl.BlockSpec(memory_space=pltpu.HBM)] * (8 + len(rows_in)),
+        out_specs=tuple(vmem(3)),
         scratch_shapes=[
             pltpu.VMEM((count, rows_in[0].shape[1]), bf16),
             pltpu.VMEM((2, pieces, 4 * cols), f32),
             pltpu.VMEM((2, 2 * outer * rows, 2 * cols), bf16),
             pltpu.SemaphoreType.DMA((4, 2 * outer)),
+            pltpu.SemaphoreType.DMA((len(rows_in),)),
         ],
-        name="up_projection",
+        name="upk",
     )(*stacks, *rows_in)
 
 
-def down_projection(up, before, after, taps, stacks, inner):
-    outer, rows, cols = stacks[0].shape
-    return pl.pallas_call(
-        down_kernel,
-        out_shape=(
-            jax.ShapeDtypeStruct(
-                (outer, up.shape[0] // (outer * inner), 2 * outer * cols), bf16
-            ),
-        )
-        * inner,
-        in_specs=vmem(4) + [pl.BlockSpec(memory_space=pltpu.HBM)] * 4,
-        out_specs=tuple(vmem(inner)),
+def down_projection(up, across, beyond, taps, taps_over, held, inner):
+    outer = len(held) // 4
+    rows, cols = held[0].shape
+    length = up.shape[0] // (outer * inner)
+    outs = pl.pallas_call(
+        functools.partial(down_kernel, outer),
+        out_shape=(jax.ShapeDtypeStruct((outer, length, outer * cols), bf16),) * (2 * inner),
+        in_specs=vmem(5) + [pl.BlockSpec(memory_space=pltpu.HBM)] * len(held),
+        out_specs=tuple(vmem(2 * inner)),
         scratch_shapes=[
-            pltpu.VMEM((2 * rows, 2 * outer * cols), bf16),
-            pltpu.SemaphoreType.DMA((4, outer)),
+            pltpu.VMEM((2, 2 * rows, outer * cols), bf16),
+            pltpu.SemaphoreType.DMA((len(held),)),
         ],
-        name="down_projection",
-    )(up, before, after, taps, *stacks)
-
-
-def edges_of(ends, outer, inner):
-    sp, tp = lax.axis_index("sp"), lax.axis_index("tp")
-    z, y, x, c = sp // pair, lax.rem(sp, pair), tp // pair, lax.rem(tp, pair)
-    ends = ends.reshape(2, outer, inner, -1)
+        name="downk",
+    )(up, across, beyond, taps, taps_over, *held)
+    return outs[:inner], outs[inner:]
+
+
+def edges_of(ends, rim):
     across = lax.ppermute(ends, "tp", ring("tp", pair, 0, 1))
-    rim = jnp.where(c == 0, lax.rem(inner - x, inner), inner - 1 - x)
-    out_edge = lax.dynamic_index_in_dim(
-        lax.dynamic_index_in_dim(ends, c, 0, False), rim, 1, False
-    )
     sizes = (lax.axis_size("sp"), lax.axis_size("tp"))
     hops = [
         (i * sizes[1] + j, (i ^ 1) * sizes[1] + (j ^ 1))
         for i in range(sizes[0])
         for j in range(sizes[1])
     ]
-    rim_rows = lax.ppermute(out_edge, ("sp", "tp"), hops)
-    block = lax.rem(z + outer - jnp.arange(outer), outer)
-    before_rim = jnp.where(y == 0, jnp.roll(rim_rows, -1, axis=0), rim_rows)
-    before_rim = jnp.where(((block == 0) & (y == 0))[:, None], 0, before_rim)
-    after_rim = jnp.where(y == pair - 1, jnp.roll(rim_rows, 1, axis=0), rim_rows)
-    after_rim = jnp.where(((block == outer - 1) & (y == pair - 1))[:, None], 0, after_rim)
-    sub = lax.rem(x + jnp.arange(inner), inner)[None, :, None]
-    before_low = jnp.where(sub == 0, before_rim[:, None], jnp.roll(across[1], 1, axis=1))
-    after_high = jnp.where(sub == inner - 1, after_rim[:, None], jnp.roll(across[0], -1, axis=1))
-    before = jnp.where(c == 0, before_low, across[1])
-    after = jnp.where(c == 0, across[0], after_high)
-    return before.reshape(outer * inner, -1), after.reshape(outer * inner, -1)
+    return across, lax.ppermute(rim, ("sp", "tp"), hops)
 
 
 def spread_body(
@@ -541,58 +610,59 @@
     outer, inner = sp_count // pair, tp_count // pair
     tok_rows, local_width = mixer_input.shape
     own_rows = tok_rows // tp_count
+    model = residual.shape[1]
     z, tp = lax.axis_index("sp") // pair, lax.axis_index("tp")
 
-    wide = (value_weight.shape[0], value_weight.shape[1] // outer)
-    deep = (down_weight.shape[0] // outer, down_weight.shape[1])
-    (value_pieces,) = cut_of((wide,), outer)(value_weight)
-    gate_pieces, down_pieces = cut_of((wide, deep), outer)(gate_weight, down_weight)
+    value_pieces, gate_pieces, down_pieces = cut_weights(
+        (value_weight, gate_weight, down_weight), outer
+    )
     value_stacks = spread(value_pieces)
     scal, xt, yt, rows_a, ends = mixer_local(mixer_input, time_step, damping, input_map, readout)
     every = lax.all_to_all(ends, "sp", 0, 0, tiled=True)
     gate_stacks = spread(gate_pieces)
-    others = outer_send(lambda s: residual, "tp", pair)
-    taps = jnp.stack((value_taps, gate_taps), axis=1).reshape(-1, value_taps.shape[1])
+    taps = jnp.concatenate((value_taps, gate_taps))
     taps = lax.dynamic_index_in_dim(taps.reshape(taps.shape[0], outer, -1), z, 1, False)
     taps_over = lax.ppermute(taps, "tp", ring("tp", pair, 0, 1))
-    taps = jnp.stack((taps, taps_over), axis=1).reshape(value_taps.shape[0], -1)
 
     mixed = mixer_carried(scal, xt, yt, rows_a, every, readout, skip_gain, out_gain)
     mixed = lax.all_gather(mixed, "tp", axis=0)
     squares = jnp.sum(mixed[:, local_width:].astype(f32), axis=(0, 1))
     inverse = lax.rsqrt(squares / (local_width * tp_count) + norm_eps)
     channels = mixed[:, :local_width].reshape(local_width * tp_count, tok_rows)
-    mixed_rows = (
-        lax.dot_general(channels, out_weight, (((0,), (0,)), ((), ())), preferred_element_type=f32)
-        * inverse[:, None]
-    )
-    picked = [
-        lax.dynamic_slice_in_dim(
-            mixed_rows, lax.rem(tp + tp_count - pair * r, tp_count) * own_rows, own_rows, axis=0
-        )
-        for r in range(inner)
-    ]
-    order = [0] + list(range(inner - 1, 0, -1))
-    picked = jnp.concatenate([picked[r] for r in order], axis=0)
-    mine = [residual] + others
-    rows = jnp.concatenate([mine[r] for r in order], axis=0)
-    hidden_state = (rows.astype(f32) + picked).astype(bf16)
+    mixed_rows = lax.dot_general(
+        channels, out_weight, (((0,), (0,)), ((), ())), preferred_element_type=f32
+    )
+    mixed_rows = mixed_rows * inverse[:, None]
+    picked = lax.dynamic_slice_in_dim(mixed_rows, tp * own_rows, own_rows, axis=0)
+    hidden_state = (residual.astype(f32) + picked).astype(bf16)
     state_wide = hidden_state.astype(f32)
     scale_rows = lax.rsqrt(jnp.mean(state_wide * state_wide, axis=1, keepdims=True) + norm_eps)
     normed = (state_wide * scale_rows * channel_gain[None, :]).astype(bf16)
-    moved = outer_send(lambda s: normed, "sp", pair)
-    up, ends = up_projection([normed] + moved, value_stacks + gate_stacks, outer * inner)
-    down_stacks = spread(down_pieces)
-    before, after = edges_of(ends, outer, inner)
-    parts = down_projection(up, before, after, taps, down_stacks, inner)
-    total = parts[0].astype(f32)
-    for got in outer_send(lambda s: parts[s], "tp", pair):
-        total = total + got.astype(f32)
-    total = total.astype(bf16)
-    summed = total[0].astype(f32)
-    for got in outer_send(lambda s: total[outer - s], "sp", pair):
-        summed = summed + got.astype(f32)
-    return (state_wide[:own_rows] + summed).astype(bf16)
+    rows_in = []
+    for s in range(outer):
+        got = normed
+        if s:
+            got = lax.ppermute(normed, "sp", ring("sp", pair, s))
+        rows_in += [got] + outer_send(lambda s: got, "tp", pair)[::-1]
+    up, ends, rim = up_projection(rows_in, value_stacks + gate_stacks, outer * inner)
+    down_stacks = spread_pieces(down_pieces)
+    across, beyond = edges_of(ends, rim)
+    halves = down_projection(up, across, beyond, taps, taps_over, down_stacks, inner)
+    sums = []
+    for parts in halves:
+        arrived = outer_send(lambda s: parts[s], "tp", pair)
+        total = parts[0].astype(f32)
+        for got in arrived:
+            total = total + got.astype(f32)
+        total = total.astype(bf16)
+        arrived = outer_send(lambda s: total[outer - s], "sp", pair)
+        summed = total[0].astype(f32)
+        for got in arrived:
+            summed = summed + got.astype(f32)
+        sums.append(summed)
+    block = down_weight.shape[1]
+    summed = jnp.stack([part.reshape(own_rows, outer, block) for part in sums], axis=2)
+    return (state_wide + summed.reshape(own_rows, model)).astype(bf16)
 
 
 def solution(mesh):

time: 183 us -> 217 us (1.19)
  waiting for transfers between devices: 58.8 us -> 98.6 us
  starting transfers between devices: 58.3 us -> 69.8 us
  Pallas kernels: 35.7 us -> 27.9 us
  local copies, waits for them, and re-layouts: 9.43 us -> 3.46 us
  other arithmetic: 9.74 us -> 7.4 us
    ppermute x1 -> x19, waiting for transfers between devices: 0.01 us -> 62.6 us  [the longest x4 44.4 us: spread_pieces(): beside.append(lax.ppermute(own[s], 'sp', ring('sp', pair, 0, 1)))]
    ppermute x1 -> x19, starting transfers between devices: 0.07 us -> 32.8 us  [the longest x3 26 us: spread_pieces(): own.append(lax.ppermute(pieces[s], 'sp', ring('sp', pair, s)))]
    ppermute x17 -> x18, starting transfers between devices: 45.1 us -> 26.7 us  [outer_send(): lax.ppermute(pick(s), axis, ring(axis, inner, s))]
    ppermute x17 -> x18, waiting for transfers between devices: 49.5 us -> 35.9 us  [outer_send(): lax.ppermute(pick(s), axis, ring(axis, inner, s))]
    ppermute x3 -> x2, waiting for transfers between devices: 7.39 us -> 0.01 us  [spread(): beside = lax.ppermute(own, 'sp', ring('sp', pair, 0, 1))]
    pallas_call x1, Pallas kernels: 14.1 us -> 7.74 us  [mixer_local(): pl.pallas_call(local_kernel, out_shape=(jax.ShapeDtypeStruct((width, rows...]
    broadcast_in_dim x11 -> x0, local copies, waits for them, and re-layouts: 3.21 us -> none  [the longest x1 1.47 us: mixer_carried(): skip_gain[:, None]]
    pallas_call x3 -> x2, Pallas kernels: 10.1 us -> 8.49 us  [the longest x1 5.2 us: down_projection(): pl.pallas_call(functools.partial(down_kernel, outer), out_shape=(jax.Shap...]
  transfers between devices with their start and end apart: 30 -> 46, of which waited for: 9 -> 17; matrix products, arithmetic and copies ran while one was open for 8% -> 4% of each run, Pallas kernels for 9% -> 7%
where the time goes in v4:
time: 217 us
  waiting for transfers between devices  98.6 us (45%)
  starting transfers between devices  69.8 us (32%)
  Pallas kernels  27.9 us (13%)
  other arithmetic  7.4 us (3%)
  blocking collectives  6.03 us (3%)
  local copies, waits for them, and re-layouts  3.46 us (2%)
  matrix products  2.92 us (1%)
    ppermute x4, waiting for transfers between devices, spread_pieces(): beside.append(lax.ppermute(own[s], 'sp', ring('sp', pair, 0, 1)))  44.4 us
    ppermute x18, waiting for transfers between devices, outer_send(): lax.ppermute(pick(s), axis, ring(axis, inner, s))  35.9 us
    ppermute x18, starting transfers between devices, outer_send(): lax.ppermute(pick(s), axis, ring(axis, inner, s))  26.7 us
    ppermute x3, starting transfers between devices, spread_pieces(): own.append(lax.ppermute(pieces[s], 'sp', ring('sp', pair, s)))  26 us
    ppermute x3, waiting for transfers between devices, spread_body(): got = lax.ppermute(normed, 'sp', ring('sp', pair, s))  15.4 us
    pallas_call x1, Pallas kernels, mixer_local(): pl.pallas_call(local_kernel, out_shape=(jax.ShapeDtypeStruct((width, rows...  7.74 us
    all_to_all x1, starting transfers between devices, spread_body(): every = lax.all_to_all(ends, 'sp', 0, 0, tiled=True)  7.31 us
    pallas_call x1, Pallas kernels, up_projection(): pl.pallas_call(up_kernel, out_shape=(jax.ShapeDtypeStruct((count, 4 * col...  7.09 us
  transfers between devices with their start and end apart: 46, of which 17 were waited for; matrix products, arithmetic and copies ran while one was open for 4% of the time, Pallas kernels for 7%

profile of v4, /device:TPU:0, one launch (start us, length us, event | category | flops | bytes accessed | tf_op | source)
XLA Modules:
  0.0 216.6 jit_solution(12302508053563814466)
XLA Ops:
  1.3 7.7 %mixl.1 = (f32[256,128]{1,0:T(8,128)}, bf16[256,128]{1,0:T(8,128)(2,1)}, f32[8,40,128]{2,1,0:T(8,128)}, f32[2,16,128]{2,1,0:T(8,128)}) custom-call(f32[3,2,16]{2,1,0:T(2,128)} %pad_maximum_fusion.4.scal, bf16[128,256]{1,0:T(8,128)(2,1)} %x_in.1, f32[2,16,128]{2,1,0:T(8,128)} %bitcast.60, bf16[2,2,16,16,64]{4,3,2,1,0:T(8,128)(2,1)} %bitcast.50, ...), custom_call_target="tpu_custom_call" | custom-call | tf_op jit(solution)/shard_map/mixl/pallas_call | solution.py:222
  9.0 7.3 %all-to-all-start = ((f32[8,40,128]{2,1,0:T(8,128)}), f32[8,40,128]{2,1,0:T(8,128)S(1)}, u32[]{:S(2)}, u32[]{:S(2)}) async-start(f32[8,40,128]{2,1,0:T(8,128)} %get-tuple-element.30), calls=%async_computation | async-start | bytes 327680 | tf_op jit(solution)/shard_map/all_to_all | solution.py:621
  16.3 3.3 %cutk.1 = (bf16[256,384]{1,0:T(8,128)(2,1)}, bf16[256,384]{1,0:T(8,128)(2,1)}, bf16[256,384]{1,0:T(8,128)(2,1)}, bf16[256,384]{1,0:T(8,128)(2,1)}, bf16[256,384]...) custom-call(bf16[256,1536]{1,0:T(8,128)(2,1)} %refs_0_.1, ...), custom_call_target="tpu_custom_call" | custom-call | tf_op jit(solution)/shard_map/cutk/pallas_call | solution.py:367
  32.4 5.7 %collective-permute-done.7 = bf16[256,384]{1,0:T(8,128)(2,1)S(1)} collective-permute-done((bf16[256,384]{1,0:T(8,128)(2,1)}, bf16[256,384]{1,0:T(8,128)(2,1)S(1)}, u32[]{:S(2)}, u32[]{:S(2)}) %collective-permute-start.7) | collective-permute-done | bytes 196640 | tf_op jit(solution)/shard_map/ppermute | solution.py:337
  40.2 9.6 %collective-permute-start.22 = (bf16[384,256]{1,0:T(8,128)(2,1)}, bf16[384,256]{1,0:T(8,128)(2,1)}, u32[]{:S(2)}, u32[]{:S(2)}) collective-permute-start(bf16[384,256]{1,0:T(8,128)(2,1)} %get-tuple-element.44), channel_id=1, source_target_pairs={{0,8},{4,12},{8,16},{12,20},{16,24},{20,28},{24,0},{28,4},{1,9},{5... | collective-permute-start | bytes 589832 | tf_op jit(solution)/shard_map/ppermute | solution.py:382
  50.9 4.9 %collective-permute-start.23 = (bf16[384,256]{1,0:T(8,128)(2,1)}, bf16[384,256]{1,0:T(8,128)(2,1)}, u32[]{:S(2)}, u32[]{:S(2)}) collective-permute-start(bf16[384,256]{1,0:T(8,128)(2,1)} %get-tuple-element.45), channel_id=1, source_target_pairs={{0,16},{4,20},{8,24},{12,28},{16,0},{20,4},{24,8},{28,12},{1,17},{... | collective-permute-start | bytes 589832 | tf_op jit(solution)/shard_map/ppermute | solution.py:382
  55.9 11.4 %collective-permute-start.24 = (bf16[384,256]{1,0:T(8,128)(2,1)}, bf16[384,256]{1,0:T(8,128)(2,1)}, u32[]{:S(2)}, u32[]{:S(2)}) collective-permute-start(bf16[384,256]{1,0:T(8,128)(2,1)} %get-tuple-element.46), channel_id=1, source_target_pairs={{0,24},{4,28},{8,0},{12,4},{16,8},{20,12},{24,16},{28,20},{1,25},{... | collective-permute-start | bytes 589832 | tf_op jit(solution)/shard_map/ppermute | solution.py:382
  70.6 4.5 %mixc.1 = bf16[272,128]{1,0:T(8,128)(2,1)} custom-call(f32[3,2,16]{2,1,0:T(2,128)} %pad_maximum_fusion.4.scal, bf16[256,128]{1,0:T(8,128)(2,1)} %get-tuple-element.28.xt, f32[2,16,128]{2,1,0:T(8,128)} %get-tuple-element.29.rows_a, f32[8,40,128]{2,1,0:T(8,128)} %copy-done.8, f32[2,2,16,16,64]{4,3,2,1,0:T(8,128)} %readout.3, f32[256,128]{1,0:T(8,128)} %get-tuple-element.31.yt, ...), custom_call_target="tpu_custom_call" | custom-call | tf_op jit(solution)/shard_map/mixc/pallas_call | solution.py:240
  75.1 6.0 %all-gather = bf16[1088,128]{1,0:T(8,128)(2,1)S(1)} all-gather(bf16[272,128]{1,0:T(8,128)(2,1)} %mixc.1), channel_id=2, replica_groups=mesh['sp'=8,'tp'=4] {'tp'}, dimensions={0}, use_global_device_ids=true | all-gather | bytes 348160 | tf_op jit(solution)/shard_map/all_gather | solution.py:628
  81.3 2.9 %fusion.12 = f32[128,2048]{1,0:T(8,128)S(1)} fusion(bf16[1024,128]{1,0:T(8,128)(2,1)S(1)} %bitcast.49, bf16[1024,2048]{1,0:T(8,128)(2,1)} %param.22), kind=kOutput, calls=%fused_computation.39 | convolution fusion | flops 536870912 | bytes 5505024 | tf_op jit(solution)/shard_map/dot_general | solution.py:632
  89.1 37.4 %collective-permute-done.26.refs_5_ = bf16[384,256]{1,0:T(8,128)(2,1)} collective-permute-done((bf16[384,256]{1,0:T(8,128)(2,1)}, bf16[384,256]{1,0:T(8,128)(2,1)}, u32[]{:S(2)}, u32[]{:S(2)}) %collective-permute-start.26) | collective-permute-done | bytes 196640 | tf_op jit(solution)/shard_map/ppermute | solution.py:385
  127.1 3.7 %collective-permute-done.27.refs_6_ = bf16[384,256]{1,0:T(8,128)(2,1)} collective-permute-done((bf16[384,256]{1,0:T(8,128)(2,1)}, bf16[384,256]{1,0:T(8,128)(2,1)}, u32[]{:S(2)}, u32[]{:S(2)}) %collective-permute-start.27) | collective-permute-done | bytes 196640 | tf_op jit(solution)/shard_map/ppermute | solution.py:385
  130.8 3.3 %collective-permute-done.28.refs_7_ = bf16[384,256]{1,0:T(8,128)(2,1)} collective-permute-done((bf16[384,256]{1,0:T(8,128)(2,1)}, bf16[384,256]{1,0:T(8,128)(2,1)}, u32[]{:S(2)}, u32[]{:S(2)}) %collective-permute-start.28) | collective-permute-done | bytes 196640 | tf_op jit(solution)/shard_map/ppermute | solution.py:385
  134.8 7.3 %collective-permute-done.13.refs_10_ = bf16[32,2048]{1,0:T(8,128)(2,1)S(1)} collective-permute-done((bf16[32,2048]{1,0:T(8,128)(2,1)S(1)}, bf16[32,2048]{1,0:T(8,128)(2,1)S(1)}, u32[]{:S(2)}, u32[]{:S(2)}) %collective-permute-start.13) | collective-permute-done | bytes 131104 | tf_op jit(solution)/shard_map/ppermute | solution.py:645
  142.7 3.1 %collective-permute-done.15.refs_12_ = bf16[32,2048]{1,0:T(8,128)(2,1)S(1)} collective-permute-done((bf16[32,2048]{1,0:T(8,128)(2,1)S(1)}, bf16[32,2048]{1,0:T(8,128)(2,1)S(1)}, u32[]{:S(2)}, u32[]{:S(2)}) %collective-permute-start.15) | collective-permute-done | bytes 131104 | tf_op jit(solution)/shard_map/ppermute | solution.py:645
  145.8 5.0 %collective-permute-done.17.refs_14_ = bf16[32,2048]{1,0:T(8,128)(2,1)S(1)} collective-permute-done((bf16[32,2048]{1,0:T(8,128)(2,1)S(1)}, bf16[32,2048]{1,0:T(8,128)(2,1)S(1)}, u32[]{:S(2)}, u32[]{:S(2)}) %collective-permute-start.17) | collective-permute-done | bytes 131104 | tf_op jit(solution)/shard_map/ppermute | solution.py:645
  152.3 4.4 %collective-permute-done.12.refs_9_ = bf16[32,2048]{1,0:T(8,128)(2,1)S(1)} collective-permute-done((bf16[32,2048]{1,0:T(8,128)(2,1)S(1)}, bf16[32,2048]{1,0:T(8,128)(2,1)S(1)}, u32[]{:S(2)}, u32[]{:S(2)}) %collective-permute-start.12) | collective-permute-done | bytes 131104 | tf_op jit(solution)/shard_map/ppermute | solution.py:337
  158.2 4.2 %collective-permute-done.14.refs_11_ = bf16[32,2048]{1,0:T(8,128)(2,1)S(1)} collective-permute-done((bf16[32,2048]{1,0:T(8,128)(2,1)S(1)}, bf16[32,2048]{1,0:T(8,128)(2,1)S(1)}, u32[]{:S(2)}, u32[]{:S(2)}) %collective-permute-start.14) | collective-permute-done | bytes 131104 | tf_op jit(solution)/shard_map/ppermute | solution.py:337
  163.9 3.5 %collective-permute-done.16.refs_13_ = bf16[32,2048]{1,0:T(8,128)(2,1)S(1)} collective-permute-done((bf16[32,2048]{1,0:T(8,128)(2,1)S(1)}, bf16[32,2048]{1,0:T(8,128)(2,1)S(1)}, u32[]{:S(2)}, u32[]{:S(2)}) %collective-permute-start.16) | collective-permute-done | bytes 131104 | tf_op jit(solution)/shard_map/ppermute | solution.py:337
  168.9 3.5 %collective-permute-done.18.refs_15_ = bf16[32,2048]{1,0:T(8,128)(2,1)S(1)} collective-permute-done((bf16[32,2048]{1,0:T(8,128)(2,1)S(1)}, bf16[32,2048]{1,0:T(8,128)(2,1)S(1)}, u32[]{:S(2)}, u32[]{:S(2)}) %collective-permute-start.18) | collective-permute-done | bytes 131104 | tf_op jit(solution)/shard_map/ppermute | solution.py:337
  175.2 7.1 %upk.1 = (bf16[256,1536]{1,0:T(8,128)(2,1)}, bf16[2,8,1536]{2,1,0:T(8,128)(2,1)}, bf16[4,1536]{1,0:T(4,128)(2,1)}) custom-call(bf16[4,256,384]{2,1,0:T(8,128)(2,1)} %copy-done.1, bf16[4,256,384]{2,1,0:T(8,128)(2,1)} %copy-done.3, bf16[4,256,384]{2,1,0:T(8,128)(2,1)} %copy-done.5, bf16[4,256,384]{2,1,0:T(8,128)(2,1)} %copy-done.7, ...), custom_call_target="tpu_custom_call" | custom-call | tf_op jit(solution)/shard_map/upk/pallas_call | solution.py:543
  183.1 2.9 %collective-permute-done.20.beyond = bf16[4,1536]{1,0:T(4,128)(2,1)S(1)} collective-permute-done((bf16[4,1536]{1,0:T(4,128)(2,1)}, bf16[4,1536]{1,0:T(4,128)(2,1)S(1)}, u32[]{:S(2)}, u32[]{:S(2)}) %collective-permute-start.20) | collective-permute-done | bytes 12320 | tf_op jit(solution)/shard_map/ppermute | solution.py:589
  186.6 5.2 %downk.1 = (bf16[4,32,1024]{2,1,0:T(8,128)(2,1)}, bf16[4,32,1024]{2,1,0:T(8,128)(2,1)}, bf16[4,32,1024]{2,1,0:T(8,128)(2,1)}, bf16[4,32,1024]{2,1,0:T(8,128)(2,1)}) custom-call(bf16[256,1536]{1,0:T(8,128)(2,1)} %get-tuple-element.40.up, bf16[2,8,1536]{2,1,0:T(8,128)(2,1)} %copy-done.26, bf16[4,1536]{1,0:T(4,128)(2,1)} %copy-done.29, f32[6,384]{1,0:T(8,128)} %copy-done.27, ...), custom_call_target="tpu_custom_call" | custom-call | tf_op jit(solution)/shard_map/downk/pallas_call | solution.py:567
  193.9 7.4 %collective-permute-done.37 = bf16[4,32,1024]{2,1,0:T(8,128)(2,1)S(1)} collective-permute-done((bf16[4,32,1024]{2,1,0:T(8,128)(2,1)}, bf16[4,32,1024]{2,1,0:T(8,128)(2,1)S(1)}, u32[]{:S(2)}, u32[]{:S(2)}) %collective-permute-start.37) | collective-permute-done | bytes 262176 | tf_op jit(solution)/shard_map/ppermute | solution.py:337
  (162 shorter events, 54.7 us)
Async XLA Ops:
  9.0 60.9 %all-to-all-start = ((f32[8,40,128]{2,1,0:T(8,128)}), f32[8,40,128]{2,1,0:T(8,128)S(1)}, u32[]{:S(2)}, u32[]{:S(2)}) async-start(f32[8,40,128]{2,1,0:T(8,128)} %get-tuple-element.30), calls=%async_computation | async-start | bytes 327680 | tf_op jit(solution)/shard_map/all_to_all | solution.py:621
  21.7 16.4 %collective-permute-start.7 = (bf16[256,384]{1,0:T(8,128)(2,1)}, bf16[256,384]{1,0:T(8,128)(2,1)S(1)}, u32[]{:S(2)}, u32[]{:S(2)}) collective-permute-start(bf16[256,384]{1,0:T(8,128)(2,1)} %get-tuple-element.38), channel_id=1, source_target_pairs={{0,16},{4,20},{8,24},{12,28},{16,0},{20,4},{24,8},{28,12},{1,17},{... | collective-permute-start | bytes 589832 | tf_op jit(solution)/shard_map/ppermute | solution.py:337
  24.1 16.2 %collective-permute-start.8 = (bf16[256,384]{1,0:T(8,128)(2,1)}, bf16[256,384]{1,0:T(8,128)(2,1)S(1)}, u32[]{:S(2)}, u32[]{:S(2)}) collective-permute-start(bf16[256,384]{1,0:T(8,128)(2,1)} %get-tuple-element.39), channel_id=1, source_target_pairs={{0,24},{4,28},{8,0},{12,4},{16,8},{20,12},{24,16},{28,20},{1,25},{... | collective-permute-start | bytes 589832 | tf_op jit(solution)/shard_map/ppermute | solution.py:337
  25.5 25.4 %collective-permute-start = (bf16[256,384]{1,0:T(8,128)(2,1)}, bf16[256,384]{1,0:T(8,128)(2,1)S(1)}, u32[]{:S(2)}, u32[]{:S(2)}) collective-permute-start(bf16[256,384]{1,0:T(8,128)(2,1)} %get-tuple-element.33), channel_id=1, source_target_pairs={{0,8},{4,12},{8,16},{12,20},{16,24},{20,28},{24,0},{28,4},{1,9},{5... | collective-permute-start | bytes 589832 | tf_op jit(solution)/shard_map/ppermute | solution.py:337
  26.1 29.8 %collective-permute-start.1 = (bf16[256,384]{1,0:T(8,128)(2,1)}, bf16[256,384]{1,0:T(8,128)(2,1)S(1)}, u32[]{:S(2)}, u32[]{:S(2)}) collective-permute-start(bf16[256,384]{1,0:T(8,128)(2,1)} %get-tuple-element.34), channel_id=1, source_target_pairs={{0,16},{4,20},{8,24},{12,28},{16,0},{20,4},{24,8},{28,12},{1,17},{... | collective-permute-start | bytes 589832 | tf_op jit(solution)/shard_map/ppermute | solution.py:337
  29.6 37.7 %collective-permute-start.2 = (bf16[256,384]{1,0:T(8,128)(2,1)}, bf16[256,384]{1,0:T(8,128)(2,1)S(1)}, u32[]{:S(2)}, u32[]{:S(2)}) collective-permute-start(bf16[256,384]{1,0:T(8,128)(2,1)} %get-tuple-element.35), channel_id=1, source_target_pairs={{0,24},{4,28},{8,0},{12,4},{16,8},{20,12},{24,16},{28,20},{1,25},{... | collective-permute-start | bytes 589832 | tf_op jit(solution)/shard_map/ppermute | solution.py:337
  38.1 46.4 %collective-permute-start.21 = (f32[6,384]{1,0:T(8,128)S(1)}, f32[6,384]{1,0:T(8,128)S(1)}, u32[]{:S(2)}, u32[]{:S(2)}) collective-permute-start(f32[6,384]{1,0:T(8,128)S(1)} %dynamic-slice_bitcast_fusion.taps), channel_id=1, source_target_pairs={{0,1},{1,0},{2,3},{3,2},{4,5},{5,4},{6,7},{7,6},{8,9},{9,8},{10,11... | collective-permute-start | bytes 27656 | tf_op jit(solution)/shard_map/ppermute | solution.py:625
  40.2 44.7 %collective-permute-start.22 = (bf16[384,256]{1,0:T(8,128)(2,1)}, bf16[384,256]{1,0:T(8,128)(2,1)}, u32[]{:S(2)}, u32[]{:S(2)}) collective-permute-start(bf16[384,256]{1,0:T(8,128)(2,1)} %get-tuple-element.44), channel_id=1, source_target_pairs={{0,8},{4,12},{8,16},{12,20},{16,24},{20,28},{24,0},{28,4},{1,9},{5... | collective-permute-start | bytes 589832 | tf_op jit(solution)/shard_map/ppermute | solution.py:382
  50.9 34.5 %collective-permute-start.23 = (bf16[384,256]{1,0:T(8,128)(2,1)}, bf16[384,256]{1,0:T(8,128)(2,1)}, u32[]{:S(2)}, u32[]{:S(2)}) collective-permute-start(bf16[384,256]{1,0:T(8,128)(2,1)} %get-tuple-element.45), channel_id=1, source_target_pairs={{0,16},{4,20},{8,24},{12,28},{16,0},{20,4},{24,8},{28,12},{1,17},{... | collective-permute-start | bytes 589832 | tf_op jit(solution)/shard_map/ppermute | solution.py:382
  55.9 31.1 %collective-permute-start.24 = (bf16[384,256]{1,0:T(8,128)(2,1)}, bf16[384,256]{1,0:T(8,128)(2,1)}, u32[]{:S(2)}, u32[]{:S(2)}) collective-permute-start(bf16[384,256]{1,0:T(8,128)(2,1)} %get-tuple-element.46), channel_id=1, source_target_pairs={{0,24},{4,28},{8,0},{12,4},{16,8},{20,12},{24,16},{28,20},{1,25},{... | collective-permute-start | bytes 589832 | tf_op jit(solution)/shard_map/ppermute | solution.py:382
  67.3 20.2 %collective-permute-start.25 = (bf16[384,256]{1,0:T(8,128)(2,1)}, bf16[384,256]{1,0:T(8,128)(2,1)}, u32[]{:S(2)}, u32[]{:S(2)}) collective-permute-start(bf16[384,256]{1,0:T(8,128)(2,1)} %get-tuple-element.43.refs_0_), channel_id=1, source_target_pairs={{0,4},{4,0},{8,12},{12,8},{16,20},{20,16},{24,28},{28,24},{1,5},{5... | collective-permute-start | bytes 589832 | tf_op jit(solution)/shard_map/ppermute | solution.py:385
  84.9 57.2 %collective-permute-start.9 = (bf16[4,256,384]{2,1,0:T(8,128)(2,1)S(1)}, bf16[4,256,384]{2,1,0:T(8,128)(2,1)S(1)}, u32[]{:S(2)}, u32[]{:S(2)}) collective-permute-start(bf16[4,256,384]{2,1,0:T(8,128)(2,1)S(1)} %pad_maximum_fusion.1.refs_4_), channel_id=1, source_target_pairs={{0,4},{4,0},{8,12},{12,8},{16,20},{20,16},{24,28},{28,24},{1,5},{5... | collective-permute-start | bytes 2359304 | tf_op jit(solution)/shard_map/ppermute | solution.py:396
  85.5 57.2 %collective-permute-start.3 = (bf16[4,256,384]{2,1,0:T(8,128)(2,1)S(1)}, bf16[4,256,384]{2,1,0:T(8,128)(2,1)S(1)}, u32[]{:S(2)}, u32[]{:S(2)}) collective-permute-start(bf16[4,256,384]{2,1,0:T(8,128)(2,1)S(1)} %pad_maximum_fusion.refs_0_), channel_id=1, source_target_pairs={{0,4},{4,0},{8,12},{12,8},{16,20},{20,16},{24,28},{28,24},{1,5},{5... | collective-permute-start | bytes 2359304 | tf_op jit(solution)/shard_map/ppermute | solution.py:396
  87.0 39.6 %collective-permute-start.26 = (bf16[384,256]{1,0:T(8,128)(2,1)}, bf16[384,256]{1,0:T(8,128)(2,1)}, u32[]{:S(2)}, u32[]{:S(2)}) collective-permute-start(bf16[384,256]{1,0:T(8,128)(2,1)} %collective-permute-done.22.refs_1_), channel_id=1, source_target_pairs={{0,4},{4,0},{8,12},{12,8},{16,20},{20,16},{24,28},{28,24},{1,5},{5... | collective-permute-start | bytes 589832 | tf_op jit(solution)/shard_map/ppermute | solution.py:385
  87.5 43.2 %collective-permute-start.27 = (bf16[384,256]{1,0:T(8,128)(2,1)}, bf16[384,256]{1,0:T(8,128)(2,1)}, u32[]{:S(2)}, u32[]{:S(2)}) collective-permute-start(bf16[384,256]{1,0:T(8,128)(2,1)} %collective-permute-done.23.refs_2_), channel_id=1, source_target_pairs={{0,4},{4,0},{8,12},{12,8},{16,20},{20,16},{24,28},{28,24},{1,5},{5... | collective-permute-start | bytes 589832 | tf_op jit(solution)/shard_map/ppermute | solution.py:385
  89.0 45.7 %collective-permute-start.30 = (bf16[384,256]{1,0:T(8,128)(2,1)}, bf16[384,256]{1,0:T(8,128)(2,1)S(1)}, u32[]{:S(2)}, u32[]{:S(2)}) collective-permute-start(bf16[384,256]{1,0:T(8,128)(2,1)} %collective-permute-done.22.refs_1_), channel_id=1, source_target_pairs={{0,1},{1,0},{2,3},{3,2},{4,5},{5,4},{6,7},{7,6},{8,9},{9,8},{10,11... | collective-permute-start | bytes 589832 | tf_op jit(solution)/shard_map/ppermute | solution.py:389
  134.1 11.7 %collective-permute-start.15 = (bf16[32,2048]{1,0:T(8,128)(2,1)S(1)}, bf16[32,2048]{1,0:T(8,128)(2,1)S(1)}, u32[]{:S(2)}, u32[]{:S(2)}) collective-permute-start(bf16[32,2048]{1,0:T(8,128)(2,1)S(1)} %fusion.2.refs_8_), channel_id=1, source_target_pairs={{0,16},{4,20},{8,24},{12,28},{16,0},{20,4},{24,8},{28,12},{1,17},{... | collective-permute-start | bytes 393224 | tf_op jit(solution)/shard_map/ppermute | solution.py:645
  134.7 37.6 %collective-permute-start.10 = (bf16[4,256,384]{2,1,0:T(8,128)(2,1)S(1)}, bf16[4,256,384]{2,1,0:T(8,128)(2,1)S(1)}, u32[]{:S(2)}, u32[]{:S(2)}) collective-permute-start(bf16[4,256,384]{2,1,0:T(8,128)(2,1)S(1)} %pad_maximum_fusion.1.refs_4_), channel_id=1, source_target_pairs={{0,1},{1,0},{2,3},{3,2},{4,5},{5,4},{6,7},{7,6},{8,9},{9,8},{10,11... | collective-permute-start | bytes 2359304 | tf_op jit(solution)/shard_map/ppermute | solution.py:398
  142.1 30.7 %collective-permute-start.4 = (bf16[4,256,384]{2,1,0:T(8,128)(2,1)S(1)}, bf16[4,256,384]{2,1,0:T(8,128)(2,1)S(1)}, u32[]{:S(2)}, u32[]{:S(2)}) collective-permute-start(bf16[4,256,384]{2,1,0:T(8,128)(2,1)S(1)} %pad_maximum_fusion.refs_0_), channel_id=1, source_target_pairs={{0,1},{1,0},{2,3},{3,2},{4,5},{5,4},{6,7},{7,6},{8,9},{9,8},{10,11... | collective-permute-start | bytes 2359304 | tf_op jit(solution)/shard_map/ppermute | solution.py:398
  142.1 30.8 %collective-permute-start.11 = (bf16[4,256,384]{2,1,0:T(8,128)(2,1)S(1)}, bf16[4,256,384]{2,1,0:T(8,128)(2,1)S(1)}, u32[]{:S(2)}, u32[]{:S(2)}) collective-permute-start(bf16[4,256,384]{2,1,0:T(8,128)(2,1)S(1)} %collective-permute-done.9.refs_5_), channel_id=1, source_target_pairs={{0,1},{1,0},{2,3},{3,2},{4,5},{5,4},{6,7},{7,6},{8,9},{9,8},{10,11... | collective-permute-start | bytes 2359304 | tf_op jit(solution)/shard_map/ppermute | solution.py:399
  142.7 30.7 %collective-permute-start.5 = (bf16[4,256,384]{2,1,0:T(8,128)(2,1)S(1)}, bf16[4,256,384]{2,1,0:T(8,128)(2,1)S(1)}, u32[]{:S(2)}, u32[]{:S(2)}) collective-permute-start(bf16[4,256,384]{2,1,0:T(8,128)(2,1)S(1)} %collective-permute-done.3.refs_1_), channel_id=1, source_target_pairs={{0,1},{1,0},{2,3},{3,2},{4,5},{5,4},{6,7},{7,6},{8,9},{9,8},{10,11... | collective-permute-start | bytes 2359304 | tf_op jit(solution)/shard_map/ppermute | solution.py:399
  172.4 10.3 %collective-permute-start.32 = (bf16[384,256]{1,0:T(8,128)(2,1)}, bf16[384,256]{1,0:T(8,128)(2,1)S(1)}, u32[]{:S(2)}, u32[]{:S(2)}) collective-permute-start(bf16[384,256]{1,0:T(8,128)(2,1)} %collective-permute-done.24.refs_3_), channel_id=1, source_target_pairs={{0,1},{1,0},{2,3},{3,2},{4,5},{5,4},{6,7},{7,6},{8,9},{9,8},{10,11... | collective-permute-start | bytes 589832 | tf_op jit(solution)/shard_map/ppermute | solution.py:389
  172.9 10.2 %collective-permute-start.34 = (bf16[384,256]{1,0:T(8,128)(2,1)}, bf16[384,256]{1,0:T(8,128)(2,1)S(1)}, u32[]{:S(2)}, u32[]{:S(2)}) collective-permute-start(bf16[384,256]{1,0:T(8,128)(2,1)} %collective-permute-done.26.refs_5_), channel_id=1, source_target_pairs={{0,1},{1,0},{2,3},{3,2},{4,5},{5,4},{6,7},{7,6},{8,9},{9,8},{10,11... | collective-permute-start | bytes 589832 | tf_op jit(solution)/shard_map/ppermute | solution.py:389
  193.3 12.8 %collective-permute-start.41 = (bf16[4,32,1024]{2,1,0:T(8,128)(2,1)}, bf16[4,32,1024]{2,1,0:T(8,128)(2,1)S(1)}, u32[]{:S(2)}, u32[]{:S(2)}) collective-permute-start(bf16[4,32,1024]{2,1,0:T(8,128)(2,1)} %get-tuple-element.50), channel_id=1, source_target_pairs={{0,2},{1,3},{2,0},{3,1},{4,6},{5,7},{6,4},{7,5},{8,10},{9,11},{10,... | collective-permute-start | bytes 786440 | tf_op jit(solution)/shard_map/ppermute | solution.py:337
  (53 other events, 989.0 us)

commit v5 on v4

--- a/solution.py
+++ b/solution.py
@@ -626,15 +626,14 @@
 
     mixed = mixer_carried(scal, xt, yt, rows_a, every, readout, skip_gain, out_gain)
     mixed = lax.all_gather(mixed, "tp", axis=0)
+    mixed = lax.dynamic_slice_in_dim(mixed, tp * own_rows, own_rows, axis=2)
     squares = jnp.sum(mixed[:, local_width:].astype(f32), axis=(0, 1))
     inverse = lax.rsqrt(squares / (local_width * tp_count) + norm_eps)
-    channels = mixed[:, :local_width].reshape(local_width * tp_count, tok_rows)
+    channels = mixed[:, :local_width].reshape(local_width * tp_count, own_rows)
     mixed_rows = lax.dot_general(
         channels, out_weight, (((0,), (0,)), ((), ())), preferred_element_type=f32
     )
-    mixed_rows = mixed_rows * inverse[:, None]
-    picked = lax.dynamic_slice_in_dim(mixed_rows, tp * own_rows, own_rows, axis=0)
-    hidden_state = (residual.astype(f32) + picked).astype(bf16)
+    hidden_state = (residual.astype(f32) + mixed_rows * inverse[:, None]).astype(bf16)
     state_wide = hidden_state.astype(f32)
     scale_rows = lax.rsqrt(jnp.mean(state_wide * state_wide, axis=1, keepdims=True) + norm_eps)
     normed = (state_wide * scale_rows * channel_gain[None, :]).astype(bf16)

time: 217 us -> 218 us (level)
  no operation moved by 1% of the time
where the time goes in v5:
time: 218 us; the launch traced here: 217 us
  waiting for transfers between devices  99 us (45%)
  starting transfers between devices  69.8 us (32%)
  Pallas kernels  27.9 us (13%)
  other arithmetic  7.22 us (3%)
  blocking collectives  6.04 us (3%)
  local copies, waits for them, and re-layouts  3.72 us (2%)
  matrix products  3.16 us (1%)
    ppermute x4, waiting for transfers between devices, spread_pieces(): beside.append(lax.ppermute(own[s], 'sp', ring('sp', pair, 0, 1)))  44.6 us
    ppermute x18, waiting for transfers between devices, outer_send(): lax.ppermute(pick(s), axis, ring(axis, inner, s))  35.9 us
    ppermute x18, starting transfers between devices, outer_send(): lax.ppermute(pick(s), axis, ring(axis, inner, s))  26.7 us
    ppermute x3, starting transfers between devices, spread_pieces(): own.append(lax.ppermute(pieces[s], 'sp', ring('sp', pair, s)))  26 us
    ppermute x3, waiting for transfers between devices, spread_body(): got = lax.ppermute(normed, 'sp', ring('sp', pair, s))  15.6 us
    pallas_call x1, Pallas kernels, mixer_local(): pl.pallas_call(local_kernel, out_shape=(jax.ShapeDtypeStruct((width, rows...  7.77 us
    all_to_all x1, starting transfers between devices, spread_body(): every = lax.all_to_all(ends, 'sp', 0, 0, tiled=True)  7.31 us
    pallas_call x1, Pallas kernels, up_projection(): pl.pallas_call(up_kernel, out_shape=(jax.ShapeDtypeStruct((count, 4 * col...  7.06 us
  transfers between devices with their start and end apart: 46, of which 17 were waited for; matrix products, arithmetic and copies ran while one was open for 4% of the time, Pallas kernels for 7%

profile of v5, /device:TPU:0, one launch (start us, length us, event | category | flops | bytes accessed | tf_op | source)
XLA Modules:
  0.0 217.2 jit_solution(468237863221880815)
XLA Ops:
  1.3 7.8 %mixl.1 = (f32[256,128]{1,0:T(8,128)}, bf16[256,128]{1,0:T(8,128)(2,1)}, f32[8,40,128]{2,1,0:T(8,128)}, f32[2,16,128]{2,1,0:T(8,128)}) custom-call(f32[3,2,16]{2,1,0:T(2,128)} %pad_maximum_fusion.4.scal, bf16[128,256]{1,0:T(8,128)(2,1)} %x_in.1, f32[2,16,128]{2,1,0:T(8,128)} %bitcast.60, bf16[2,2,16,16,64]{4,3,2,1,0:T(8,128)(2,1)} %bitcast.50, ...), custom_call_target="tpu_custom_call" | custom-call | tf_op jit(solution)/shard_map/mixl/pallas_call | solution.py:222
  9.1 7.3 %all-to-all-start = ((f32[8,40,128]{2,1,0:T(8,128)}), f32[8,40,128]{2,1,0:T(8,128)S(1)}, u32[]{:S(2)}, u32[]{:S(2)}) async-start(f32[8,40,128]{2,1,0:T(8,128)} %get-tuple-element.30), calls=%async_computation | async-start | bytes 327680 | tf_op jit(solution)/shard_map/all_to_all | solution.py:621
  16.4 3.3 %cutk.1 = (bf16[256,384]{1,0:T(8,128)(2,1)}, bf16[256,384]{1,0:T(8,128)(2,1)}, bf16[256,384]{1,0:T(8,128)(2,1)}, bf16[256,384]{1,0:T(8,128)(2,1)}, bf16[256,384]...) custom-call(bf16[256,1536]{1,0:T(8,128)(2,1)} %refs_0_.1, ...), custom_call_target="tpu_custom_call" | custom-call | tf_op jit(solution)/shard_map/cutk/pallas_call | solution.py:367
  32.4 5.7 %collective-permute-done.7 = bf16[256,384]{1,0:T(8,128)(2,1)S(1)} collective-permute-done((bf16[256,384]{1,0:T(8,128)(2,1)}, bf16[256,384]{1,0:T(8,128)(2,1)S(1)}, u32[]{:S(2)}, u32[]{:S(2)}) %collective-permute-start.7) | collective-permute-done | bytes 196640 | tf_op jit(solution)/shard_map/ppermute | solution.py:337
  40.2 9.6 %collective-permute-start.22 = (bf16[384,256]{1,0:T(8,128)(2,1)}, bf16[384,256]{1,0:T(8,128)(2,1)}, u32[]{:S(2)}, u32[]{:S(2)}) collective-permute-start(bf16[384,256]{1,0:T(8,128)(2,1)} %get-tuple-element.44), channel_id=1, source_target_pairs={{0,8},{4,12},{8,16},{12,20},{16,24},{20,28},{24,0},{28,4},{1,9},{5... | collective-permute-start | bytes 589832 | tf_op jit(solution)/shard_map/ppermute | solution.py:382
  51.0 4.9 %collective-permute-start.23 = (bf16[384,256]{1,0:T(8,128)(2,1)}, bf16[384,256]{1,0:T(8,128)(2,1)}, u32[]{:S(2)}, u32[]{:S(2)}) collective-permute-start(bf16[384,256]{1,0:T(8,128)(2,1)} %get-tuple-element.45), channel_id=1, source_target_pairs={{0,16},{4,20},{8,24},{12,28},{16,0},{20,4},{24,8},{28,12},{1,17},{... | collective-permute-start | bytes 589832 | tf_op jit(solution)/shard_map/ppermute | solution.py:382
  55.9 11.4 %collective-permute-start.24 = (bf16[384,256]{1,0:T(8,128)(2,1)}, bf16[384,256]{1,0:T(8,128)(2,1)}, u32[]{:S(2)}, u32[]{:S(2)}) collective-permute-start(bf16[384,256]{1,0:T(8,128)(2,1)} %get-tuple-element.46), channel_id=1, source_target_pairs={{0,24},{4,28},{8,0},{12,4},{16,8},{20,12},{24,16},{28,20},{1,25},{... | collective-permute-start | bytes 589832 | tf_op jit(solution)/shard_map/ppermute | solution.py:382
  70.6 4.5 %mixc.1 = bf16[272,128]{1,0:T(8,128)(2,1)} custom-call(f32[3,2,16]{2,1,0:T(2,128)} %pad_maximum_fusion.4.scal, bf16[256,128]{1,0:T(8,128)(2,1)} %get-tuple-element.28.xt, f32[2,16,128]{2,1,0:T(8,128)} %get-tuple-element.29.rows_a, f32[8,40,128]{2,1,0:T(8,128)} %copy-done.8, f32[2,2,16,16,64]{4,3,2,1,0:T(8,128)} %readout.3, f32[256,128]{1,0:T(8,128)} %get-tuple-element.31.yt, ...), custom_call_target="tpu_custom_call" | custom-call | tf_op jit(solution)/shard_map/mixc/pallas_call | solution.py:240
  75.1 6.0 %all-gather = bf16[1088,128]{1,0:T(8,128)(2,1)S(1)} all-gather(bf16[272,128]{1,0:T(8,128)(2,1)} %mixc.1), channel_id=2, replica_groups=mesh['sp'=8,'tp'=4] {'tp'}, dimensions={0}, use_global_device_ids=true | all-gather | bytes 348160 | tf_op jit(solution)/shard_map/all_gather | solution.py:628
  81.4 3.2 %multiply_reduce_fusion = (f32[32]{0:T(128)S(1)}, f32[32,2048]{1,0:T(8,128)S(1)}) fusion(f32[32]{0:T(128)S(1)} %add_rsqrt_fusion.1, bf16[1024,32]{1,0:T(8,128)(2,1)S(1)} %bitcast.49, bf16[1024,2048]{1,0:T(8,128)(2,1)} %param.22, bf16[32,2048]{1,0:T(8,128)(2,1)S(1)} %copy-done.24), kind=kOutput, calls=%fused_computation.11 | convolution fusion | flops 134676448 | bytes 4653312 | tf_op jit(solution)/shard_map/dot_general | solution.py:633
  89.3 37.4 %collective-permute-done.26.refs_5_ = bf16[384,256]{1,0:T(8,128)(2,1)} collective-permute-done((bf16[384,256]{1,0:T(8,128)(2,1)}, bf16[384,256]{1,0:T(8,128)(2,1)}, u32[]{:S(2)}, u32[]{:S(2)}) %collective-permute-start.26) | collective-permute-done | bytes 196640 | tf_op jit(solution)/shard_map/ppermute | solution.py:385
  127.3 3.6 %collective-permute-done.27.refs_6_ = bf16[384,256]{1,0:T(8,128)(2,1)} collective-permute-done((bf16[384,256]{1,0:T(8,128)(2,1)}, bf16[384,256]{1,0:T(8,128)(2,1)}, u32[]{:S(2)}, u32[]{:S(2)}) %collective-permute-start.27) | collective-permute-done | bytes 196640 | tf_op jit(solution)/shard_map/ppermute | solution.py:385
  131.1 3.5 %collective-permute-done.28.refs_7_ = bf16[384,256]{1,0:T(8,128)(2,1)} collective-permute-done((bf16[384,256]{1,0:T(8,128)(2,1)}, bf16[384,256]{1,0:T(8,128)(2,1)}, u32[]{:S(2)}, u32[]{:S(2)}) %collective-permute-start.28) | collective-permute-done | bytes 196640 | tf_op jit(solution)/shard_map/ppermute | solution.py:385
  135.2 7.5 %collective-permute-done.13.refs_10_ = bf16[32,2048]{1,0:T(8,128)(2,1)S(1)} collective-permute-done((bf16[32,2048]{1,0:T(8,128)(2,1)S(1)}, bf16[32,2048]{1,0:T(8,128)(2,1)S(1)}, u32[]{:S(2)}, u32[]{:S(2)}) %collective-permute-start.13) | collective-permute-done | bytes 131104 | tf_op jit(solution)/shard_map/ppermute | solution.py:644
  143.4 3.1 %collective-permute-done.15.refs_12_ = bf16[32,2048]{1,0:T(8,128)(2,1)S(1)} collective-permute-done((bf16[32,2048]{1,0:T(8,128)(2,1)S(1)}, bf16[32,2048]{1,0:T(8,128)(2,1)S(1)}, u32[]{:S(2)}, u32[]{:S(2)}) %collective-permute-start.15) | collective-permute-done | bytes 131104 | tf_op jit(solution)/shard_map/ppermute | solution.py:644
  146.5 5.0 %collective-permute-done.17.refs_14_ = bf16[32,2048]{1,0:T(8,128)(2,1)S(1)} collective-permute-done((bf16[32,2048]{1,0:T(8,128)(2,1)S(1)}, bf16[32,2048]{1,0:T(8,128)(2,1)S(1)}, u32[]{:S(2)}, u32[]{:S(2)}) %collective-permute-start.17) | collective-permute-done | bytes 131104 | tf_op jit(solution)/shard_map/ppermute | solution.py:644
  152.9 4.4 %collective-permute-done.12.refs_9_ = bf16[32,2048]{1,0:T(8,128)(2,1)S(1)} collective-permute-done((bf16[32,2048]{1,0:T(8,128)(2,1)S(1)}, bf16[32,2048]{1,0:T(8,128)(2,1)S(1)}, u32[]{:S(2)}, u32[]{:S(2)}) %collective-permute-start.12) | collective-permute-done | bytes 131104 | tf_op jit(solution)/shard_map/ppermute | solution.py:337
  158.8 4.2 %collective-permute-done.14.refs_11_ = bf16[32,2048]{1,0:T(8,128)(2,1)S(1)} collective-permute-done((bf16[32,2048]{1,0:T(8,128)(2,1)S(1)}, bf16[32,2048]{1,0:T(8,128)(2,1)S(1)}, u32[]{:S(2)}, u32[]{:S(2)}) %collective-permute-start.14) | collective-permute-done | bytes 131104 | tf_op jit(solution)/shard_map/ppermute | solution.py:337
  164.5 3.5 %collective-permute-done.16.refs_13_ = bf16[32,2048]{1,0:T(8,128)(2,1)S(1)} collective-permute-done((bf16[32,2048]{1,0:T(8,128)(2,1)S(1)}, bf16[32,2048]{1,0:T(8,128)(2,1)S(1)}, u32[]{:S(2)}, u32[]{:S(2)}) %collective-permute-start.16) | collective-permute-done | bytes 131104 | tf_op jit(solution)/shard_map/ppermute | solution.py:337
  169.5 3.5 %collective-permute-done.18.refs_15_ = bf16[32,2048]{1,0:T(8,128)(2,1)S(1)} collective-permute-done((bf16[32,2048]{1,0:T(8,128)(2,1)S(1)}, bf16[32,2048]{1,0:T(8,128)(2,1)S(1)}, u32[]{:S(2)}, u32[]{:S(2)}) %collective-permute-start.18) | collective-permute-done | bytes 131104 | tf_op jit(solution)/shard_map/ppermute | solution.py:337
  175.8 7.1 %upk.1 = (bf16[256,1536]{1,0:T(8,128)(2,1)}, bf16[2,8,1536]{2,1,0:T(8,128)(2,1)}, bf16[4,1536]{1,0:T(4,128)(2,1)}) custom-call(bf16[4,256,384]{2,1,0:T(8,128)(2,1)} %copy-done.1, bf16[4,256,384]{2,1,0:T(8,128)(2,1)} %copy-done.3, bf16[4,256,384]{2,1,0:T(8,128)(2,1)} %copy-done.5, bf16[4,256,384]{2,1,0:T(8,128)(2,1)} %copy-done.7, ...), custom_call_target="tpu_custom_call" | custom-call | tf_op jit(solution)/shard_map/upk/pallas_call | solution.py:543
  183.7 2.9 %collective-permute-done.20.beyond = bf16[4,1536]{1,0:T(4,128)(2,1)S(1)} collective-permute-done((bf16[4,1536]{1,0:T(4,128)(2,1)}, bf16[4,1536]{1,0:T(4,128)(2,1)S(1)}, u32[]{:S(2)}, u32[]{:S(2)}) %collective-permute-start.20) | collective-permute-done | bytes 12320 | tf_op jit(solution)/shard_map/ppermute | solution.py:589
  187.2 5.2 %downk.1 = (bf16[4,32,1024]{2,1,0:T(8,128)(2,1)}, bf16[4,32,1024]{2,1,0:T(8,128)(2,1)}, bf16[4,32,1024]{2,1,0:T(8,128)(2,1)}, bf16[4,32,1024]{2,1,0:T(8,128)(2,1)}) custom-call(bf16[256,1536]{1,0:T(8,128)(2,1)} %get-tuple-element.40.up, bf16[2,8,1536]{2,1,0:T(8,128)(2,1)} %copy-done.25, bf16[4,1536]{1,0:T(4,128)(2,1)} %copy-done.28, f32[6,384]{1,0:T(8,128)} %copy-done.26, ...), custom_call_target="tpu_custom_call" | custom-call | tf_op jit(solution)/shard_map/downk/pallas_call | solution.py:567
  194.5 7.4 %collective-permute-done.37 = bf16[4,32,1024]{2,1,0:T(8,128)(2,1)S(1)} collective-permute-done((bf16[4,32,1024]{2,1,0:T(8,128)(2,1)}, bf16[4,32,1024]{2,1,0:T(8,128)(2,1)S(1)}, u32[]{:S(2)}, u32[]{:S(2)}) %collective-permute-start.37) | collective-permute-done | bytes 262176 | tf_op jit(solution)/shard_map/ppermute | solution.py:337
  (158 shorter events, 54.7 us)
Async XLA Ops:
  9.1 60.8 %all-to-all-start = ((f32[8,40,128]{2,1,0:T(8,128)}), f32[8,40,128]{2,1,0:T(8,128)S(1)}, u32[]{:S(2)}, u32[]{:S(2)}) async-start(f32[8,40,128]{2,1,0:T(8,128)} %get-tuple-element.30), calls=%async_computation | async-start | bytes 327680 | tf_op jit(solution)/shard_map/all_to_all | solution.py:621
  21.7 16.4 %collective-permute-start.7 = (bf16[256,384]{1,0:T(8,128)(2,1)}, bf16[256,384]{1,0:T(8,128)(2,1)S(1)}, u32[]{:S(2)}, u32[]{:S(2)}) collective-permute-start(bf16[256,384]{1,0:T(8,128)(2,1)} %get-tuple-element.38), channel_id=1, source_target_pairs={{0,16},{4,20},{8,24},{12,28},{16,0},{20,4},{24,8},{28,12},{1,17},{... | collective-permute-start | bytes 589832 | tf_op jit(solution)/shard_map/ppermute | solution.py:337
  24.1 16.2 %collective-permute-start.8 = (bf16[256,384]{1,0:T(8,128)(2,1)}, bf16[256,384]{1,0:T(8,128)(2,1)S(1)}, u32[]{:S(2)}, u32[]{:S(2)}) collective-permute-start(bf16[256,384]{1,0:T(8,128)(2,1)} %get-tuple-element.39), channel_id=1, source_target_pairs={{0,24},{4,28},{8,0},{12,4},{16,8},{20,12},{24,16},{28,20},{1,25},{... | collective-permute-start | bytes 589832 | tf_op jit(solution)/shard_map/ppermute | solution.py:337
  25.5 25.4 %collective-permute-start = (bf16[256,384]{1,0:T(8,128)(2,1)}, bf16[256,384]{1,0:T(8,128)(2,1)S(1)}, u32[]{:S(2)}, u32[]{:S(2)}) collective-permute-start(bf16[256,384]{1,0:T(8,128)(2,1)} %get-tuple-element.33), channel_id=1, source_target_pairs={{0,8},{4,12},{8,16},{12,20},{16,24},{20,28},{24,0},{28,4},{1,9},{5... | collective-permute-start | bytes 589832 | tf_op jit(solution)/shard_map/ppermute | solution.py:337
  26.1 29.8 %collective-permute-start.1 = (bf16[256,384]{1,0:T(8,128)(2,1)}, bf16[256,384]{1,0:T(8,128)(2,1)S(1)}, u32[]{:S(2)}, u32[]{:S(2)}) collective-permute-start(bf16[256,384]{1,0:T(8,128)(2,1)} %get-tuple-element.34), channel_id=1, source_target_pairs={{0,16},{4,20},{8,24},{12,28},{16,0},{20,4},{24,8},{28,12},{1,17},{... | collective-permute-start | bytes 589832 | tf_op jit(solution)/shard_map/ppermute | solution.py:337
  29.6 37.7 %collective-permute-start.2 = (bf16[256,384]{1,0:T(8,128)(2,1)}, bf16[256,384]{1,0:T(8,128)(2,1)S(1)}, u32[]{:S(2)}, u32[]{:S(2)}) collective-permute-start(bf16[256,384]{1,0:T(8,128)(2,1)} %get-tuple-element.35), channel_id=1, source_target_pairs={{0,24},{4,28},{8,0},{12,4},{16,8},{20,12},{24,16},{28,20},{1,25},{... | collective-permute-start | bytes 589832 | tf_op jit(solution)/shard_map/ppermute | solution.py:337
  38.1 46.5 %collective-permute-start.21 = (f32[6,384]{1,0:T(8,128)S(1)}, f32[6,384]{1,0:T(8,128)S(1)}, u32[]{:S(2)}, u32[]{:S(2)}) collective-permute-start(f32[6,384]{1,0:T(8,128)S(1)} %dynamic-slice_bitcast_fusion.taps), channel_id=1, source_target_pairs={{0,1},{1,0},{2,3},{3,2},{4,5},{5,4},{6,7},{7,6},{8,9},{9,8},{10,11... | collective-permute-start | bytes 27656 | tf_op jit(solution)/shard_map/ppermute | solution.py:625
  40.2 44.9 %collective-permute-start.22 = (bf16[384,256]{1,0:T(8,128)(2,1)}, bf16[384,256]{1,0:T(8,128)(2,1)}, u32[]{:S(2)}, u32[]{:S(2)}) collective-permute-start(bf16[384,256]{1,0:T(8,128)(2,1)} %get-tuple-element.44), channel_id=1, source_target_pairs={{0,8},{4,12},{8,16},{12,20},{16,24},{20,28},{24,0},{28,4},{1,9},{5... | collective-permute-start | bytes 589832 | tf_op jit(solution)/shard_map/ppermute | solution.py:382
  51.0 34.8 %collective-permute-start.23 = (bf16[384,256]{1,0:T(8,128)(2,1)}, bf16[384,256]{1,0:T(8,128)(2,1)}, u32[]{:S(2)}, u32[]{:S(2)}) collective-permute-start(bf16[384,256]{1,0:T(8,128)(2,1)} %get-tuple-element.45), channel_id=1, source_target_pairs={{0,16},{4,20},{8,24},{12,28},{16,0},{20,4},{24,8},{28,12},{1,17},{... | collective-permute-start | bytes 589832 | tf_op jit(solution)/shard_map/ppermute | solution.py:382
  55.9 31.3 %collective-permute-start.24 = (bf16[384,256]{1,0:T(8,128)(2,1)}, bf16[384,256]{1,0:T(8,128)(2,1)}, u32[]{:S(2)}, u32[]{:S(2)}) collective-permute-start(bf16[384,256]{1,0:T(8,128)(2,1)} %get-tuple-element.46), channel_id=1, source_target_pairs={{0,24},{4,28},{8,0},{12,4},{16,8},{20,12},{24,16},{28,20},{1,25},{... | collective-permute-start | bytes 589832 | tf_op jit(solution)/shard_map/ppermute | solution.py:382
  67.3 20.5 %collective-permute-start.25 = (bf16[384,256]{1,0:T(8,128)(2,1)}, bf16[384,256]{1,0:T(8,128)(2,1)}, u32[]{:S(2)}, u32[]{:S(2)}) collective-permute-start(bf16[384,256]{1,0:T(8,128)(2,1)} %get-tuple-element.43.refs_0_), channel_id=1, source_target_pairs={{0,4},{4,0},{8,12},{12,8},{16,20},{20,16},{24,28},{28,24},{1,5},{5... | collective-permute-start | bytes 589832 | tf_op jit(solution)/shard_map/ppermute | solution.py:385
  85.2 57.6 %collective-permute-start.9 = (bf16[4,256,384]{2,1,0:T(8,128)(2,1)S(1)}, bf16[4,256,384]{2,1,0:T(8,128)(2,1)S(1)}, u32[]{:S(2)}, u32[]{:S(2)}) collective-permute-start(bf16[4,256,384]{2,1,0:T(8,128)(2,1)S(1)} %pad_maximum_fusion.1.refs_4_), channel_id=1, source_target_pairs={{0,4},{4,0},{8,12},{12,8},{16,20},{20,16},{24,28},{28,24},{1,5},{5... | collective-permute-start | bytes 2359304 | tf_op jit(solution)/shard_map/ppermute | solution.py:396
  85.8 57.5 %collective-permute-start.3 = (bf16[4,256,384]{2,1,0:T(8,128)(2,1)S(1)}, bf16[4,256,384]{2,1,0:T(8,128)(2,1)S(1)}, u32[]{:S(2)}, u32[]{:S(2)}) collective-permute-start(bf16[4,256,384]{2,1,0:T(8,128)(2,1)S(1)} %pad_maximum_fusion.refs_0_), channel_id=1, source_target_pairs={{0,4},{4,0},{8,12},{12,8},{16,20},{20,16},{24,28},{28,24},{1,5},{5... | collective-permute-start | bytes 2359304 | tf_op jit(solution)/shard_map/ppermute | solution.py:396
  87.2 39.5 %collective-permute-start.26 = (bf16[384,256]{1,0:T(8,128)(2,1)}, bf16[384,256]{1,0:T(8,128)(2,1)}, u32[]{:S(2)}, u32[]{:S(2)}) collective-permute-start(bf16[384,256]{1,0:T(8,128)(2,1)} %collective-permute-done.22.refs_1_), channel_id=1, source_target_pairs={{0,4},{4,0},{8,12},{12,8},{16,20},{20,16},{24,28},{28,24},{1,5},{5... | collective-permute-start | bytes 589832 | tf_op jit(solution)/shard_map/ppermute | solution.py:385
  87.8 43.2 %collective-permute-start.27 = (bf16[384,256]{1,0:T(8,128)(2,1)}, bf16[384,256]{1,0:T(8,128)(2,1)}, u32[]{:S(2)}, u32[]{:S(2)}) collective-permute-start(bf16[384,256]{1,0:T(8,128)(2,1)} %collective-permute-done.23.refs_2_), channel_id=1, source_target_pairs={{0,4},{4,0},{8,12},{12,8},{16,20},{20,16},{24,28},{28,24},{1,5},{5... | collective-permute-start | bytes 589832 | tf_op jit(solution)/shard_map/ppermute | solution.py:385
  89.3 45.9 %collective-permute-start.30 = (bf16[384,256]{1,0:T(8,128)(2,1)}, bf16[384,256]{1,0:T(8,128)(2,1)S(1)}, u32[]{:S(2)}, u32[]{:S(2)}) collective-permute-start(bf16[384,256]{1,0:T(8,128)(2,1)} %collective-permute-done.22.refs_1_), channel_id=1, source_target_pairs={{0,1},{1,0},{2,3},{3,2},{4,5},{5,4},{6,7},{7,6},{8,9},{9,8},{10,11... | collective-permute-start | bytes 589832 | tf_op jit(solution)/shard_map/ppermute | solution.py:389
  134.6 11.9 %collective-permute-start.15 = (bf16[32,2048]{1,0:T(8,128)(2,1)S(1)}, bf16[32,2048]{1,0:T(8,128)(2,1)S(1)}, u32[]{:S(2)}, u32[]{:S(2)}) collective-permute-start(bf16[32,2048]{1,0:T(8,128)(2,1)S(1)} %multiply_convert_fusion.refs_8_), channel_id=1, source_target_pairs={{0,16},{4,20},{8,24},{12,28},{16,0},{20,4},{24,8},{28,12},{1,17},{... | collective-permute-start | bytes 393224 | tf_op jit(solution)/shard_map/ppermute | solution.py:644
  135.2 37.8 %collective-permute-start.10 = (bf16[4,256,384]{2,1,0:T(8,128)(2,1)S(1)}, bf16[4,256,384]{2,1,0:T(8,128)(2,1)S(1)}, u32[]{:S(2)}, u32[]{:S(2)}) collective-permute-start(bf16[4,256,384]{2,1,0:T(8,128)(2,1)S(1)} %pad_maximum_fusion.1.refs_4_), channel_id=1, source_target_pairs={{0,1},{1,0},{2,3},{3,2},{4,5},{5,4},{6,7},{7,6},{8,9},{9,8},{10,11... | collective-permute-start | bytes 2359304 | tf_op jit(solution)/shard_map/ppermute | solution.py:398
  142.8 30.7 %collective-permute-start.4 = (bf16[4,256,384]{2,1,0:T(8,128)(2,1)S(1)}, bf16[4,256,384]{2,1,0:T(8,128)(2,1)S(1)}, u32[]{:S(2)}, u32[]{:S(2)}) collective-permute-start(bf16[4,256,384]{2,1,0:T(8,128)(2,1)S(1)} %pad_maximum_fusion.refs_0_), channel_id=1, source_target_pairs={{0,1},{1,0},{2,3},{3,2},{4,5},{5,4},{6,7},{7,6},{8,9},{9,8},{10,11... | collective-permute-start | bytes 2359304 | tf_op jit(solution)/shard_map/ppermute | solution.py:398
  142.8 30.8 %collective-permute-start.11 = (bf16[4,256,384]{2,1,0:T(8,128)(2,1)S(1)}, bf16[4,256,384]{2,1,0:T(8,128)(2,1)S(1)}, u32[]{:S(2)}, u32[]{:S(2)}) collective-permute-start(bf16[4,256,384]{2,1,0:T(8,128)(2,1)S(1)} %collective-permute-done.9.refs_5_), channel_id=1, source_target_pairs={{0,1},{1,0},{2,3},{3,2},{4,5},{5,4},{6,7},{7,6},{8,9},{9,8},{10,11... | collective-permute-start | bytes 2359304 | tf_op jit(solution)/shard_map/ppermute | solution.py:399
  143.3 30.7 %collective-permute-start.5 = (bf16[4,256,384]{2,1,0:T(8,128)(2,1)S(1)}, bf16[4,256,384]{2,1,0:T(8,128)(2,1)S(1)}, u32[]{:S(2)}, u32[]{:S(2)}) collective-permute-start(bf16[4,256,384]{2,1,0:T(8,128)(2,1)S(1)} %collective-permute-done.3.refs_1_), channel_id=1, source_target_pairs={{0,1},{1,0},{2,3},{3,2},{4,5},{5,4},{6,7},{7,6},{8,9},{9,8},{10,11... | collective-permute-start | bytes 2359304 | tf_op jit(solution)/shard_map/ppermute | solution.py:399
  173.0 10.2 %collective-permute-start.32 = (bf16[384,256]{1,0:T(8,128)(2,1)}, bf16[384,256]{1,0:T(8,128)(2,1)S(1)}, u32[]{:S(2)}, u32[]{:S(2)}) collective-permute-start(bf16[384,256]{1,0:T(8,128)(2,1)} %collective-permute-done.24.refs_3_), channel_id=1, source_target_pairs={{0,1},{1,0},{2,3},{3,2},{4,5},{5,4},{6,7},{7,6},{8,9},{9,8},{10,11... | collective-permute-start | bytes 589832 | tf_op jit(solution)/shard_map/ppermute | solution.py:389
  173.5 10.2 %collective-permute-start.34 = (bf16[384,256]{1,0:T(8,128)(2,1)}, bf16[384,256]{1,0:T(8,128)(2,1)S(1)}, u32[]{:S(2)}, u32[]{:S(2)}) collective-permute-start(bf16[384,256]{1,0:T(8,128)(2,1)} %collective-permute-done.26.refs_5_), channel_id=1, source_target_pairs={{0,1},{1,0},{2,3},{3,2},{4,5},{5,4},{6,7},{7,6},{8,9},{9,8},{10,11... | collective-permute-start | bytes 589832 | tf_op jit(solution)/shard_map/ppermute | solution.py:389
  194.0 12.8 %collective-permute-start.41 = (bf16[4,32,1024]{2,1,0:T(8,128)(2,1)}, bf16[4,32,1024]{2,1,0:T(8,128)(2,1)S(1)}, u32[]{:S(2)}, u32[]{:S(2)}) collective-permute-start(bf16[4,32,1024]{2,1,0:T(8,128)(2,1)} %get-tuple-element.50), channel_id=1, source_target_pairs={{0,2},{1,3},{2,0},{3,1},{4,6},{5,7},{6,4},{7,5},{8,10},{9,11},{10,... | collective-permute-start | bytes 786440 | tf_op jit(solution)/shard_map/ppermute | solution.py:337
  (52 other events, 960.6 us)
